TPU v7x, 512 devices: a whole 4x8x8 slice. The times are simulated.
512 devices in a mesh: sp: 32 (over z, x), tp: 16 (over y, core).
Axes of the slice: x: 4, y: 8, z: 8, core: 2. Of those that a mesh axis runs over, the one named last changes fastest.
Arguments:
- layer_source_vector: bfloat16 [10240, 2048], P('sp', 'tp'), may hold values from -40 to 40
- attention_lane_source: bfloat16 [10240, 1024], P('sp', 'tp'), may hold values from -6 to 6
- result_valve_logits: bfloat16 [10240, 1024], P('sp', 'tp'), may hold values from -6 to 6
- memory_write_matrix: bfloat16 [10240, 512], P('sp'), may hold values from -6 to 6
- memory_query_matrix: bfloat16 [10240, 512], P('sp'), may hold values from -6 to 6
- increment_logits: bfloat16 [2, 10240, 16], P(None, 'sp', 'tp'), may hold values from -3 to 3
- increment_offset: float32 [2, 16], P(None, 'tp'), may hold values from -16 to -3
- log_fade_speed: float32 [2, 16], P(None, 'tp'), may hold values from 0 to 1.4
- extra_log_fade: float32 [2, 10240, 16], P(None, 'sp', 'tp'), may hold values from -3 to 0
- attention_bypass_factor: float32 [16], P('tp'), may hold values from 0.1 to 1.9
- attention_lane_kernel: bfloat16 [5, 1024], P(None, 'tp'), may hold values from -2.5 to 2.5
- memory_write_kernel: bfloat16 [5, 512], replicated, may hold values from -2.5 to 2.5
- memory_query_kernel: bfloat16 [5, 512], replicated, may hold values from -2.5 to 2.5
- cluster_rescale_factor: float32 [1024], P('tp'), may hold values from 0.1 to 1.9
- blender_result_matrix: bfloat16 [1024, 2048], P(None, 'tp'), may hold values from -0.1875 to 0.1875
- specialist_rescale_factor: float32 [2048], P('tp'), may hold values from 0.1 to 1.9
- chosen_specialists: int32 [10240, 2], P('sp'), may hold values from 0 to 31, all different within a row; in each aligned block of 320 rows (0 to 319, 320 to 639, ...) at most 30 rows name the same one
- specialist_shares: float32 [10240, 2], P('sp'), may hold values from 0.25 to 1.25
- specialist_valve_matrix: bfloat16 [32, 2048, 2048], P('sp', None, 'tp'), may hold values from -0.125 to 0.125
- specialist_raising_matrix: bfloat16 [32, 2048, 2048], P('sp', None, 'tp'), may hold values from -0.125 to 0.125
- specialist_lowering_matrix: bfloat16 [32, 2048, 2048], P('sp', None, 'tp'), may hold values from -0.125 to 0.125
- common_valve_matrix: bfloat16 [2048, 2048], P(None, 'tp'), may hold values from -0.125 to 0.125
- common_raising_matrix: bfloat16 [2048, 2048], P(None, 'tp'), may hold values from -0.125 to 0.125
- common_lowering_matrix: bfloat16 [2048, 2048], P(None, 'tp'), may hold values from -0.125 to 0.125
Outputs:
- result: bfloat16 [10240, 2048], P('sp', 'tp')
Inputs may be any that keep to these rules, and one draw needn't show every extreme that they name: `chosen_specialists`: each row names 2 different experts; among the rows of one index of sp no expert is named more than 30 times, a bound that some block reaches there.
All inputs are finite; a program needn't handle non-finite values.
Results may differ from a plain program's by a relative error of at most 0.013.
Values may be sent and summed in bfloat16 or wider, within the bound.
A program may use at most 64 MiB of HBM per device.

v0:
```python
import jax
import jax.numpy as jnp
from jax import lax
from jax.sharding import PartitionSpec as P

D = 2048
HEADS = 16
HEAD_DIM = 64
GROUPS = 4
STATE = 128
CONV = 5


def extended(cells, sides, width):
    for axis, dim in sides:
        count = lax.axis_size(axis)
        ends = count - 1
        head = lax.slice_in_dim(cells, 0, width, axis=dim)
        tail = lax.slice_in_dim(cells, cells.shape[dim] - width, cells.shape[dim], axis=dim)
        cells = jnp.concatenate(
            [
                lax.ppermute(tail, axis, [(i, (i + 1) % count) for i in range(ends)]),
                cells,
                lax.ppermute(head, axis, [((i + 1) % count, i) for i in range(ends)]),
            ],
            axis=dim,
        )
    return cells


def from_everyone(shard, axis):
    peers = lax.axis_size(axis)
    return lax.all_to_all(
        jnp.broadcast_to(shard[None], (peers, *shard.shape)), axis, 0, 0, tiled=True
    )


def gathered_once(shard, axis):
    leaves = jax.tree.leaves(shard)
    turns = sorted(range(len(leaves)), key=lambda k: -leaves[k].size)
    width = (1, *leaves[turns[0]].shape)[-1]
    lines = [
        jnp.pad(leaves[k].reshape(-1), (0, -leaves[k].size % width)).reshape(-1, width)
        for k in turns
    ]
    both, at, found = (from_everyone(jnp.concatenate(lines), axis), 0, {})
    for k, line in zip(turns, lines):
        piece = both[:, at : at + len(line)].reshape(len(both), -1)
        found[k] = piece[:, : leaves[k].size].reshape(-1, *leaves[k].shape)
        at += len(line)
    numbers = iter(range(len(leaves)))
    return jax.tree.map(lambda _: found[next(numbers)], shard)


def folded_in_pairs(pieces, combine):
    while len(jax.tree.leaves(pieces)[0]) > 1:
        pieces = jax.vmap(combine)(
            *(jax.tree.map(lambda part: part[side::2], pieces) for side in (0, 1))
        )
    return jax.tree.map(lambda part: part[0], pieces)


def entering(shard, axis, combine, identity, reverse):
    peers, place = (lax.axis_size(axis), lax.axis_index(axis))
    passed = jnp.arange(peers) > place if reverse else jnp.arange(peers) < place

    def kept(part, zero, own):
        part = jnp.where(
            passed.reshape(-1, *(1 for _ in own.shape)),
            part.astype(own.dtype),
            jnp.asarray(zero, own.dtype),
        )
        return part[::-1] if reverse else part

    pieces = gathered_once(
        jax.tree.map(lambda part, kind: part.astype(kind), shard, (jnp.bfloat16, jnp.bfloat16)),
        axis,
    )
    return folded_in_pairs(jax.tree.map(kept, pieces, identity, shard), combine)


def over_copies(shard, axis):
    return from_everyone(shard, axis).sum(axis=0)


def laid_out(tiles, dim):
    lengths = list(tiles.shape[1:])
    lengths[dim] *= tiles.shape[0]
    return jnp.moveaxis(tiles, 0, dim).reshape(lengths)


def gathered_copies(shard, axis, dim):
    return laid_out(from_everyone(shard, axis), dim)


def side_by_side(arrays, axis, dim, along):
    both = jnp.concatenate(arrays, axis=along)
    result, at, gathered = (lax.all_gather(both, axis, axis=dim, tiled=True), 0, [])
    for a in arrays:
        gathered.append(lax.slice_in_dim(result, at, at + a.shape[along], axis=along))
        at += a.shape[along]
    return tuple(gathered)


def combine_states(earlier, later):
    return (earlier[0] + later[0], jnp.exp(later[0])[:, None, None] * earlier[1] + later[1])


def shards(
    layer_source_vector,
    attention_lane_source,
    result_valve_logits,
    memory_write_matrix,
    memory_query_matrix,
    increment_logits,
    increment_offset,
    log_fade_speed,
    extra_log_fade,
    attention_bypass_factor,
    attention_lane_kernel,
    memory_write_kernel,
    memory_query_kernel,
    cluster_rescale_factor,
    blender_result_matrix,
    specialist_rescale_factor,
    chosen_specialists,
    specialist_shares,
    specialist_valve_matrix,
    specialist_raising_matrix,
    specialist_lowering_matrix,
    common_valve_matrix,
    common_raising_matrix,
    common_lowering_matrix,
):
    length = attention_lane_source.shape[0]
    heads_here = increment_offset.shape[1]
    channels = attention_lane_source.shape[1]
    head_size = channels // heads_here
    spread = HEADS // GROUPS
    group = lax.axis_index("tp") * heads_here // spread
    b_own = lax.dynamic_slice_in_dim(memory_write_matrix, group * STATE, STATE, 1)
    c_own = lax.dynamic_slice_in_dim(memory_query_matrix, group * STATE, STATE, 1)
    joined = jnp.concatenate([attention_lane_source, b_own, c_own], axis=1)
    taps = jnp.concatenate(
        [
            attention_lane_kernel,
            lax.dynamic_slice_in_dim(memory_write_kernel, group * STATE, STATE, 1),
            lax.dynamic_slice_in_dim(memory_query_kernel, group * STATE, STATE, 1),
        ],
        axis=1,
    )
    padded = extended(joined, (("sp", 0),), CONV // 2)
    total = jnp.zeros(joined.shape, jnp.float32)
    for offset in range(CONV):
        total = total + padded[offset : offset + length].astype(jnp.float32) * taps[offset].astype(
            jnp.float32
        )
    convolved = jax.nn.silu(total).astype(jnp.bfloat16)
    x_conv = convolved[:, :channels].reshape(length, heads_here, head_size)
    b_conv = convolved[:, channels : channels + STATE]
    c_conv = convolved[:, channels + STATE :]
    increment_lengths = jax.nn.softplus(
        increment_logits.astype(jnp.float32) + increment_offset[:, None, :]
    )
    log_fade_amount = -jnp.exp(log_fade_speed)[:, None, :] * increment_lengths + extra_log_fade
    forward_cum = jnp.cumsum(log_fade_amount[0], axis=0)
    backward_cum = jnp.cumsum(log_fade_amount[1], axis=0) - log_fade_amount[1]
    forward_total = forward_cum[-1]
    backward_total = backward_cum[-1] + log_fade_amount[1][-1]
    scores = lax.dot_general(
        c_conv, b_conv, (((1,), (1,)), ((), ())), preferred_element_type=jnp.float32
    )
    position = jnp.arange(length)
    lower = position[:, None] >= position[None, :]
    upper = position[:, None] <= position[None, :]
    forward_gap = forward_cum.T[:, :, None] - forward_cum.T[:, None, :]
    backward_gap = backward_cum.T[:, None, :] - backward_cum.T[:, :, None]
    forward_part = (
        jnp.where(lower, jnp.exp(jnp.where(lower, forward_gap, 0.0)), 0.0)
        * increment_lengths[0].T[:, None, :]
    )
    backward_part = (
        jnp.where(upper, jnp.exp(jnp.where(upper, backward_gap, 0.0)), 0.0)
        * increment_lengths[1].T[:, None, :]
    )
    mixing = (scores[None] * (forward_part + backward_part)).astype(jnp.bfloat16)
    inner = jnp.einsum("hts,shp->thp", mixing, x_conv, preferred_element_type=jnp.float32)
    forward_scale = jnp.exp(forward_total[None, :] - forward_cum) * increment_lengths[0]
    backward_scale = jnp.exp(backward_cum) * increment_lengths[1]
    scaled = (
        jnp.stack([forward_scale, backward_scale])[..., None] * x_conv.astype(jnp.float32)[None]
    ).astype(jnp.bfloat16)
    own_states = jnp.einsum("dshp,sn->dhpn", scaled, b_conv, preferred_element_type=jnp.float32)
    own_logs = jnp.stack([forward_total, backward_total])
    empty = (jnp.zeros_like(own_logs[0]), jnp.zeros_like(own_states[0]))
    carried_forward = entering((own_logs[0], own_states[0]), "sp", combine_states, empty, False)[1]
    carried_backward = entering((own_logs[1], own_states[1]), "sp", combine_states, empty, True)[1]
    carried = jnp.stack([carried_forward, carried_backward]).astype(jnp.bfloat16)
    readout = jnp.einsum("tn,dhpn->dthp", c_conv, carried, preferred_element_type=jnp.float32)
    mixer = (
        inner
        + jnp.exp(forward_cum)[..., None] * readout[0]
        + jnp.exp(backward_total[None, :] - backward_cum)[..., None] * readout[1]
        + attention_bypass_factor[None, :, None] * x_conv.astype(jnp.float32)
    )
    gated = mixer * jax.nn.silu(result_valve_logits.astype(jnp.float32)).reshape(
        length, heads_here, head_size
    )
    squares = jnp.sum(gated * gated, axis=(1, 2))
    group_marks = (jnp.arange(GROUPS) == group).astype(jnp.float32)
    group_sums = over_copies(squares[:, None] * group_marks[None, :], "tp")
    own_sum = lax.dynamic_index_in_dim(group_sums, group, 1, keepdims=False)
    scale = lax.rsqrt(own_sum / (spread * HEAD_DIM) + 1e-06)
    normed = (
        gated.reshape(length, channels) * scale[:, None] * cluster_rescale_factor[None, :]
    ).astype(jnp.bfloat16)
    projected = jnp.dot(
        gathered_copies(normed, "tp", 1), blender_result_matrix, preferred_element_type=jnp.float32
    )
    after_mixer = (layer_source_vector.astype(jnp.float32) + projected).astype(jnp.bfloat16)
    resid = after_mixer.astype(jnp.float32)
    total_squares = over_copies(jnp.sum(resid * resid, axis=1), "tp")
    features = (
        resid * lax.rsqrt(total_squares / D + 1e-06)[:, None] * specialist_rescale_factor[None, :]
    ).astype(jnp.bfloat16)
    full_features = gathered_copies(features, "tp", 1)
    shared_hidden = (
        jax.nn.silu(jnp.dot(full_features, common_valve_matrix, preferred_element_type=jnp.float32))
        * jnp.dot(full_features, common_raising_matrix, preferred_element_type=jnp.float32)
    ).astype(jnp.bfloat16)
    top = chosen_specialists.shape[1]
    experts = lax.axis_size("sp")
    capacity = 3 * length * top // (2 * experts)
    flat = chosen_specialists.reshape(-1)
    one_hot = (flat[:, None] == jnp.arange(experts, dtype=jnp.int32)[None, :]).astype(jnp.int32)
    rank = jnp.sum((jnp.cumsum(one_hot, axis=0) - one_hot) * one_hot, axis=1)
    slot = flat * capacity + rank
    token = jnp.arange(length * top, dtype=jnp.int32) // top
    owner = jnp.zeros((experts * capacity,), jnp.int32).at[slot].set(token)
    filled = jnp.zeros((experts * capacity,), jnp.bool_).at[slot].set(True)
    outgoing = jnp.where(
        filled[:, None], jnp.take(features, owner, axis=0), jnp.zeros((), jnp.bfloat16)
    ).reshape(experts, capacity, -1)
    shares = lax.all_to_all(outgoing, "sp", split_axis=0, concat_axis=0, tiled=True)
    arrived = lax.all_gather(shares, "tp", axis=2, tiled=True)
    arrived = arrived.reshape(-1, arrived.shape[2])
    expert_hidden = (
        jax.nn.silu(
            jnp.dot(arrived, specialist_valve_matrix[0], preferred_element_type=jnp.float32)
        )
        * jnp.dot(arrived, specialist_raising_matrix[0], preferred_element_type=jnp.float32)
    ).astype(jnp.bfloat16)
    expert_all, shared_all = side_by_side((expert_hidden, shared_hidden), "tp", 1, 0)
    expert_out = jnp.dot(
        expert_all, specialist_lowering_matrix[0], preferred_element_type=jnp.float32
    ).astype(jnp.bfloat16)
    shared_out = jnp.dot(
        shared_all, common_lowering_matrix, preferred_element_type=jnp.float32
    ).astype(jnp.bfloat16)
    returned = lax.all_to_all(
        expert_out.reshape(experts, capacity, -1), "sp", split_axis=0, concat_axis=0, tiled=True
    )
    picked = jnp.take(returned.reshape(experts * capacity, -1), slot, axis=0).astype(jnp.float32)
    picked = picked.reshape(length, top, -1)
    routed = jnp.sum(picked * specialist_shares[:, :, None], axis=1)
    return (resid + shared_out.astype(jnp.float32) + routed).astype(jnp.bfloat16)


def solution(mesh):
    return jax.shard_map(
        shards,
        mesh=mesh,
        in_specs=(
            P("sp", "tp"),
            P("sp", "tp"),
            P("sp", "tp"),
            P("sp", None),
            P("sp", None),
            P(None, "sp", "tp"),
            P(None, "tp"),
            P(None, "tp"),
            P(None, "sp", "tp"),
            P("tp"),
            P(None, "tp"),
            P(),
            P(),
            P("tp"),
            P(None, "tp"),
            P("tp"),
            P("sp", None),
            P("sp", None),
            P("sp", None, "tp"),
            P("sp", None, "tp"),
            P("sp", None, "tp"),
            P(None, "tp"),
            P(None, "tp"),
            P(None, "tp"),
        ),
        out_specs=P("sp", "tp"),
        check_vma=False,
    )
```

profile of v0, /device:TPU:1, one launch (start us, length us, event | category | flops | bytes accessed | tf_op | source)
XLA Modules:
  0.0 324.1 jit_solution(10892311120303256452)
XLA Ops:
  8.8 3.9 %collective-permute-start = (bf16[2,320]{0,1:T(8,128)(2,1)S(1)}, bf16[2,320]{0,1:T(8,128)(2,1)S(1)}, u32[]{:S(2)}, u32[]{:S(2)}) collective-permute-start(bf16[2,320]{0,1:T(8,128)(2,1)S(1)} %get-tuple-element.24), channel_id=1, source_target_pairs={{0,16},{16,32},{32,48},{48,64},{64,80},{80,96},{96,112},{112,128},... | collective-permute-start | bytes 3848 | tf_op jit(solution)/shard_map/ppermute | solution.py:22
  20.5 14.6 %all-to-all-start = ((bf16[32,65,128]{2,1,0:T(8,128)(2,1)}), bf16[32,65,128]{2,1,0:T(8,128)(2,1)S(1)}, u32[]{:S(2)}, u32[]{:S(2)}) async-start(bf16[32,65,128]{2,1,0:T(8,128)(2,1)} %broadcast_in_dim.82), calls=%async_computation | async-start | bytes 1179648 | tf_op jit(solution)/shard_map/all_to_all | solution.py:33
  38.9 12.7 %all-to-all-done = bf16[32,65,128]{2,1,0:T(8,128)(2,1)S(1)} async-done(((bf16[32,65,128]{2,1,0:T(8,128)(2,1)}), bf16[32,65,128]{2,1,0:T(8,128)(2,1)S(1)}, u32[]{:S(2)}, u32[]{:S(2)}) %all-to-all-start) | async-done | bytes 532512 | tf_op jit(solution)/shard_map/all_to_all | solution.py:33
  52.6 6.2 %all-to-all-start.1 = ((bf16[32,65,128]{2,1,0:T(8,128)(2,1)}), bf16[32,65,128]{2,1,0:T(8,128)(2,1)S(1)}, u32[]{:S(2)}, u32[]{:S(2)}) async-start(bf16[32,65,128]{2,1,0:T(8,128)(2,1)} %broadcast_in_dim.89), calls=%async_computation.1 | async-start | bytes 1179648 | tf_op jit(solution)/shard_map/all_to_all | solution.py:33
  60.0 15.0 %all-to-all-done.1 = bf16[32,65,128]{2,1,0:T(8,128)(2,1)S(1)} async-done(((bf16[32,65,128]{2,1,0:T(8,128)(2,1)}), bf16[32,65,128]{2,1,0:T(8,128)(2,1)S(1)}, u32[]{:S(2)}, u32[]{:S(2)}) %all-to-all-start.1) | async-done | bytes 532512 | tf_op jit(solution)/shard_map/all_to_all | solution.py:33
  81.0 11.1 %all-to-all-start.2 = ((f32[16,320,4]{1,2,0:T(4,128)}), f32[16,320,4]{1,2,0:T(4,128)S(1)}, u32[]{:S(2)}, u32[]{:S(2)}) async-start(f32[16,320,4]{1,2,0:T(4,128)} %broadcast_in_dim.95), calls=%async_computation.2 | async-start | bytes 196608 | tf_op jit(solution)/shard_map/all_to_all | solution.py:33
  92.4 8.2 %all-to-all-done.2 = f32[16,320,4]{1,2,0:T(4,128)S(1)} async-done(((f32[16,320,4]{1,2,0:T(4,128)}), f32[16,320,4]{1,2,0:T(4,128)S(1)}, u32[]{:S(2)}, u32[]{:S(2)}) %all-to-all-start.2) | async-done | bytes 81952 | tf_op jit(solution)/shard_map/all_to_all | solution.py:33
  101.7 3.6 %all-to-all-start.3 = ((bf16[16,320,64]{1,2,0:T(8,128)(2,1)}), bf16[16,320,64]{1,2,0:T(8,128)(2,1)S(1)}, u32[]{:S(2)}, u32[]{:S(2)}) async-start(bf16[16,320,64]{1,2,0:T(8,128)(2,1)} %broadcast_in_dim.96), calls=%async_computation.3 | async-start | bytes 1572864 | tf_op jit(solution)/shard_map/all_to_all | solution.py:33
  107.7 4.1 %scatter_custom_fusion.1 = s32[960]{0:T(1024)S(1)} fusion(s32[640]{0:T(1024)S(1)} %fusion.100, s32[640]{0:T(1024)S(1)} %add_select_fusion, s32[]{:T(128)} %constant.96.clone.1), kind=kCustom, calls=%fused_computation.164 | custom fusion | bytes 3844 | tf_op jit(solution)/shard_map/scatter | solution.py:239
  111.8 16.1 %all-to-all-done.3 = bf16[16,320,64]{1,2,0:T(8,128)(2,1)S(1)} async-done(((bf16[16,320,64]{1,2,0:T(8,128)(2,1)}), bf16[16,320,64]{1,2,0:T(8,128)(2,1)S(1)}, u32[]{:S(2)}, u32[]{:S(2)}) %all-to-all-start.3) | async-done | bytes 655392 | tf_op jit(solution)/shard_map/all_to_all | solution.py:33
  129.1 3.4 %all-to-all-start.4 = ((f32[16,1,320]{2,1,0:T(1,128)}), f32[16,1,320]{2,1,0:T(1,128)S(1)}, u32[]{:S(2)}, u32[]{:S(2)}) async-start(f32[16,1,320]{2,1,0:T(1,128)} %broadcast_in_dim.174), calls=%async_computation.4 | async-start | bytes 49152 | tf_op jit(solution)/shard_map/all_to_all | solution.py:33
  132.7 2.9 scatter_custom_fusion
  135.7 3.8 %all-to-all-done.4 = f32[16,1,320]{2,1,0:T(1,128)S(1)} async-done(((f32[16,1,320]{2,1,0:T(1,128)}), f32[16,1,320]{2,1,0:T(1,128)S(1)}, u32[]{:S(2)}, u32[]{:S(2)}) %all-to-all-start.4) | async-done | bytes 20512 | tf_op jit(solution)/shard_map/all_to_all | solution.py:33
  139.7 3.3 %gather_fusion = bf16[960,128]{1,0:T(8,128)(2,1)S(1)} fusion(bf16[320,128]{1,0:T(8,128)(2,1)S(1)} %multiply_convert_fusion.2, s32[1024]{0:T(1024)S(1)} %pad_clamp_fusion.1), kind=kCustom, calls=%fused_computation | custom fusion | bytes 495360 | tf_op jit(solution)/shard_map/jit(_take)/gather | solution.py:242
  143.4 15.9 %all_to_all.41 = bf16[32,30,128]{2,1,0:T(8,128)(2,1)} all-to-all(bf16[32,30,128]{2,1,0:T(8,128)(2,1)S(1)} %select_select_fusion), channel_id=1, replica_groups=mesh['sp'=32,'tp'=16] {'sp'}, dimensions={0} | all-to-all | bytes 491520 | tf_op jit(solution)/shard_map/all_to_all | solution.py:244
  159.7 47.9 %all_to_all.42 = bf16[16,320,128]{2,1,0:T(8,128)(2,1)S(1)} all-to-all(bf16[16,320,128]{2,1,0:T(8,128)(2,1)S(1)} %broadcast_in_dim.178), channel_id=1, replica_groups=mesh['sp'=32,'tp'=16] {'tp'}, dimensions={0} | all-to-all | bytes 2621440 | tf_op jit(solution)/shard_map/all_to_all | solution.py:33
  209.2 15.8 %all-gather.3.cloned.1.call-done = bf16[32,30,2048]{2,1,0:T(8,128)(2,1)} async-done(((bf16[32,30,128]{2,1,0:T(8,128)(2,1)}), bf16[32,30,2048]{2,1,0:T(8,128)(2,1)}) %all-gather.3.cloned.1.call-update) | async-done | bytes 3932176 | tf_op jit(solution)/shard_map/all_gather | solution.py:245
  225.0 5.0 %reshape.638 = bf16[960,2048]{1,0:T(8,128)(2,1)} reshape(bf16[32,30,2048]{2,1,0:T(8,128)(2,1)} %all-gather.3.cloned.1.call-done) | data formatting | bytes 7864320 | tf_op jit(solution)/shard_map/reshape | solution.py:246
  230.0 3.4 %fusion.46 = f32[960,128]{1,0:T(8,128)S(1)} fusion(bf16[960,2048]{1,0:T(8,128)(2,1)} %reshape.638, bf16[1,2048,128]{2,1,0:T(8,128)(2,1)S(1)} %copy-done), kind=kOutput, calls=%fused_computation.41 | convolution fusion | flops 503316480 | bytes 4947968 | tf_op jit(solution)/shard_map/dot_general | solution.py:249
  235.4 51.8 %all-gather.5.cloned.1.call-done = bf16[1280,2048]{1,0:T(8,128)(2,1)} async-done(((bf16[1280,128]{1,0:T(8,128)(2,1)}), bf16[1280,2048]{1,0:T(8,128)(2,1)}) %all-gather.5.cloned.1.call-update) | async-done | bytes 5242896 | tf_op jit(solution)/shard_map/all_gather | solution.py:98
  287.2 3.3 %fusion.8 = bf16[960,128]{1,0:T(8,128)(2,1)S(1)} fusion(bf16[1280,2048]{1,0:T(8,128)(2,1)} %all-gather.5.cloned.1.call-done, bf16[1,2048,128]{2,1,0:T(8,128)(2,1)S(1)} %copy-done.16), kind=kOutput, calls=%fused_computation.14 | convolution fusion | flops 503439360 | bytes 4702208 | tf_op jit(solution)/shard_map/dot_general | solution.py:254
  291.3 7.7 %all-to-all-start.7 = ((bf16[32,30,128]{2,1,0:T(8,128)(2,1)}), bf16[32,30,128]{2,1,0:T(8,128)(2,1)S(1)}, u32[]{:S(2)}, u32[]{:S(2)}) async-start(bf16[32,30,128]{2,1,0:T(8,128)(2,1)} %reshape.640), calls=%async_computation.7 | async-start | bytes 524288 | tf_op jit(solution)/shard_map/all_to_all | solution.py:260
  299.7 11.0 %all-to-all-done.7 = bf16[32,30,128]{2,1,0:T(8,128)(2,1)S(1)} async-done(((bf16[32,30,128]{2,1,0:T(8,128)(2,1)}), bf16[32,30,128]{2,1,0:T(8,128)(2,1)S(1)}, u32[]{:S(2)}, u32[]{:S(2)}) %all-to-all-start.7) | async-done | bytes 245792 | tf_op jit(solution)/shard_map/all_to_all | solution.py:260
  314.8 2.5 fusion.36
  (195 shorter events, 32.0 us)
Async XLA Ops:
  6.5 223.4 %copy-start = (bf16[1,2048,128]{2,1,0:T(8,128)(2,1)S(1)}, bf16[1,2048,128]{2,1,0:T(8,128)(2,1)}, u32[]{:S(2)}) copy-start(bf16[1,2048,128]{2,1,0:T(8,128)(2,1)} %param.42) | copy-start | bytes 1572868
  6.5 12.1 %copy-start.2 = (bf16[320,64]{0,1:T(8,128)(2,1)S(1)}, bf16[320,64]{0,1:T(8,128)(2,1)}, u32[]{:S(2)}) copy-start(bf16[320,64]{0,1:T(8,128)(2,1)} %param.25) | copy-start | bytes 122884
  6.5 8.3 %copy-start.12 = (f32[2,1]{0,1:T(1,128)S(1)}, f32[2,1]{0,1:T(1,128)}, u32[]{:S(2)}) copy-start(f32[2,1]{0,1:T(1,128)} %param.30) | copy-start | bytes 28
  6.5 8.3 %copy-start.9 = (bf16[2,320,1]{1,0,2:T(2,128)(2,1)S(1)}, bf16[2,320,1]{1,0,2:T(2,128)(2,1)}, u32[]{:S(2)}) copy-start(bf16[2,320,1]{1,0,2:T(2,128)(2,1)} %param.29) | copy-start | bytes 3844
  6.6 8.3 %copy-start.6 = (f32[2,320,1]{1,2,0:T(1,128)S(1)}, f32[2,320,1]{1,2,0:T(1,128)}, u32[]{:S(2)}) copy-start(f32[2,320,1]{1,2,0:T(1,128)} %param.32) | copy-start | bytes 7684
  8.8 9.8 %collective-permute-start = (bf16[2,320]{0,1:T(8,128)(2,1)S(1)}, bf16[2,320]{0,1:T(8,128)(2,1)S(1)}, u32[]{:S(2)}, u32[]{:S(2)}) collective-permute-start(bf16[2,320]{0,1:T(8,128)(2,1)S(1)} %get-tuple-element.24), channel_id=1, source_target_pairs={{0,16},{16,32},{32,48},{48,64},{64,80},{80,96},{96,112},{112,128},... | collective-permute-start | bytes 3848 | tf_op jit(solution)/shard_map/ppermute | solution.py:22
  12.7 5.9 %collective-permute-start.1 = (bf16[2,320]{0,1:T(8,128)(2,1)S(1)}, bf16[2,320]{0,1:T(8,128)(2,1)S(1)}, u32[]{:S(2)}, u32[]{:S(2)}) collective-permute-start(bf16[2,320]{0,1:T(8,128)(2,1)S(1)} %get-tuple-element.25), channel_id=1, source_target_pairs={{16,0},{32,16},{48,32},{64,48},{80,64},{96,80},{112,96},{128,112},... | collective-permute-start | bytes 3848 | tf_op jit(solution)/shard_map/ppermute | solution.py:24
  20.5 31.1 %all-to-all-start = ((bf16[32,65,128]{2,1,0:T(8,128)(2,1)}), bf16[32,65,128]{2,1,0:T(8,128)(2,1)S(1)}, u32[]{:S(2)}, u32[]{:S(2)}) async-start(bf16[32,65,128]{2,1,0:T(8,128)(2,1)} %broadcast_in_dim.82), calls=%async_computation | async-start | bytes 1179648 | tf_op jit(solution)/shard_map/all_to_all | solution.py:33
  52.6 22.4 %all-to-all-start.1 = ((bf16[32,65,128]{2,1,0:T(8,128)(2,1)}), bf16[32,65,128]{2,1,0:T(8,128)(2,1)S(1)}, u32[]{:S(2)}, u32[]{:S(2)}) async-start(bf16[32,65,128]{2,1,0:T(8,128)(2,1)} %broadcast_in_dim.89), calls=%async_computation.1 | async-start | bytes 1179648 | tf_op jit(solution)/shard_map/all_to_all | solution.py:33
  79.8 12.2 %copy-start.5 = (s32[320,2]{0,1:T(2,128)S(1)}, s32[320,2]{0,1:T(2,128)}, u32[]{:S(2)}) copy-start(s32[320,2]{0,1:T(2,128)} %param.40) | copy-start | bytes 7684
  79.9 20.8 %copy-start.10 = (f32[64]{0:T(128)S(1)}, f32[64]{0:T(128)}, u32[]{:S(2)}) copy-start(f32[64]{0:T(128)} %param.37) | copy-start | bytes 772
  81.0 19.5 %all-to-all-start.2 = ((f32[16,320,4]{1,2,0:T(4,128)}), f32[16,320,4]{1,2,0:T(4,128)S(1)}, u32[]{:S(2)}, u32[]{:S(2)}) async-start(f32[16,320,4]{1,2,0:T(4,128)} %broadcast_in_dim.95), calls=%async_computation.2 | async-start | bytes 196608 | tf_op jit(solution)/shard_map/all_to_all | solution.py:33
  101.7 26.3 %copy-start.3 = (bf16[1024,128]{1,0:T(8,128)(2,1)S(1)}, bf16[1024,128]{1,0:T(8,128)(2,1)}, u32[]{:S(2)}) copy-start(bf16[1024,128]{1,0:T(8,128)(2,1)} %param.38) | copy-start | bytes 786436
  101.7 26.3 %copy-start.4 = (bf16[320,128]{1,0:T(8,128)(2,1)S(1)}, bf16[320,128]{1,0:T(8,128)(2,1)}, u32[]{:S(2)}) copy-start(bf16[320,128]{1,0:T(8,128)(2,1)} %param.24) | copy-start | bytes 245764
  101.7 26.3 %all-to-all-start.3 = ((bf16[16,320,64]{1,2,0:T(8,128)(2,1)}), bf16[16,320,64]{1,2,0:T(8,128)(2,1)S(1)}, u32[]{:S(2)}, u32[]{:S(2)}) async-start(bf16[16,320,64]{1,2,0:T(8,128)(2,1)} %broadcast_in_dim.96), calls=%async_computation.3 | async-start | bytes 1572864 | tf_op jit(solution)/shard_map/all_to_all | solution.py:33
  105.3 34.2 %copy-start.11 = (f32[128]{0:T(128)S(1)}, f32[128]{0:T(128)}, u32[]{:S(2)}) copy-start(f32[128]{0:T(128)} %param.39) | copy-start | bytes 1540
  129.1 10.4 %all-to-all-start.4 = ((f32[16,1,320]{2,1,0:T(1,128)}), f32[16,1,320]{2,1,0:T(1,128)S(1)}, u32[]{:S(2)}, u32[]{:S(2)}) async-start(f32[16,1,320]{2,1,0:T(1,128)} %broadcast_in_dim.174), calls=%async_computation.4 | async-start | bytes 49152 | tf_op jit(solution)/shard_map/all_to_all | solution.py:33
  132.5 92.5 %all-gather.3.cloned.1.call-start = ((), (), s32[]{:S(2)}) async-start(), calls=%async_computation.8 | async-start | bytes 4456448 | tf_op jit(solution)/shard_map/all_gather | solution.py:245
  159.4 127.8 %all-gather.5.cloned.1.call-start = ((), (), s32[]{:S(2)}) async-start(), calls=%async_computation.9 | async-start | bytes 5570560 | tf_op jit(solution)/shard_map/all_gather | solution.py:98
  159.7 48.0 %copy-start.13 = (bf16[2048,128]{1,0:T(8,128)(2,1)S(1)}, bf16[2048,128]{1,0:T(8,128)(2,1)}, u32[]{:S(2)}) copy-start(bf16[2048,128]{1,0:T(8,128)(2,1)} %param.45) | copy-start | bytes 1572868
  233.4 53.8 %copy-start.16 = (bf16[1,2048,128]{2,1,0:T(8,128)(2,1)S(1)}, bf16[1,2048,128]{2,1,0:T(8,128)(2,1)}, u32[]{:S(2)}) copy-start(bf16[1,2048,128]{2,1,0:T(8,128)(2,1)} %param.44) | copy-start | bytes 1572868
  290.5 9.0 %copy-start.7 = (f32[320,2]{0,1:T(2,128)S(1)}, f32[320,2]{0,1:T(2,128)}, u32[]{:S(2)}) copy-start(f32[320,2]{0,1:T(2,128)} %param.41) | copy-start | bytes 7684
  291.3 19.4 %all-to-all-start.7 = ((bf16[32,30,128]{2,1,0:T(8,128)(2,1)}), bf16[32,30,128]{2,1,0:T(8,128)(2,1)S(1)}, u32[]{:S(2)}, u32[]{:S(2)}) async-start(bf16[32,30,128]{2,1,0:T(8,128)(2,1)} %reshape.640), calls=%async_computation.7 | async-start | bytes 524288 | tf_op jit(solution)/shard_map/all_to_all | solution.py:260
  299.5 15.3 %copy-start.17 = (bf16[2048,128]{1,0:T(8,128)(2,1)S(1)}, bf16[2048,128]{1,0:T(8,128)(2,1)}, u32[]{:S(2)}) copy-start(bf16[2048,128]{1,0:T(8,128)(2,1)} %param.47) | copy-start | bytes 1572868
  (6 other events, 25.3 us)
Sparse Core Ops, SparseCore 0:
  159.5 65.4 all-gather.2
  235.5 51.6 all-gather.4
where the time goes:
time: 326 us; the launch traced here: 324 us
  waiting for transfers between devices  134 us (41%)
  blocking collectives  63.9 us (20%)
  starting transfers between devices  51.9 us (16%)
  local copies, waits for them, and re-layouts  31.6 us (10%)
  between operations  18.8 us (6%)
  matrix products  12.7 us (4%)
  other arithmetic  10.8 us (3%)
    all_to_all x5, waiting for transfers between devices, from_everyone(): lax.all_to_all(jnp.broadcast_to(shard[None], (peers, *shard.shape)), axis...  55.9 us
    all_gather x1, waiting for transfers between devices, side_by_side(): lax.all_gather(both, axis, axis=dim, tiled=True)  51.8 us
    all_to_all x1, blocking collectives, from_everyone(): lax.all_to_all(jnp.broadcast_to(shard[None], (peers, *shard.shape)), axis...  47.9 us
    all_to_all x5, starting transfers between devices, from_everyone(): lax.all_to_all(jnp.broadcast_to(shard[None], (peers, *shard.shape)), axis...  38.8 us
    all_to_all x1, blocking collectives, shards(): lax.all_to_all(outgoing, 'sp', split_axis=0, concat_axis=0, tiled=True)  15.9 us
    all_gather x1, waiting for transfers between devices, shards(): arrived = lax.all_gather(shares, 'tp', axis=2, tiled=True)  15.8 us
    all_to_all x1, waiting for transfers between devices, shards(): lax.all_to_all(expert_out.reshape(experts, capacity, -1), 'sp', split_axi...  11 us
    all_to_all x1, starting transfers between devices, shards(): lax.all_to_all(expert_out.reshape(experts, capacity, -1), 'sp', split_axi...  7.74 us
  transfers between devices with their start and end apart: 10, of which 8 were waited for; matrix products, arithmetic and copies ran while one was open for 6% of the time, Pallas kernels for 0%

commit v1 on v0

v1 whole, which is shorter than its diff:
```python
import jax
import jax.numpy as jnp
from jax import lax
from jax.experimental import pallas as pl
from jax.experimental.pallas import tpu as pltpu
from jax.sharding import PartitionSpec as P

D = 2048
HEADS = 16
HEAD_DIM = 64
GROUPS = 4
STATE = 128
CONV = 5

NZ, NX, NY = 8, 4, 8
SP, TP = NZ * NX, NY * 2
T = 320
HALF = T // 2
SLOTS = 32
ROWS = SP * SLOTS
BLOCK = 80
CHUNKS = 2
MESH = pl.DeviceIdType.MESH
F32, BF16 = jnp.float32, jnp.bfloat16


def dot(a, b):
    return jnp.dot(a, b, preferred_element_type=F32)


class Ring:
    def __init__(self, buf, first, rows, sems, index):
        self.buf, self.first, self.rows = buf, first, rows
        self.send, self.recv, self.rsend, self.rrecv = (s.at[index] for s in sems)
        self.sp, tp = lax.axis_index("sp"), lax.axis_index("tp")
        self.y, self.core = tp // 2, tp % 2

    def part(self, chip, core, half=None):
        column = ((chip + 2 * NY) % NY) * 2 + core
        first, rows = self.first, self.rows
        if half is not None:
            rows = rows // 2
            first = first + half * rows
        return self.buf.at[pl.ds(first, rows), pl.ds(pl.multiple_of(column * 128, 128), 128)]

    def hop(self, way, step):
        turn = 1 - 2 * way
        block = self.part(self.y - turn * (step - 1), self.core, way if step == 4 else None)
        return pltpu.make_async_remote_copy(
            src_ref=block,
            dst_ref=block,
            send_sem=self.send.at[4 * way + step - 1],
            recv_sem=self.recv.at[4 * way + step - 1],
            device_id=(self.sp, ((self.y + turn + NY) % NY) * 2 + self.core),
            device_id_type=MESH,
        )

    def landed(self, way, step):
        turn = 1 - 2 * way
        block = self.part(self.y - turn * step, self.core, way if step == 4 else None)
        return pltpu.make_async_remote_copy(
            src_ref=block,
            dst_ref=block,
            send_sem=self.send.at[4 * way + step - 1],
            recv_sem=self.recv.at[4 * way + step - 1],
            device_id=(self.sp, ((self.y + turn + NY) % NY) * 2 + self.core),
            device_id_type=MESH,
        )

    def relay(self, way, step, theirs=False):
        turn = 1 - 2 * way
        core = 1 - self.core if theirs else self.core
        block = self.part(self.y - turn * step, core, way if step == 4 else None)
        slot = 0 if step == 0 else 4 * way + step
        return pltpu.make_async_remote_copy(
            src_ref=block,
            dst_ref=block,
            send_sem=self.rsend.at[slot],
            recv_sem=self.rrecv.at[slot],
            device_id=(self.sp, self.y * 2 + 1 - self.core),
            device_id_type=MESH,
        )

    def start(self):
        self.hop(0, 1).start()
        self.hop(1, 1).start()
        self.relay(0, 0).start()

    def step(self, step):
        for way in (0, 1):
            self.landed(way, step).wait_recv()
            if step < 4:
                self.hop(way, step + 1).start()
            self.relay(way, step).start()

    def finish(self):
        self.relay(0, 0, True).wait_recv()
        for step in range(1, 5):
            for way in (0, 1):
                self.relay(way, step, True).wait_recv()

    def drain(self):
        self.relay(0, 0).wait_send()
        for step in range(1, 5):
            for way in (0, 1):
                self.hop(way, step).wait_send()
                self.relay(way, step).wait_send()


def run(rings):
    for step in range(1, 5):
        for ring in rings:
            ring.step(step)


def kernel(
    st_ref, base_ref, ef_ref, eb_ref, gate_ref, c_ref, ft_ref, src_ref, ch_ref, cht_ref, sh_ref,
    blender_hbm, valve_hbm, raising_hbm, lowering_hbm, cvalve_hbm, craising_hbm, clowering_hbm,
    out_ref,
    rx, tb, rz, ft, wb, wx, wc, wl, wcl, wide, bn, nn, am, ff, sh, xx, hh, dd, oo, ret, pp, qhi, qlo,
    wsem, xs, xr, zs, zr, fs, fr, rsend, rrecv, psend, precv, ds_, dr, os_, or_,
):
    sp, tp = lax.axis_index("sp"), lax.axis_index("tp")
    z, x = sp // NX, sp % NX

    barrier = pltpu.get_barrier_semaphore()

    def greet_tp(k, carry):
        pl.semaphore_signal(barrier, inc=1, device_id=(sp, (tp + k) % TP), device_id_type=MESH)
        return carry

    def greet_sp(k, carry):
        pl.semaphore_signal(barrier, inc=1, device_id=((sp + k) % SP, tp), device_id_type=MESH)
        return carry

    lax.fori_loop(1, TP, greet_tp, 0)
    lax.fori_loop(1, SP, greet_sp, 0)

    loads = [
        pltpu.make_async_copy(blender_hbm, wb, wsem.at[0]),
        pltpu.make_async_copy(valve_hbm.at[0], wx.at[:, pl.ds(0, 128)], wsem.at[1]),
        pltpu.make_async_copy(raising_hbm.at[0], wx.at[:, pl.ds(128, 128)], wsem.at[2]),
        pltpu.make_async_copy(lowering_hbm.at[0], wl, wsem.at[3]),
        pltpu.make_async_copy(cvalve_hbm, wc.at[:, pl.ds(0, 128)], wsem.at[4]),
        pltpu.make_async_copy(craising_hbm, wc.at[:, pl.ds(128, 128)], wsem.at[5]),
        pltpu.make_async_copy(clowering_hbm, wcl, wsem.at[6]),
    ]
    for load in loads:
        load.start()

    rx[x] = st_ref[...]
    ft[tp] = ft_ref[...]
    pl.semaphore_wait(barrier, TP + SP - 2)

    def state_row(k, source):
        return pltpu.make_async_remote_copy(
            src_ref=st_ref,
            dst_ref=rx.at[source],
            send_sem=xs.at[k],
            recv_sem=xr.at[source],
            device_id=(z * NX + (x + k) % NX, tp),
            device_id_type=MESH,
        )

    for k in (2, 1, 3):
        state_row(k, x).start()

    def tile(k, source):
        return pltpu.make_async_remote_copy(
            src_ref=ft_ref,
            dst_ref=ft.at[source],
            send_sem=fs.at[k],
            recv_sem=fr.at[source],
            device_id=(sp, (tp + k) % TP),
            device_id_type=MESH,
        )

    def send_tile(k, carry):
        tile(k, tp).start()
        return carry

    lax.fori_loop(1, TP, send_tile, 0)

    experts = lax.broadcasted_iota(jnp.int32, (T, SP), 1)
    first, second = ch_ref[:, 0:1] == experts, ch_ref[:, 1:2] == experts
    named = jnp.where(first | second, 1.0, 0.0)
    row = lax.broadcasted_iota(jnp.int32, (T, T), 0)
    col = lax.broadcasted_iota(jnp.int32, (T, T), 1)
    lower = jnp.where(col < row, 1.0, 0.0).astype(BF16)
    upper = jnp.where(row < col, 1.0, 0.0).astype(BF16)
    rank = dot(lower, named.astype(BF16))
    rank = jnp.where(named > 0, rank, 99.0).astype(BF16)
    shares = jnp.where(first, sh_ref[:, 0:1], 0.0) + jnp.where(second, sh_ref[:, 1:2], 0.0)
    share_hi = shares.astype(BF16)
    share_lo = (shares - share_hi.astype(F32)).astype(BF16)
    spread = jnp.where(
        lax.broadcasted_iota(jnp.int32, (SP, ROWS), 1) // SLOTS
        == lax.broadcasted_iota(jnp.int32, (SP, ROWS), 0),
        1.0,
        0.0,
    ).astype(BF16)
    place = (lax.broadcasted_iota(jnp.int32, (T, ROWS), 1) % SLOTS).astype(F32)
    here = dot(rank, spread) == place
    qhi[...] = jnp.where(here, dot(share_hi, spread), 0.0).astype(BF16)
    qlo[...] = jnp.where(here, dot(share_lo, spread), 0.0).astype(BF16)
    experts = lax.broadcasted_iota(jnp.int32, (SP, T), 0)
    named = jnp.where((cht_ref[0:1, :] == experts) | (cht_ref[1:2, :] == experts), 1.0, 0.0)
    rank = dot(named.astype(BF16), upper)
    rank = jnp.where(named > 0, rank, 99.0).astype(BF16)
    spread = jnp.where(
        lax.broadcasted_iota(jnp.int32, (ROWS, SP), 0) // SLOTS
        == lax.broadcasted_iota(jnp.int32, (ROWS, SP), 1),
        1.0,
        0.0,
    ).astype(BF16)
    place = (lax.broadcasted_iota(jnp.int32, (ROWS, T), 0) % SLOTS).astype(F32)
    pp[...] = jnp.where(dot(spread, rank) == place, 1.0, 0.0).astype(BF16)

    for k in (1, 2, 3):
        state_row(k, (x + k) % NX).wait_recv()

    def state(block):
        return block[0:64].astype(F32)

    def log_of(block):
        logs = block[64:80].astype(F32)
        return logs[0:1] + logs[1:2] + logs[2:3]

    pad = jnp.zeros((13, 128), BF16)

    def packed(total, log):
        hi = log.astype(BF16)
        rest = log - hi.astype(F32)
        mid = rest.astype(BF16)
        low = (rest - mid.astype(F32)).astype(BF16)
        tail = lax.broadcasted_iota(jnp.int32, (16, 128), 0)
        rows = jnp.where(
            tail == 0,
            hi.astype(F32),
            jnp.where(tail == 1, mid.astype(F32), jnp.where(tail == 2, low.astype(F32), 0.0)),
        )
        return total.astype(BF16), rows.astype(BF16)

    for way in (0, 1):
        total, log = jnp.zeros((64, 128), F32), jnp.zeros((1, 128), F32)
        for i in range(NX) if way == 0 else reversed(range(NX)):
            block = rx[i, way]
            own = log_of(block)
            total = jnp.exp(own) * total + state(block)
            log = log + own
        top, tail = packed(total, log)
        tb[way, 0:64] = top
        tb[way, 64:80] = tail
    rz[z] = tb[0]

    def state_column(k, source):
        return pltpu.make_async_remote_copy(
            src_ref=tb.at[(z + k) // NZ],
            dst_ref=rz.at[source],
            send_sem=zs.at[k],
            recv_sem=zr.at[source],
            device_id=(((z + k) % NZ) * NX + x, tp),
            device_id_type=MESH,
        )

    for k in (4, 3, 5, 2, 6, 1, 7):
        state_column(k, z).start()

    loads[0].wait()
    wide[...] = jnp.zeros(wide.shape, BF16)

    def widen(j, carry):
        block = wb[pl.ds(pl.multiple_of(j * 64, 64), 64), :]
        wide[pl.ds(pl.multiple_of(j * 128, 128), 64), pl.ds(0, 128)] = block
        wide[pl.ds(pl.multiple_of(j * 128 + 64, 64), 64), pl.ds(128, 128)] = block
        return carry

    lax.fori_loop(0, HEADS, widen, 0)

    for k in range(1, NZ):
        state_column(k, (z + k) % NZ).wait_recv()

    carried = []
    for way in (0, 1):
        total = jnp.zeros((64, 128), F32)
        for i in range(NZ) if way == 0 else reversed(range(NZ)):
            block = rz[i]
            passed = (i < z) if way == 0 else (i > z)
            total = jnp.where(passed, jnp.exp(log_of(block)) * total + state(block), total)
        for i in range(NX) if way == 0 else reversed(range(NX)):
            block = rx[i, way]
            passed = (i < x) if way == 0 else (i > x)
            total = jnp.where(passed, jnp.exp(log_of(block)) * total + state(block), total)
        carried.append(total.astype(BF16))

    def read(state_block):
        none = jnp.zeros((64, 128), BF16)
        dims = (((1,), (1,)), ((), ()))
        left = jnp.concatenate([state_block, none], axis=0)
        right = jnp.concatenate([none, state_block], axis=0)
        return lax.dot_general(
            c_ref[0:HALF], left, dims, preferred_element_type=F32
        ) + lax.dot_general(c_ref[HALF:T], right, dims, preferred_element_type=F32)

    mixer = base_ref[...] + ef_ref[...] * read(carried[0]) + eb_ref[...] * read(carried[1])
    mine = pl.ds(pl.multiple_of(tp * 128, 128), 128)
    bn[:, mine] = (mixer * gate_ref[...]).astype(BF16)

    sems = (rsend, rrecv, psend, precv)
    ring = Ring(bn, 0, HALF, sems, 0)
    ring.start()

    def wait_tile(k, carry):
        tile(k, (tp + k) % TP).wait_recv()
        return carry

    lax.fori_loop(1, TP, wait_tile, 0)
    run([ring])
    ring.finish()
    done = [ring]

    left = lax.broadcasted_iota(jnp.int32, (HALF, 128), 1) < 64
    for g in range(GROUPS):
        squares = jnp.zeros((HALF, 128), F32)
        for j in range(4 * g, 4 * g + 4):
            v = bn[:, 128 * j : 128 * j + 128].astype(F32)
            squares = squares + v * v
        top = jnp.sum(jnp.where(left, squares, 0.0), axis=1, keepdims=True)
        bottom = jnp.sum(jnp.where(left, 0.0, squares), axis=1, keepdims=True)
        scale = lax.rsqrt(jnp.where(left, top, bottom) / (4 * HEAD_DIM) + 1e-06)
        for j in range(4 * g, 4 * g + 4):
            v = bn[:, 128 * j : 128 * j + 128].astype(F32)
            nn[:, 128 * j : 128 * j + 128] = (v * scale * ft[j, 1:2]).astype(BF16)
    projected = dot(nn[...], wide[...])
    am[0:HALF, mine] = (src_ref[0:HALF].astype(F32) + projected[:, 0:128]).astype(BF16)
    am[HALF:T, mine] = (src_ref[HALF:T].astype(F32) + projected[:, 128:256]).astype(BF16)

    rings = [Ring(am, i * HALF, HALF, sems, 1 + i) for i in range(2)]
    for ring in rings:
        ring.start()
    run(rings)
    for ring in rings:
        ring.finish()
    done += rings

    squares = jnp.zeros((T, 128), F32)
    for j in range(TP):
        v = am[:, 128 * j : 128 * j + 128].astype(F32)
        squares = squares + v * v
    scale = lax.rsqrt(jnp.sum(squares, axis=1, keepdims=True) / D + 1e-06)
    own = (am[:, mine].astype(F32) * scale * ft[tp, 0:1]).astype(BF16)
    dd[...] = dot(pp[...], own).astype(BF16)

    def rows_of(i):
        return pl.ds(pl.multiple_of(i * SLOTS, SLOTS), SLOTS)

    def deliver(k, source):
        target = (sp + k) % SP
        return pltpu.make_async_remote_copy(
            src_ref=dd.at[rows_of(target)],
            dst_ref=xx.at[rows_of(source), mine],
            send_sem=ds_.at[k],
            recv_sem=dr.at[source],
            device_id=(target, tp),
            device_id_type=MESH,
        )

    def send_rows(k, carry):
        deliver(k, sp).start()
        return carry

    lax.fori_loop(1, SP, send_rows, 0)
    xx[rows_of(sp), mine] = dd[rows_of(sp)]

    for j in range(TP):
        v = am[:, 128 * j : 128 * j + 128].astype(F32)
        ff[:, 128 * j : 128 * j + 128] = (v * scale * ft[j, 0:1]).astype(BF16)
    loads[4].wait()
    loads[5].wait()
    both = dot(ff[...], wc[...])
    sh[:, mine] = (jax.nn.silu(both[:, 0:128]) * both[:, 128:256]).astype(BF16)
    ring = Ring(sh, 0, T, sems, 3)
    ring.start()
    run([ring])

    size = ROWS // CHUNKS
    per = SP // CHUNKS

    def wait_rows(i, carry):
        @pl.when(i != sp)
        def _():
            deliver(1, i).wait_recv()

        return carry

    gathers = []
    for q in range(CHUNKS):
        lax.fori_loop(q * per, (q + 1) * per, wait_rows, 0)
        gathers.append(Ring(xx, q * size, size, sems, 4 + q))
        gathers[-1].start()
    ring.finish()
    done.append(ring)
    loads[6].wait()
    shared = dot(sh[...], wcl[...]).astype(BF16).astype(F32)
    run(gathers)
    done += gathers

    loads[1].wait()
    loads[2].wait()
    hiddens = []
    for q in range(CHUNKS):
        gathers[q].finish()

        def hidden(i, carry):
            at = pl.ds(pl.multiple_of(i * 128, 128), 128)
            both = dot(xx[at, :], wx[...])
            hh[at, mine] = (jax.nn.silu(both[:, 0:128]) * both[:, 128:256]).astype(BF16)
            return carry

        lax.fori_loop(q * size // 128, (q + 1) * size // 128, hidden, 0)
        hiddens.append(Ring(hh, q * size, size, sems, 4 + CHUNKS + q))
        hiddens[-1].start()
    run(hiddens)
    done += hiddens

    def give(i, source):
        return pltpu.make_async_remote_copy(
            src_ref=oo.at[rows_of(i)],
            dst_ref=ret.at[rows_of(source)],
            send_sem=os_.at[i],
            recv_sem=or_.at[source],
            device_id=(i, tp),
            device_id_type=MESH,
        )

    loads[3].wait()
    for q in range(CHUNKS):
        hiddens[q].finish()

        def lowered(i, carry):
            at = pl.ds(pl.multiple_of(i * 128, 128), 128)
            oo[at, :] = dot(hh[at, :], wl[...]).astype(BF16)
            return carry

        lax.fori_loop(q * size // 128, (q + 1) * size // 128, lowered, 0)

        def send_back(k, carry):
            i = q * per + (sp + k) % per

            @pl.when(i != sp)
            def _():
                give(i, sp).start()

            return carry

        lax.fori_loop(0, per, send_back, 0)
    ret[rows_of(sp), :] = oo[rows_of(sp), :]

    def wait_back(k, carry):
        i = (sp + k) % SP
        give(i, i).wait_recv()
        return carry

    lax.fori_loop(1, SP, wait_back, 0)
    routed = dot(qhi[...], ret[...]) + dot(qlo[...], ret[...])
    out_ref[...] = (am[:, mine].astype(F32) + shared + routed).astype(BF16)

    for k in (1, 2, 3):
        state_row(k, x).wait_send()
    for k in range(1, NZ):
        state_column(k, z).wait_send()

    def drain_tp(k, carry):
        tile(k, tp).wait_send()
        return carry

    lax.fori_loop(1, TP, drain_tp, 0)

    def drain_sp(k, carry):
        deliver(k, sp).wait_send()
        give((sp + k) % SP, sp).wait_send()
        return carry

    lax.fori_loop(1, SP, drain_sp, 0)
    for ring in done:
        ring.drain()


def whole(*operands):
    vmem = pl.BlockSpec(memory_space=pltpu.VMEM)
    hbm = pl.BlockSpec(memory_space=pl.ANY)
    rings = 4 + 2 * CHUNKS
    dma = pltpu.SemaphoreType.DMA
    return pl.pallas_call(
        kernel,
        out_shape=jax.ShapeDtypeStruct((T, 128), BF16),
        in_specs=[vmem] * 11 + [hbm] * 7,
        out_specs=vmem,
        scratch_shapes=[
            pltpu.VMEM((NX, 2, BLOCK, 128), BF16),
            pltpu.VMEM((2, BLOCK, 128), BF16),
            pltpu.VMEM((NZ, BLOCK, 128), BF16),
            pltpu.VMEM((TP, 8, 128), F32),
            pltpu.VMEM((1024, 128), BF16),
            pltpu.VMEM((D, 256), BF16),
            pltpu.VMEM((D, 256), BF16),
            pltpu.VMEM((D, 128), BF16),
            pltpu.VMEM((D, 128), BF16),
            pltpu.VMEM((D, 256), BF16),
            pltpu.VMEM((HALF, D), BF16),
            pltpu.VMEM((HALF, D), BF16),
            pltpu.VMEM((T, D), BF16),
            pltpu.VMEM((T, D), BF16),
            pltpu.VMEM((T, D), BF16),
            pltpu.VMEM((ROWS, D), BF16),
            pltpu.VMEM((ROWS, D), BF16),
            pltpu.VMEM((ROWS, 128), BF16),
            pltpu.VMEM((ROWS, 128), BF16),
            pltpu.VMEM((ROWS, 128), BF16),
            pltpu.VMEM((ROWS, T), BF16),
            pltpu.VMEM((T, ROWS), BF16),
            pltpu.VMEM((T, ROWS), BF16),
            dma((7,)),
            dma((NX,)), dma((NX,)),
            dma((NZ,)), dma((NZ,)),
            dma((TP,)), dma((TP,)),
            dma((rings, 8)), dma((rings, 8)), dma((rings, 9)), dma((rings, 9)),
            dma((SP,)), dma((SP,)), dma((SP,)), dma((SP,)),
        ],
        compiler_params=pltpu.CompilerParams(collective_id=0, has_side_effects=True),
        name="mixer_experts",
    )(*operands)


def extended(cells, width):
    count = lax.axis_size("sp")
    ends = count - 1
    head, tail = cells[:width], cells[-width:]
    return jnp.concatenate(
        [
            lax.ppermute(tail, "sp", [(i, (i + 1) % count) for i in range(ends)]),
            cells,
            lax.ppermute(head, "sp", [((i + 1) % count, i) for i in range(ends)]),
        ],
        axis=0,
    )


def halves(rows):
    return jnp.concatenate([rows[:HALF], rows[HALF:]], axis=1)


def shards(
    layer_source_vector,
    attention_lane_source,
    result_valve_logits,
    memory_write_matrix,
    memory_query_matrix,
    increment_logits,
    increment_offset,
    log_fade_speed,
    extra_log_fade,
    attention_bypass_factor,
    attention_lane_kernel,
    memory_write_kernel,
    memory_query_kernel,
    cluster_rescale_factor,
    blender_result_matrix,
    specialist_rescale_factor,
    chosen_specialists,
    specialist_shares,
    specialist_valve_matrix,
    specialist_raising_matrix,
    specialist_lowering_matrix,
    common_valve_matrix,
    common_raising_matrix,
    common_lowering_matrix,
):
    length = attention_lane_source.shape[0]
    channels = attention_lane_source.shape[1]
    group = lax.axis_index("tp") * GROUPS // HEADS
    b_own = lax.dynamic_slice_in_dim(memory_write_matrix, group * STATE, STATE, 1)
    c_own = lax.dynamic_slice_in_dim(memory_query_matrix, group * STATE, STATE, 1)
    joined = jnp.concatenate([attention_lane_source, b_own, c_own], axis=1)
    taps = jnp.concatenate(
        [
            attention_lane_kernel,
            lax.dynamic_slice_in_dim(memory_write_kernel, group * STATE, STATE, 1),
            lax.dynamic_slice_in_dim(memory_query_kernel, group * STATE, STATE, 1),
        ],
        axis=1,
    )
    padded = extended(joined, CONV // 2)
    total = jnp.zeros(joined.shape, F32)
    for offset in range(CONV):
        total = total + padded[offset : offset + length].astype(F32) * taps[offset].astype(F32)
    convolved = jax.nn.silu(total).astype(BF16)
    x_conv = convolved[:, :channels]
    b_conv = convolved[:, channels : channels + STATE]
    c_conv = convolved[:, channels + STATE :]
    steps = jax.nn.softplus(increment_logits[:, :, 0].astype(F32) + increment_offset)
    fades = -jnp.exp(log_fade_speed) * steps + extra_log_fade[:, :, 0]
    forward_cum = jnp.cumsum(fades[0])
    backward_cum = jnp.cumsum(fades[1]) - fades[1]
    forward_total = forward_cum[-1]
    backward_total = backward_cum[-1] + fades[1, -1]
    scores = lax.dot_general(
        c_conv, b_conv, (((1,), (1,)), ((), ())), preferred_element_type=F32
    )
    position = jnp.arange(length)
    lower = position[:, None] >= position[None, :]
    upper = position[:, None] <= position[None, :]
    forward_gap = forward_cum[:, None] - forward_cum[None, :]
    backward_gap = backward_cum[None, :] - backward_cum[:, None]
    mixing = scores * (
        jnp.where(lower, jnp.exp(jnp.where(lower, forward_gap, 0.0)), 0.0) * steps[0][None, :]
        + jnp.where(upper, jnp.exp(jnp.where(upper, backward_gap, 0.0)), 0.0) * steps[1][None, :]
    )
    inner = jnp.dot(mixing.astype(BF16), x_conv, preferred_element_type=F32)
    forward_scale = jnp.exp(forward_total - forward_cum) * steps[0]
    backward_scale = jnp.exp(backward_cum) * steps[1]
    scaled = (
        jnp.stack([forward_scale, backward_scale])[:, :, None] * x_conv.astype(F32)[None]
    ).astype(BF16)
    own_states = jnp.einsum("dsp,sn->dpn", scaled, b_conv, preferred_element_type=F32)
    logs = jnp.stack([forward_total, backward_total])
    hi = lax.reduce_precision(logs, 8, 7)
    mid = lax.reduce_precision(logs - hi, 8, 7)
    low = logs - hi - mid
    tail = jnp.stack([hi, mid, low] + [jnp.zeros_like(hi)] * 13, axis=1)
    states = jnp.concatenate(
        [own_states, jnp.broadcast_to(tail[:, :, None], (2, 16, STATE))], axis=1
    ).astype(BF16)
    base = halves(inner + attention_bypass_factor[0] * x_conv.astype(F32))
    wide = (length, channels)
    from_left = halves(jnp.broadcast_to(jnp.exp(forward_cum)[:, None], wide))
    from_right = halves(jnp.broadcast_to(jnp.exp(backward_total - backward_cum)[:, None], wide))
    gate = halves(jax.nn.silu(result_valve_logits.astype(F32)))
    gains = jnp.concatenate(
        [
            specialist_rescale_factor[None],
            jnp.concatenate([cluster_rescale_factor, cluster_rescale_factor])[None],
            jnp.zeros((6, 128), F32),
        ]
    )
    return whole(
        states, base, from_left, from_right, gate, c_conv, gains, layer_source_vector,
        chosen_specialists, chosen_specialists.T, specialist_shares,
        blender_result_matrix, specialist_valve_matrix, specialist_raising_matrix,
        specialist_lowering_matrix, common_valve_matrix, common_raising_matrix, common_lowering_matrix,
    )


def solution(mesh):
    return jax.shard_map(
        shards,
        mesh=mesh,
        in_specs=(
            P("sp", "tp"),
            P("sp", "tp"),
            P("sp", "tp"),
            P("sp", None),
            P("sp", None),
            P(None, "sp", "tp"),
            P(None, "tp"),
            P(None, "tp"),
            P(None, "sp", "tp"),
            P("tp"),
            P(None, "tp"),
            P(),
            P(),
            P("tp"),
            P(None, "tp"),
            P("tp"),
            P("sp", None),
            P("sp", None),
            P("sp", None, "tp"),
            P("sp", None, "tp"),
            P("sp", None, "tp"),
            P(None, "tp"),
            P(None, "tp"),
            P(None, "tp"),
        ),
        out_specs=P("sp", "tp"),
        check_vma=False,
    )
```

time: 326 us -> 166 us (0.51)
  Pallas kernels: 0 us -> 136 us
  waiting for transfers between devices: 134 us -> 0.01 us
  blocking collectives: 63.9 us -> 0 us
  starting transfers between devices: 51.9 us -> 5.23 us
  local copies, waits for them, and re-layouts: 31.6 us -> 11.6 us
  between operations: 18.8 us -> 2.3 us
  matrix products: 12.7 us -> 0.71 us
    pallas_call x0 -> x1, Pallas kernels: none -> 136 us  [whole(): pl.pallas_call(kernel, out_shape=jax.ShapeDtypeStruct((T, 128), BF16), in...]
    all_gather x2 -> x0, waiting for transfers between devices: 67.6 us -> none  [the longest x1 51.8 us: side_by_side(): lax.all_gather(both, axis, axis=dim, tiled=True)]
    all_to_all x6 -> x0, waiting for transfers between devices: 66.9 us -> none  [the longest x5 55.9 us: from_everyone(): lax.all_to_all(jnp.broadcast_to(shard[None], (peers, *shard.shape)), axis...]
    all_to_all x2 -> x0, blocking collectives: 63.9 us -> none  [the longest x1 47.9 us: from_everyone(): lax.all_to_all(jnp.broadcast_to(shard[None], (peers, *shard.shape)), axis...]
    all_to_all x6 -> x0, starting transfers between devices: 46.6 us -> none  [the longest x5 38.8 us: from_everyone(): lax.all_to_all(jnp.broadcast_to(shard[None], (peers, *shard.shape)), axis...]
    dot_general x10 -> x2, matrix products: 12.7 us -> 0.71 us  [the longest x1 0.48 us: shards(): inner = jnp.dot(mixing.astype(BF16), x_conv, preferred_element_type=F32)]
    scatter x2 -> x0, local copies, waits for them, and re-layouts: 7 us -> none  [the longest x1 4.1 us: shards(): owner = jnp.zeros((experts * capacity,), jnp.int32).at[slot].set(token)]
    reshape x6 -> x0, local copies, waits for them, and re-layouts: 5.87 us -> none  [the longest x1 5 us: shards(): arrived = arrived.reshape(-1, arrived.shape[2])]
  transfers between devices with their start and end apart: 10 -> 2, of which waited for: 8 -> 0; matrix products, arithmetic and copies ran while one was open for 6% -> 7% of each run, Pallas kernels for 0% -> 0%
where the time goes in v1:
time: 166 us; the launch traced here: 165 us
  Pallas kernels  136 us (82%)
  local copies, waits for them, and re-layouts  11.6 us (7%)
  other arithmetic  8.79 us (5%)
  starting transfers between devices  5.23 us (3%)
  between operations  2.3 us (1%)
    pallas_call x1, Pallas kernels, whole(): pl.pallas_call(kernel, out_shape=jax.ShapeDtypeStruct((T, 128), BF16), in...  136 us
    unnamed x24, local copies, waits for them, and re-layouts  5.99 us
    ppermute x1, starting transfers between devices, extended(): lax.ppermute(tail, 'sp', [(i, (i + 1) % count) for i in range(ends)])  3.93 us
  transfers between devices with their start and end apart: 2, of which 0 were waited for; matrix products, arithmetic and copies ran while one was open for 7% of the time, Pallas kernels for 0%

profile of v1, /device:TPU:1, one launch (start us, length us, event | category | flops | bytes accessed | tf_op | source)
XLA Modules:
  0.0 164.7 jit_solution(15456831794512810175)
XLA Ops:
  0.0 0.9 copy.37
  0.9 0.9 constant_dynamic-slice_fusion.2
  2.1 3.9 %collective-permute-start = (bf16[2,320]{1,0:T(2,128)(2,1)S(1)}, bf16[2,320]{1,0:T(2,128)(2,1)S(1)}, u32[]{:S(2)}, u32[]{:S(2)}) collective-permute-start(bf16[2,320]{1,0:T(2,128)(2,1)S(1)} %get-tuple-element.20), channel_id=1, source_target_pairs={{0,16},{16,32},{32,48},{48,64},{64,80},{80,96},{96,112},{112,128},... | collective-permute-start | bytes 3848 | tf_op jit(solution)/shard_map/ppermute | solution.py:541
  6.0 1.3 collective-permute-start.1
  7.4 0.6 copy-done.6
  8.1 0.7 slice.173
  9.4 0.6 slice.124
  12.6 0.6 reduce-precision_subtract_fusion
  13.2 0.6 fusion.42
  13.9 0.7 constant_dynamic-slice_fusion
  15.7 0.6 copy-done.9
  16.6 0.7 pad_maximum_fusion.4.eb_ref
  17.5 0.7 pad_maximum_fusion.3.ef_ref
  18.2 0.7 pad_maximum_fusion.5.gate_ref
  19.0 0.7 copy-done.7
  19.6 0.7 maximum_maximum_fusion.1.ft_ref
  20.3 0.6 fusion.40
  21.6 0.8 copy.42.ch_ref
  22.4 0.8 copy.43.sh_ref
  24.1 0.7 slice.174.c_ref
  25.5 0.7 pad_maximum_fusion.2.base_ref
  26.5 0.6 pad_maximum_fusion.6.st_ref
  27.1 136.1 %mixer_experts.1 = bf16[320,128]{1,0:T(8,128)(2,1)} custom-call(bf16[2,80,128]{2,1,0:T(8,128)(2,1)} %pad_maximum_fusion.6.st_ref, f32[160,128]{1,0:T(8,128)} %pad_maximum_fusion.2.base_ref, f32[160,128]{1,0:T(8,128)} %pad_maximum_fusion.3.ef_ref, f32[160,128]{1,0:T(8,128)} %pad_maximum_fusion.4.eb_ref, f32[160,128]{1,0:T(8,128)} %pad_maximum_fusion.5.gate_ref, ...), custom_call_target="tpu_custom_call" | custom-call | tf_op jit(solution)/shard_map/mixer_experts/pallas_call | solution.py:494
  163.2 1.5 copy.49
  (69 shorter events, 5.5 us)
Async XLA Ops:
  2.0 5.3 %copy-start.8 = (f32[2,1]{0,1:T(1,128)S(1)}, f32[2,1]{0,1:T(1,128)}, u32[]{:S(2)}) copy-start(f32[2,1]{0,1:T(1,128)} %param.31) | copy-start | bytes 28
  2.1 5.3 %copy-start.2 = (f32[2,320,1]{1,2,0:T(1,128)S(1)}, f32[2,320,1]{1,2,0:T(1,128)}, u32[]{:S(2)}) copy-start(f32[2,320,1]{1,2,0:T(1,128)} %param.32) | copy-start | bytes 7684
  2.1 21.2 %collective-permute-start = (bf16[2,320]{1,0:T(2,128)(2,1)S(1)}, bf16[2,320]{1,0:T(2,128)(2,1)S(1)}, u32[]{:S(2)}, u32[]{:S(2)}) collective-permute-start(bf16[2,320]{1,0:T(2,128)(2,1)S(1)} %get-tuple-element.20), channel_id=1, source_target_pairs={{0,16},{16,32},{32,48},{48,64},{64,80},{80,96},{96,112},{112,128},... | collective-permute-start | bytes 3848 | tf_op jit(solution)/shard_map/ppermute | solution.py:541
  6.0 1.4 copy-start.5
  6.0 17.3 %collective-permute-start.1 = (bf16[2,320]{1,0:T(2,128)(2,1)S(1)}, bf16[2,320]{1,0:T(2,128)(2,1)S(1)}, u32[]{:S(2)}, u32[]{:S(2)}) collective-permute-start(bf16[2,320]{1,0:T(2,128)(2,1)S(1)} %get-tuple-element.21), channel_id=1, source_target_pairs={{16,0},{32,16},{48,32},{64,48},{80,64},{96,80},{112,96},{128,112},... | collective-permute-start | bytes 3848 | tf_op jit(solution)/shard_map/ppermute | solution.py:543
  7.3 0.7 copy-start.6
  10.7 3.9 %copy-start.4 = (bf16[5,64]{1,0:T(8,128)(2,1)S(1)}, bf16[5,64]{1,0:T(8,128)(2,1)}, u32[]{:S(2)}) copy-start(bf16[5,64]{1,0:T(8,128)(2,1)} %param.34) | copy-start | bytes 1924
  10.7 4.8 %copy-start = (bf16[320,64]{0,1:T(8,128)(2,1)S(1)}, bf16[320,64]{0,1:T(8,128)(2,1)}, u32[]{:S(2)}) copy-start(bf16[320,64]{0,1:T(8,128)(2,1)} %param.26) | copy-start | bytes 122884
  15.6 0.7 copy-start.9
  19.0 0.7 copy-start.7
  20.3 1.3 copy-start.1
  21.6 0.8 copy-start.3

commit v2 on v1

--- a/solution.py
+++ b/solution.py
@@ -29,8 +29,8 @@
 
 
 class Ring:
-    def __init__(self, buf, first, rows, sems, index):
-        self.buf, self.first, self.rows = buf, first, rows
+    def __init__(self, buf, first, rows, sems, index, direct=False):
+        self.buf, self.first, self.rows, self.direct = buf, first, rows, direct
         self.send, self.recv, self.rsend, self.rrecv = (s.at[index] for s in sems)
         self.sp, tp = lax.axis_index("sp"), lax.axis_index("tp")
         self.y, self.core = tp // 2, tp % 2
@@ -43,29 +43,25 @@
             first = first + half * rows
         return self.buf.at[pl.ds(first, rows), pl.ds(pl.multiple_of(column * 128, 128), 128)]
 
-    def hop(self, way, step):
+    def along(self, way, step, chip, far):
         turn = 1 - 2 * way
-        block = self.part(self.y - turn * (step - 1), self.core, way if step == 4 else None)
+        block = self.part(chip, self.core, way if step == 4 else None)
         return pltpu.make_async_remote_copy(
             src_ref=block,
             dst_ref=block,
             send_sem=self.send.at[4 * way + step - 1],
             recv_sem=self.recv.at[4 * way + step - 1],
-            device_id=(self.sp, ((self.y + turn + NY) % NY) * 2 + self.core),
+            device_id=(self.sp, ((self.y + turn * far + NY) % NY) * 2 + self.core),
             device_id_type=MESH,
         )
 
+    def hop(self, way, step):
+        if self.direct:
+            return self.along(way, step, self.y, step)
+        return self.along(way, step, self.y - (1 - 2 * way) * (step - 1), 1)
+
     def landed(self, way, step):
-        turn = 1 - 2 * way
-        block = self.part(self.y - turn * step, self.core, way if step == 4 else None)
-        return pltpu.make_async_remote_copy(
-            src_ref=block,
-            dst_ref=block,
-            send_sem=self.send.at[4 * way + step - 1],
-            recv_sem=self.recv.at[4 * way + step - 1],
-            device_id=(self.sp, ((self.y + turn + NY) % NY) * 2 + self.core),
-            device_id_type=MESH,
-        )
+        return self.along(way, step, self.y - (1 - 2 * way) * step, 1)
 
     def relay(self, way, step, theirs=False):
         turn = 1 - 2 * way
@@ -82,14 +78,15 @@
         )
 
     def start(self):
-        self.hop(0, 1).start()
-        self.hop(1, 1).start()
+        for step in (4, 3, 2, 1) if self.direct else (1,):
+            self.hop(0, step).start()
+            self.hop(1, step).start()
         self.relay(0, 0).start()
 
     def step(self, step):
         for way in (0, 1):
             self.landed(way, step).wait_recv()
-            if step < 4:
+            if step < 4 and not self.direct:
                 self.hop(way, step + 1).start()
             self.relay(way, step).start()
 
@@ -117,8 +114,8 @@
     st_ref, base_ref, ef_ref, eb_ref, gate_ref, c_ref, ft_ref, src_ref, ch_ref, cht_ref, sh_ref,
     blender_hbm, valve_hbm, raising_hbm, lowering_hbm, cvalve_hbm, craising_hbm, clowering_hbm,
     out_ref,
-    rx, tb, rz, ft, wb, wx, wc, wl, wcl, wide, bn, nn, am, ff, sh, xx, hh, dd, oo, ret, pp, qhi, qlo,
-    wsem, xs, xr, zs, zr, fs, fr, rsend, rrecv, psend, precv, ds_, dr, os_, or_,
+    rx, tb, rz, ft, sq, so, wb, wx, wc, wl, wcl, wide, bn, nn, am, ff, sh, xx, hh, dd, oo, ret, pp, qhi, qlo,
+    wsem, xs, xr, zs, zr, fs, fr, qs, qr, rsend, rrecv, psend, precv, ds_, dr, os_, or_,
 ):
     sp, tp = lax.axis_index("sp"), lax.axis_index("tp")
     z, x = sp // NX, sp % NX
@@ -150,8 +147,6 @@
 
     rx[x] = st_ref[...]
     ft[tp] = ft_ref[...]
-    pl.semaphore_wait(barrier, TP + SP - 2)
-
     def state_row(k, source):
         return pltpu.make_async_remote_copy(
             src_ref=st_ref,
@@ -162,9 +157,6 @@
             device_id_type=MESH,
         )
 
-    for k in (2, 1, 3):
-        state_row(k, x).start()
-
     def tile(k, source):
         return pltpu.make_async_remote_copy(
             src_ref=ft_ref,
@@ -178,8 +170,6 @@
     def send_tile(k, carry):
         tile(k, tp).start()
         return carry
-
-    lax.fori_loop(1, TP, send_tile, 0)
 
     experts = lax.broadcasted_iota(jnp.int32, (T, SP), 1)
     first, second = ch_ref[:, 0:1] == experts, ch_ref[:, 1:2] == experts
@@ -216,6 +206,11 @@
     place = (lax.broadcasted_iota(jnp.int32, (ROWS, T), 0) % SLOTS).astype(F32)
     pp[...] = jnp.where(dot(spread, rank) == place, 1.0, 0.0).astype(BF16)
 
+    pl.semaphore_wait(barrier, TP + SP - 2)
+    for k in (2, 1, 3):
+        state_row(k, x).start()
+    lax.fori_loop(1, TP, send_tile, 0)
+
     for k in (1, 2, 3):
         state_row(k, (x + k) % NX).wait_recv()
 
@@ -307,7 +302,7 @@
     bn[:, mine] = (mixer * gate_ref[...]).astype(BF16)
 
     sems = (rsend, rrecv, psend, precv)
-    ring = Ring(bn, 0, HALF, sems, 0)
+    ring = Ring(bn, 0, HALF, sems, 0, direct=True)
     ring.start()
 
     def wait_tile(k, carry):
@@ -317,7 +312,6 @@
     lax.fori_loop(1, TP, wait_tile, 0)
     run([ring])
     ring.finish()
-    done = [ring]
 
     left = lax.broadcasted_iota(jnp.int32, (HALF, 128), 1) < 64
     for g in range(GROUPS):
@@ -332,23 +326,69 @@
             v = bn[:, 128 * j : 128 * j + 128].astype(F32)
             nn[:, 128 * j : 128 * j + 128] = (v * scale * ft[j, 1:2]).astype(BF16)
     projected = dot(nn[...], wide[...])
-    am[0:HALF, mine] = (src_ref[0:HALF].astype(F32) + projected[:, 0:128]).astype(BF16)
-    am[HALF:T, mine] = (src_ref[HALF:T].astype(F32) + projected[:, 128:256]).astype(BF16)
-
-    rings = [Ring(am, i * HALF, HALF, sems, 1 + i) for i in range(2)]
-    for ring in rings:
-        ring.start()
-    run(rings)
-    for ring in rings:
-        ring.finish()
-    done += rings
-
-    squares = jnp.zeros((T, 128), F32)
-    for j in range(TP):
-        v = am[:, 128 * j : 128 * j + 128].astype(F32)
-        squares = squares + v * v
-    scale = lax.rsqrt(jnp.sum(squares, axis=1, keepdims=True) / D + 1e-06)
-    own = (am[:, mine].astype(F32) * scale * ft[tp, 0:1]).astype(BF16)
+    am[0:HALF] = (src_ref[0:HALF].astype(F32) + projected[:, 0:128]).astype(BF16)
+    am[HALF:T] = (src_ref[HALF:T].astype(F32) + projected[:, 128:256]).astype(BF16)
+
+    dims = (((1,), (1,)), ((), ()))
+    squares = am[...].astype(F32) * am[...].astype(F32)
+    high = squares.astype(BF16)
+    rest = (squares - high.astype(F32)).astype(BF16)
+    ones = jnp.ones((8, 128), BF16)
+    sums = lax.dot_general(ones, high, dims, preferred_element_type=F32) + lax.dot_general(
+        ones, rest, dims, preferred_element_type=F32
+    )
+    line = jnp.concatenate([sums, jnp.zeros((8, 3 * 128 - T), F32)], axis=1)
+    level = lax.broadcasted_iota(jnp.int32, (8, 128), 0)
+    own = jnp.where(
+        level == 0,
+        line[:, 0:128],
+        jnp.where(level == 1, line[:, 128:256], jnp.where(level == 2, line[:, 256:384], 0.0)),
+    )
+    sq[tp] = own
+    so[...] = own
+
+    def sums_to(k, source):
+        return pltpu.make_async_remote_copy(
+            src_ref=so,
+            dst_ref=sq.at[source],
+            send_sem=qs.at[k],
+            recv_sem=qr.at[source],
+            device_id=(sp, (tp + k) % TP),
+            device_id_type=MESH,
+        )
+
+    def send_sums(k, carry):
+        sums_to((k + 7) % (TP - 1) + 1, tp).start()
+        return carry
+
+    lax.fori_loop(0, TP - 1, send_sums, 0)
+    ring.drain()
+
+    def wait_sums(k, carry):
+        sums_to(k, (tp + k) % TP).wait_recv()
+        return carry
+
+    lax.fori_loop(1, TP, wait_sums, 0)
+    total = sq[0]
+    for j in range(1, TP):
+        total = total + sq[j]
+    line = jnp.concatenate([total[0:1], total[1:2], total[2:3]], axis=1)
+    high = line.astype(BF16).astype(F32)
+    middle = (line - high).astype(BF16).astype(F32)
+    low = line - high - middle
+    level = lax.broadcasted_iota(jnp.int32, (8, 384), 0)
+    parts = jnp.where(
+        level == 0, high, jnp.where(level == 1, middle, jnp.where(level == 2, low, 0.0))
+    ).astype(BF16)
+    same = jnp.where(
+        lax.broadcasted_iota(jnp.int32, (T, 384), 0) == lax.broadcasted_iota(jnp.int32, (T, 384), 1),
+        1.0,
+        0.0,
+    ).astype(BF16)
+    upright = lax.dot_general(same, parts, dims, preferred_element_type=F32)
+    scale = lax.rsqrt((upright[:, 0:1] + upright[:, 1:2] + upright[:, 2:3]) / D + 1e-06)
+    own = (am[...].astype(F32) * scale * ft_ref[0:1]).astype(BF16)
+    ff[:, mine] = own
     dd[...] = dot(pp[...], own).astype(BF16)
 
     def rows_of(i):
@@ -372,16 +412,9 @@
     lax.fori_loop(1, SP, send_rows, 0)
     xx[rows_of(sp), mine] = dd[rows_of(sp)]
 
-    for j in range(TP):
-        v = am[:, 128 * j : 128 * j + 128].astype(F32)
-        ff[:, 128 * j : 128 * j + 128] = (v * scale * ft[j, 0:1]).astype(BF16)
-    loads[4].wait()
-    loads[5].wait()
-    both = dot(ff[...], wc[...])
-    sh[:, mine] = (jax.nn.silu(both[:, 0:128]) * both[:, 128:256]).astype(BF16)
-    ring = Ring(sh, 0, T, sems, 3)
-    ring.start()
-    run([ring])
+    spread_out = [Ring(ff, i * HALF, HALF, sems, 1 + i) for i in range(2)]
+    for ring in spread_out:
+        ring.start()
 
     size = ROWS // CHUNKS
     per = SP // CHUNKS
@@ -393,35 +426,72 @@
 
         return carry
 
+    for step in (1, 2):
+        for ring in spread_out:
+            ring.step(step)
     gathers = []
     for q in range(CHUNKS):
         lax.fori_loop(q * per, (q + 1) * per, wait_rows, 0)
         gathers.append(Ring(xx, q * size, size, sems, 4 + q))
         gathers[-1].start()
-    ring.finish()
-    done.append(ring)
-    loads[6].wait()
-    shared = dot(sh[...], wcl[...]).astype(BF16).astype(F32)
-    run(gathers)
-    done += gathers
+    for step in (3, 4):
+        for ring in spread_out:
+            ring.step(step)
+    for ring in gathers:
+        ring.step(1)
+    for ring in spread_out:
+        ring.finish()
+    loads[4].wait()
+    loads[5].wait()
+    both = dot(ff[...], wc[...])
+    sh[:, mine] = (jax.nn.silu(both[:, 0:128]) * both[:, 128:256]).astype(BF16)
+    hidden_out = Ring(sh, 0, T, sems, 3)
+    hidden_out.start()
+    for step in (2, 3, 4):
+        for ring in gathers:
+            ring.step(step)
+        hidden_out.step(step - 1)
 
     loads[1].wait()
     loads[2].wait()
     hiddens = []
     for q in range(CHUNKS):
         gathers[q].finish()
-
-        def hidden(i, carry):
-            at = pl.ds(pl.multiple_of(i * 128, 128), 128)
-            both = dot(xx[at, :], wx[...])
-            hh[at, mine] = (jax.nn.silu(both[:, 0:128]) * both[:, 128:256]).astype(BF16)
-            return carry
-
-        lax.fori_loop(q * size // 128, (q + 1) * size // 128, hidden, 0)
+        at = pl.ds(q * size, size)
+        both = dot(xx[at, :], wx[...])
+        hh[at, mine] = (jax.nn.silu(both[:, 0:128]) * both[:, 128:256]).astype(BF16)
         hiddens.append(Ring(hh, q * size, size, sems, 4 + CHUNKS + q))
         hiddens[-1].start()
-    run(hiddens)
-    done += hiddens
+    hidden_out.step(4)
+    for k in (1, 2, 3):
+        state_row(k, x).wait_send()
+    for k in range(1, NZ):
+        state_column(k, z).wait_send()
+
+    def drain_tp(k, carry):
+        tile(k, tp).wait_send()
+        sums_to(k, tp).wait_send()
+        return carry
+
+    lax.fori_loop(1, TP, drain_tp, 0)
+
+    def drain_sp(k, carry):
+        deliver(k, sp).wait_send()
+        return carry
+
+    lax.fori_loop(1, SP, drain_sp, 0)
+    for ring in spread_out + gathers:
+        ring.drain()
+    for ring in hiddens:
+        ring.step(1)
+    hidden_out.finish()
+    loads[6].wait()
+    shared = dot(sh[...], wcl[...]).astype(BF16).astype(F32)
+    out_ref[...] = shared.astype(BF16)
+    hidden_out.drain()
+    for step in (2, 3, 4):
+        for ring in hiddens:
+            ring.step(step)
 
     def give(i, source):
         return pltpu.make_async_remote_copy(
@@ -437,12 +507,8 @@
     for q in range(CHUNKS):
         hiddens[q].finish()
 
-        def lowered(i, carry):
-            at = pl.ds(pl.multiple_of(i * 128, 128), 128)
-            oo[at, :] = dot(hh[at, :], wl[...]).astype(BF16)
-            return carry
-
-        lax.fori_loop(q * size // 128, (q + 1) * size // 128, lowered, 0)
+        at = pl.ds(q * size, size)
+        oo[at, :] = dot(hh[at, :], wl[...]).astype(BF16)
 
         def send_back(k, carry):
             i = q * per + (sp + k) % per
@@ -456,34 +522,18 @@
         lax.fori_loop(0, per, send_back, 0)
     ret[rows_of(sp), :] = oo[rows_of(sp), :]
 
+    for ring in hiddens:
+        ring.drain()
+
     def wait_back(k, carry):
         i = (sp + k) % SP
         give(i, i).wait_recv()
+        give(i, sp).wait_send()
         return carry
 
     lax.fori_loop(1, SP, wait_back, 0)
     routed = dot(qhi[...], ret[...]) + dot(qlo[...], ret[...])
-    out_ref[...] = (am[:, mine].astype(F32) + shared + routed).astype(BF16)
-
-    for k in (1, 2, 3):
-        state_row(k, x).wait_send()
-    for k in range(1, NZ):
-        state_column(k, z).wait_send()
-
-    def drain_tp(k, carry):
-        tile(k, tp).wait_send()
-        return carry
-
-    lax.fori_loop(1, TP, drain_tp, 0)
-
-    def drain_sp(k, carry):
-        deliver(k, sp).wait_send()
-        give((sp + k) % SP, sp).wait_send()
-        return carry
-
-    lax.fori_loop(1, SP, drain_sp, 0)
-    for ring in done:
-        ring.drain()
+    out_ref[...] = (am[...].astype(F32) + out_ref[...].astype(F32) + routed).astype(BF16)
 
 
 def whole(*operands):
@@ -501,6 +551,8 @@
             pltpu.VMEM((2, BLOCK, 128), BF16),
             pltpu.VMEM((NZ, BLOCK, 128), BF16),
             pltpu.VMEM((TP, 8, 128), F32),
+            pltpu.VMEM((TP, 8, 128), F32),
+            pltpu.VMEM((8, 128), F32),
             pltpu.VMEM((1024, 128), BF16),
             pltpu.VMEM((D, 256), BF16),
             pltpu.VMEM((D, 256), BF16),
@@ -509,7 +561,7 @@
             pltpu.VMEM((D, 256), BF16),
             pltpu.VMEM((HALF, D), BF16),
             pltpu.VMEM((HALF, D), BF16),
-            pltpu.VMEM((T, D), BF16),
+            pltpu.VMEM((T, 128), BF16),
             pltpu.VMEM((T, D), BF16),
             pltpu.VMEM((T, D), BF16),
             pltpu.VMEM((ROWS, D), BF16),
@@ -523,6 +575,7 @@
             dma((7,)),
             dma((NX,)), dma((NX,)),
             dma((NZ,)), dma((NZ,)),
+            dma((TP,)), dma((TP,)),
             dma((TP,)), dma((TP,)),
             dma((rings, 8)), dma((rings, 8)), dma((rings, 9)), dma((rings, 9)),
             dma((SP,)), dma((SP,)), dma((SP,)), dma((SP,)),

time: 166 us -> 150 us (0.904)
  Pallas kernels: 136 us -> 121 us
    pallas_call x1, Pallas kernels: 136 us -> 121 us  [whole(): pl.pallas_call(kernel, out_shape=jax.ShapeDtypeStruct((T, 128), BF16), in...]
  transfers between devices with their start and end apart: 2 -> 2, of which waited for: 0 -> 0; matrix products, arithmetic and copies ran while one was open for 7% -> 8% of each run, Pallas kernels for 0% -> 0%
where the time goes in v2:
time: 150 us
  Pallas kernels  121 us (81%)
  local copies, waits for them, and re-layouts  11.6 us (8%)
  other arithmetic  8.79 us (6%)
  starting transfers between devices  5.23 us (3%)
  between operations  2.3 us (2%)
    pallas_call x1, Pallas kernels, whole(): pl.pallas_call(kernel, out_shape=jax.ShapeDtypeStruct((T, 128), BF16), in...  121 us
    unnamed x24, local copies, waits for them, and re-layouts  5.99 us
    ppermute x1, starting transfers between devices, extended(): lax.ppermute(tail, 'sp', [(i, (i + 1) % count) for i in range(ends)])  3.93 us
  transfers between devices with their start and end apart: 2, of which 0 were waited for; matrix products, arithmetic and copies ran while one was open for 8% of the time, Pallas kernels for 0%

profile of v2, /device:TPU:1, one launch (start us, length us, event | category | flops | bytes accessed | tf_op | source)
XLA Modules:
  0.0 149.6 jit_solution(9823010654700380225)
XLA Ops:
  0.0 0.9 copy.37
  0.9 0.9 constant_dynamic-slice_fusion.2
  2.1 3.9 %collective-permute-start = (bf16[2,320]{1,0:T(2,128)(2,1)S(1)}, bf16[2,320]{1,0:T(2,128)(2,1)S(1)}, u32[]{:S(2)}, u32[]{:S(2)}) collective-permute-start(bf16[2,320]{1,0:T(2,128)(2,1)S(1)} %get-tuple-element.20), channel_id=1, source_target_pairs={{0,16},{16,32},{32,48},{48,64},{64,80},{80,96},{96,112},{112,128},... | collective-permute-start | bytes 3848 | tf_op jit(solution)/shard_map/ppermute | solution.py:594
  6.0 1.3 collective-permute-start.1
  7.4 0.6 copy-done.6
  8.1 0.7 slice.173
  9.4 0.6 slice.124
  12.6 0.6 reduce-precision_subtract_fusion
  13.2 0.6 fusion.42
  13.9 0.7 constant_dynamic-slice_fusion
  15.7 0.6 copy-done.9
  16.6 0.7 pad_maximum_fusion.4.eb_ref
  17.5 0.7 pad_maximum_fusion.3.ef_ref
  18.2 0.7 pad_maximum_fusion.5.gate_ref
  19.0 0.7 copy-done.7
  19.6 0.7 maximum_maximum_fusion.1.ft_ref
  20.3 0.6 fusion.40
  21.6 0.8 copy.42.ch_ref
  22.4 0.8 copy.43.sh_ref
  24.1 0.7 slice.174.c_ref
  25.5 0.7 pad_maximum_fusion.2.base_ref
  26.5 0.6 pad_maximum_fusion.6.st_ref
  27.1 121.0 %mixer_experts.1 = bf16[320,128]{1,0:T(8,128)(2,1)} custom-call(bf16[2,80,128]{2,1,0:T(8,128)(2,1)} %pad_maximum_fusion.6.st_ref, f32[160,128]{1,0:T(8,128)} %pad_maximum_fusion.2.base_ref, f32[160,128]{1,0:T(8,128)} %pad_maximum_fusion.3.ef_ref, f32[160,128]{1,0:T(8,128)} %pad_maximum_fusion.4.eb_ref, f32[160,128]{1,0:T(8,128)} %pad_maximum_fusion.5.gate_ref, ...), custom_call_target="tpu_custom_call" | custom-call | tf_op jit(solution)/shard_map/mixer_experts/pallas_call | solution.py:544
  148.1 1.5 %copy.49 = bf16[320,128]{1,0:T(8,128)(2,1)} copy(bf16[320,128]{1,0:T(8,128)(2,1)} %mixer_experts.1) | data formatting | bytes 163840
  (69 shorter events, 5.5 us)
Async XLA Ops:
  2.0 5.3 %copy-start.8 = (f32[2,1]{0,1:T(1,128)S(1)}, f32[2,1]{0,1:T(1,128)}, u32[]{:S(2)}) copy-start(f32[2,1]{0,1:T(1,128)} %param.31) | copy-start | bytes 28
  2.1 5.3 %copy-start.2 = (f32[2,320,1]{1,2,0:T(1,128)S(1)}, f32[2,320,1]{1,2,0:T(1,128)}, u32[]{:S(2)}) copy-start(f32[2,320,1]{1,2,0:T(1,128)} %param.32) | copy-start | bytes 7684
  2.1 21.2 %collective-permute-start = (bf16[2,320]{1,0:T(2,128)(2,1)S(1)}, bf16[2,320]{1,0:T(2,128)(2,1)S(1)}, u32[]{:S(2)}, u32[]{:S(2)}) collective-permute-start(bf16[2,320]{1,0:T(2,128)(2,1)S(1)} %get-tuple-element.20), channel_id=1, source_target_pairs={{0,16},{16,32},{32,48},{48,64},{64,80},{80,96},{96,112},{112,128},... | collective-permute-start | bytes 3848 | tf_op jit(solution)/shard_map/ppermute | solution.py:594
  6.0 1.4 copy-start.5
  6.0 17.3 %collective-permute-start.1 = (bf16[2,320]{1,0:T(2,128)(2,1)S(1)}, bf16[2,320]{1,0:T(2,128)(2,1)S(1)}, u32[]{:S(2)}, u32[]{:S(2)}) collective-permute-start(bf16[2,320]{1,0:T(2,128)(2,1)S(1)} %get-tuple-element.21), channel_id=1, source_target_pairs={{16,0},{32,16},{48,32},{64,48},{80,64},{96,80},{112,96},{128,112},... | collective-permute-start | bytes 3848 | tf_op jit(solution)/shard_map/ppermute | solution.py:596
  7.3 0.7 copy-start.6
  10.7 3.9 %copy-start.4 = (bf16[5,64]{1,0:T(8,128)(2,1)S(1)}, bf16[5,64]{1,0:T(8,128)(2,1)}, u32[]{:S(2)}) copy-start(bf16[5,64]{1,0:T(8,128)(2,1)} %param.34) | copy-start | bytes 1924
  10.7 4.8 %copy-start = (bf16[320,64]{0,1:T(8,128)(2,1)S(1)}, bf16[320,64]{0,1:T(8,128)(2,1)}, u32[]{:S(2)}) copy-start(bf16[320,64]{0,1:T(8,128)(2,1)} %param.26) | copy-start | bytes 122884
  15.6 0.7 copy-start.9
  19.0 0.7 copy-start.7
  20.3 1.3 copy-start.1
  21.6 0.8 copy-start.3

commit v3 on v2

v3 whole, which is shorter than its diff:
```python
import jax
import jax.numpy as jnp
from jax import lax
from jax.experimental import pallas as pl
from jax.experimental.pallas import tpu as pltpu
from jax.sharding import PartitionSpec as P

D = 2048
HEADS = 16
HEAD_DIM = 64
GROUPS = 4
STATE = 128
CONV = 5

NZ, NX, NY = 8, 4, 8
SP, TP = NZ * NX, NY * 2
T = 320
HALF = T // 2
SLOTS = 32
ROWS = SP * SLOTS
BLOCK = 80
CHUNKS = 2
MESH = pl.DeviceIdType.MESH
F32, BF16 = jnp.float32, jnp.bfloat16


def dot(a, b):
    return jnp.dot(a, b, preferred_element_type=F32)


class Ring:
    def __init__(self, buf, first, rows, sems, index, direct=False):
        self.buf, self.first, self.rows, self.direct = buf, first, rows, direct
        self.out, self.near = sems[0].at[index, 0], sems[0].at[index, 1]
        self.recv = sems[1].at[index]
        self.sp, tp = lax.axis_index("sp"), lax.axis_index("tp")
        self.y, self.core = tp // 2, tp % 2

    def part(self, chip, core, half=None):
        column = ((chip + 2 * NY) % NY) * 2 + core
        first, rows = self.first, self.rows
        if half is not None:
            rows = rows // 2
            first = first + half * rows
        return self.buf.at[pl.ds(first, rows), pl.ds(pl.multiple_of(column * 128, 128), 128)]

    def along(self, way, step, chip, far):
        turn = 1 - 2 * way
        block = self.part(chip, self.core, way if step == 4 else None)
        return pltpu.make_async_remote_copy(
            src_ref=block,
            dst_ref=block,
            send_sem=self.out,
            recv_sem=self.recv.at[4 * way + step - 1],
            device_id=(self.sp, ((self.y + turn * far + NY) % NY) * 2 + self.core),
            device_id_type=MESH,
        )

    def hop(self, way, step):
        if self.direct:
            return self.along(way, step, self.y, step)
        return self.along(way, step, self.y - (1 - 2 * way) * (step - 1), 1)

    def landed(self, way, step):
        return self.along(way, step, self.y - (1 - 2 * way) * step, 1)

    def relay(self, way, step):
        turn = 1 - 2 * way
        return self.over(self.part(self.y - turn * step, self.core, way if step == 4 else None))

    def over(self, block):
        return pltpu.make_async_remote_copy(
            src_ref=block,
            dst_ref=block,
            send_sem=self.out,
            recv_sem=self.near,
            device_id=(self.sp, self.y * 2 + 1 - self.core),
            device_id_type=MESH,
        )

    def several(self, blocks):
        return self.over(self.buf.at[pl.ds(self.first, self.rows), pl.ds(0, 128 * blocks)])

    def start(self):
        for step in (4, 3, 2, 1) if self.direct else (1,):
            self.hop(0, step).start()
            self.hop(1, step).start()
        self.relay(0, 0).start()

    def step(self, step):
        for way in (0, 1):
            self.landed(way, step).wait_recv()
            if step < 4 and not self.direct:
                self.hop(way, step + 1).start()
            self.relay(way, step).start()

    def finish(self):
        self.several(NY).wait_recv()

    def drain(self):
        self.several(2 * NY - 1).wait_send()


def run(rings):
    for step in range(1, 5):
        for ring in rings:
            ring.step(step)


def stacked(rows):
    level = lax.broadcasted_iota(jnp.int32, (8, rows[0].shape[1]), 0)
    total = jnp.zeros(level.shape, F32)
    for k, row in enumerate(rows):
        total = jnp.where(level == k, row, total)
    return total


def three(v):
    high = v.astype(BF16).astype(F32)
    middle = (v - high).astype(BF16).astype(F32)
    return [high, middle, v - high - middle]


def one_hot(shape, test):
    row, col = lax.broadcasted_iota(jnp.int32, shape, 0), lax.broadcasted_iota(jnp.int32, shape, 1)
    return jnp.where(test(row, col), 1.0, 0.0).astype(BF16)


def across(a, b):
    return lax.dot_general(a, b, (((1,), (1,)), ((), ())), preferred_element_type=F32)


def log1p(u):
    series = u * (1 - u * (1 / 2 - u * (1 / 3 - u * (1 / 4 - u * (1 / 5 - u / 6)))))
    return jnp.where(u < 0.03, series, jnp.log(1 + u))


def silu(v):
    return v / (1 + jnp.exp(-v))


def kernel(
    xt_ref, zt_ref, inc_ref, off_ref, spd_ref, fade_ref, byp_ref, xk_ref, bk_ref, ck_ref, gain_ref,
    after_ref, src_ref, cht_ref, sht_ref,
    bm_hbm, cm_hbm, blender_hbm, valve_hbm, raising_hbm, lowering_hbm, cvalve_hbm, craising_hbm, clowering_hbm,
    out_ref,
    xpad, braw, craw, hx, hb, hc, bext, cext, gap, cv, mixed, fto,
    st_ref, rx, tb, rz, ft, sq, so, wb, wx, wc, wl, wcl, wide, bn, nn, am, ff, sh, xx, hh, dd, oo, ret, pp, qhi, qlo,
    wsem, hs, hr, one, dr, rsem, rrecv,
):
    sp, tp = lax.axis_index("sp"), lax.axis_index("tp")
    z, x = sp // NX, sp % NX

    barrier = pltpu.get_barrier_semaphore()

    def greet_tp(k, carry):
        pl.semaphore_signal(barrier, inc=1, device_id=(sp, (tp + k) % TP), device_id_type=MESH)
        return carry

    def greet_sp(k, carry):
        pl.semaphore_signal(barrier, inc=1, device_id=((sp + k) % SP, tp), device_id_type=MESH)
        return carry

    lax.fori_loop(1, TP, greet_tp, 0)
    lax.fori_loop(1, SP, greet_sp, 0)

    at_group = pl.ds(pl.multiple_of((tp // 4) * 128, 128), 128)
    loads = [
        pltpu.make_async_copy(blender_hbm, wb, wsem.at[0]),
        pltpu.make_async_copy(valve_hbm.at[0], wx.at[:, pl.ds(0, 128)], wsem.at[1]),
        pltpu.make_async_copy(raising_hbm.at[0], wx.at[:, pl.ds(128, 128)], wsem.at[2]),
        pltpu.make_async_copy(lowering_hbm.at[0], wl, wsem.at[3]),
        pltpu.make_async_copy(cvalve_hbm, wc.at[:, pl.ds(0, 128)], wsem.at[4]),
        pltpu.make_async_copy(craising_hbm, wc.at[:, pl.ds(128, 128)], wsem.at[5]),
        pltpu.make_async_copy(clowering_hbm, wcl, wsem.at[6]),
    ]
    grouped = [
        pltpu.make_async_copy(bm_hbm.at[:, at_group], braw, wsem.at[7]),
        pltpu.make_async_copy(cm_hbm.at[:, at_group], craw, wsem.at[8]),
    ]
    for load in grouped + loads:
        load.start()

    xpad[...] = jnp.zeros(xpad.shape, BF16)
    xpad[:, 0:T] = xt_ref[...]
    gains = jnp.concatenate([gain_ref[...], gain_ref[...]], axis=1)
    fto[...] = jnp.broadcast_to(gains, (8, 128))
    ft[tp] = fto[...]

    def state_row(k, source):
        return pltpu.make_async_remote_copy(
            src_ref=st_ref,
            dst_ref=rx.at[source],
            send_sem=one.at[0],
            recv_sem=one.at[1],
            device_id=(z * NX + (x + k) % NX, tp),
            device_id_type=MESH,
        )

    def tile(k, source):
        return pltpu.make_async_remote_copy(
            src_ref=fto,
            dst_ref=ft.at[source],
            send_sem=one.at[4],
            recv_sem=one.at[5],
            device_id=(sp, (tp + k) % TP),
            device_id_type=MESH,
        )

    def send_tile(k, carry):
        tile(k, tp).start()
        return carry

    lower = one_hot((T, T), lambda row, col: col < row)
    upper = one_hot((T, T), lambda row, col: row < col)
    same = one_hot((T, T), lambda row, col: row == col)
    experts = lax.broadcasted_iota(jnp.int32, (SP, T), 0)
    first, second = cht_ref[0:1, :] == experts, cht_ref[1:2, :] == experts
    named = jnp.where(first | second, 1.0, 0.0)
    rank = dot(named.astype(BF16), upper)
    rank = jnp.where(named > 0, rank, 99.0).astype(BF16)
    spread = one_hot((ROWS, SP), lambda row, col: row // SLOTS == col)
    place = (lax.broadcasted_iota(jnp.int32, (ROWS, T), 0) % SLOTS).astype(F32)
    pp[...] = jnp.where(dot(spread, rank) == place, 1.0, 0.0).astype(BF16)
    shares = jnp.where(first, sht_ref[0:1, :], 0.0) + jnp.where(second, sht_ref[1:2, :], 0.0)
    share_hi = shares.astype(BF16)
    share_lo = (shares - share_hi.astype(F32)).astype(BF16)
    spread = one_hot((SP, ROWS), lambda row, col: col // SLOTS == row)
    place = (lax.broadcasted_iota(jnp.int32, (T, ROWS), 1) % SLOTS).astype(F32)
    here = dot(across(same, rank).astype(BF16), spread) == place
    qhi[...] = jnp.where(here, dot(across(same, share_hi).astype(BF16), spread), 0.0).astype(BF16)
    qlo[...] = jnp.where(here, dot(across(same, share_lo).astype(BF16), spread), 0.0).astype(BF16)

    steps, fades = [], []
    for d in range(2):
        v = inc_ref[d : d + 1, :].astype(F32) + off_ref[0:1, d : d + 1]
        step = jnp.maximum(v, 0.0) + log1p(jnp.exp(-jnp.abs(v)))
        steps.append(step)
        fades.append(-jnp.exp(spd_ref[0:1, d : d + 1]) * step + fade_ref[d])
    parts = stacked(three(fades[0]) + three(fades[1])).astype(BF16)
    along = dot(parts, upper + same)
    forward_row = along[0:1] + along[1:2] + along[2:3]
    along = dot(parts, upper)
    backward_row = along[3:4] + along[4:5] + along[5:6]
    along = across(lower + same, parts)
    forward_col = along[:, 0:1] + along[:, 1:2] + along[:, 2:3]
    along = across(lower, parts)
    backward_col = along[:, 3:4] + along[:, 4:5] + along[:, 5:6]
    row = lax.broadcasted_iota(jnp.int32, (T, T), 0)
    col = lax.broadcasted_iota(jnp.int32, (T, T), 1)
    gap[...] = (
        jnp.where(row >= col, jnp.exp(forward_col - forward_row), 0.0) * steps[0]
        + jnp.where(row <= col, jnp.exp(backward_row - backward_col), 0.0) * steps[1]
    )
    forward_end = forward_row[:, T - 1 : T]
    backward_end = backward_row[:, T - 1 : T] + fades[1][:, T - 1 : T]
    weigh = [jnp.exp(forward_end - forward_row) * steps[0], jnp.exp(backward_row) * steps[1]]
    seen = [jnp.exp(forward_row), jnp.exp(backward_end - backward_row)]
    cv[...] = stacked(weigh + seen)
    ends = [jnp.broadcast_to(forward_end, (1, 128)), jnp.broadcast_to(backward_end, (1, 128))]

    for load in grouped:
        load.wait()
    pl.semaphore_wait(barrier, TP + SP - 2)

    def halo(side, k):
        there = (sp + 1) % SP if side == 0 else (sp + SP - 1) % SP
        rows = pl.ds(T - 16, 16) if side == 0 else pl.ds(0, 16)
        lanes = pl.ds(256, 128) if side == 0 else pl.ds(0, 128)
        source = (xpad.at[:, lanes], braw.at[rows], craw.at[rows])[k]
        return pltpu.make_async_remote_copy(
            src_ref=source,
            dst_ref=(hx, hb, hc)[k].at[side],
            send_sem=hs.at[3 * side + k],
            recv_sem=hr.at[3 * side + k],
            device_id=(there, tp),
            device_id_type=MESH,
        )

    for k in range(3):
        halo(0, k).start()
        halo(1, k).start()
    lax.fori_loop(1, TP, send_tile, 0)

    taps = across(same[0:64, 0:64], stacked([xk_ref[j : j + 1, :].astype(F32) for j in range(CONV)]).astype(BF16))
    lane = lax.broadcasted_iota(jnp.int32, (64, 128), 1)
    body = xpad[...].astype(F32)
    bext[pl.ds(16, T), :] = braw[...].astype(F32)
    cext[pl.ds(16, T), :] = craw[...].astype(F32)
    for k in range(3):
        halo(0, k).wait_recv()
        halo(1, k).wait_recv()
    before, behind = sp > 0, sp < SP - 1
    last = jnp.where(before, pltpu.roll(hx[0].astype(F32), 64, 1), 0.0)
    coming = jnp.where(behind, pltpu.roll(hx[1].astype(F32), 64, 1), 0.0)
    end = jnp.where(
        lane < 64, body[:, 256:384], jnp.where(lane < 66, coming, jnp.where(lane > 125, last, 0.0))
    )
    cells = jnp.concatenate([body[:, 0:256], end], axis=1)
    total = cells * taps[:, 2:3]
    for j in (0, 1, 3, 4):
        total = total + pltpu.roll(cells, (2 - j) % 384, 1) * taps[:, j : j + 1]
    x_conv = silu(total)[:, 0:T].astype(BF16)
    for ext, halos, kernel_ref in ((bext, hb, bk_ref), (cext, hc, ck_ref)):
        ext[pl.ds(0, 16), :] = jnp.where(before, halos[0].astype(F32), 0.0)
        ext[pl.ds(T + 16, 16), :] = jnp.where(behind, halos[1].astype(F32), 0.0)
        total = jnp.zeros((T, 128), F32)
        for j in range(CONV):
            tap = kernel_ref[j : j + 1, at_group].astype(F32)
            total = total + ext[pl.ds(14 + j, T), :] * tap
        mixed[0 if ext is bext else 1] = silu(total).astype(BF16)
    b_conv, c_conv = mixed[0], mixed[1]

    def packed(total, log):
        tail = jnp.concatenate([stacked(three(log)), jnp.zeros((8, 128), F32)], axis=0)
        return total.astype(BF16), tail.astype(BF16)

    x_wide = x_conv.astype(F32)
    for d in range(2):
        scaled = (cv[d : d + 1, :] * x_wide).astype(BF16)
        top, tail = packed(dot(scaled, b_conv), ends[d])
        st_ref[d, 0:64] = top
        st_ref[d, 64:80] = tail
    rx[x] = st_ref[...]
    for k in (2, 1, 3):
        state_row(k, x).start()
    inner = across(x_conv, (across(c_conv, b_conv) * gap[...]).astype(BF16))
    inner = inner + byp_ref[...] * x_wide
    gate = silu(zt_ref[...].astype(F32))

    def all_rows(k):
        return pltpu.make_async_remote_copy(
            src_ref=rx.at[pl.ds(0, k)],
            dst_ref=rx.at[pl.ds(0, k)],
            send_sem=one.at[0],
            recv_sem=one.at[1],
            device_id=(z * NX + (x + 1) % NX, tp),
            device_id_type=MESH,
        )

    all_rows(NX - 1).wait_recv()

    def state(block):
        return block[0:64].astype(F32)

    def log_of(block):
        logs = block[64:80].astype(F32)
        return logs[0:1] + logs[1:2] + logs[2:3]

    for way in (0, 1):
        total, log = jnp.zeros((64, 128), F32), jnp.zeros((1, 128), F32)
        for i in range(NX) if way == 0 else reversed(range(NX)):
            block = rx[i, way]
            own = log_of(block)
            total = jnp.exp(own) * total + state(block)
            log = log + own
        top, tail = packed(total, log)
        tb[way, 0:64] = top
        tb[way, 64:80] = tail
    rz[z] = tb[0]

    def state_column(k, source):
        return pltpu.make_async_remote_copy(
            src_ref=tb.at[(z + k) // NZ],
            dst_ref=rz.at[source],
            send_sem=one.at[2],
            recv_sem=one.at[3],
            device_id=(((z + k) % NZ) * NX + x, tp),
            device_id_type=MESH,
        )

    for k in (4, 3, 5, 2, 6, 1, 7):
        state_column(k, z).start()

    loads[0].wait()
    wide[...] = jnp.zeros(wide.shape, BF16)

    def widen(j, carry):
        block = wb[pl.ds(pl.multiple_of(j * 64, 64), 64), :]
        wide[pl.ds(pl.multiple_of(j * 128, 128), 64), pl.ds(0, 128)] = block
        wide[pl.ds(pl.multiple_of(j * 128 + 64, 64), 64), pl.ds(128, 128)] = block
        return carry

    lax.fori_loop(0, HEADS, widen, 0)

    def all_columns():
        return pltpu.make_async_remote_copy(
            src_ref=rz.at[pl.ds(0, NZ - 1)],
            dst_ref=rz.at[pl.ds(0, NZ - 1)],
            send_sem=one.at[2],
            recv_sem=one.at[3],
            device_id=(((z + 1) % NZ) * NX + x, tp),
            device_id_type=MESH,
        )

    all_columns().wait_recv()

    carried = []
    for way in (0, 1):
        total = jnp.zeros((64, 128), F32)
        for i in range(NZ) if way == 0 else reversed(range(NZ)):
            block = rz[i]
            passed = (i < z) if way == 0 else (i > z)
            total = jnp.where(passed, jnp.exp(log_of(block)) * total + state(block), total)
        for i in range(NX) if way == 0 else reversed(range(NX)):
            block = rx[i, way]
            passed = (i < x) if way == 0 else (i > x)
            total = jnp.where(passed, jnp.exp(log_of(block)) * total + state(block), total)
        carried.append(total.astype(BF16))

    mixer = inner + cv[2:3, :] * across(carried[0], mixed[1]) + cv[3:4, :] * across(carried[1], mixed[1])
    gated = (mixer * gate).astype(BF16)
    none = jnp.zeros((64, T), BF16)
    upper_half = one_hot((HALF, T), lambda row, col: row == col)
    lower_half = one_hot((HALF, T), lambda row, col: row + HALF == col)
    mine = pl.ds(pl.multiple_of(tp * 128, 128), 128)
    bn[:, mine] = (
        across(upper_half, jnp.concatenate([gated, none], axis=0))
        + across(lower_half, jnp.concatenate([none, gated], axis=0))
    ).astype(BF16)

    sems = (rsem, rrecv)
    ring = Ring(bn, 0, HALF, sems, 0, direct=True)
    ring.start()

    def all_tiles(ref, at):
        return pltpu.make_async_remote_copy(
            src_ref=ref.at[pl.ds(0, TP - 1)],
            dst_ref=ref.at[pl.ds(0, TP - 1)],
            send_sem=one.at[at],
            recv_sem=one.at[at + 1],
            device_id=(sp, (tp + 1) % TP),
            device_id_type=MESH,
        )

    all_tiles(ft, 4).wait_recv()
    run([ring])
    ring.finish()

    left = lax.broadcasted_iota(jnp.int32, (HALF, 128), 1) < 64
    for g in range(GROUPS):
        squares = jnp.zeros((HALF, 128), F32)
        for j in range(4 * g, 4 * g + 4):
            v = bn[:, 128 * j : 128 * j + 128].astype(F32)
            squares = squares + v * v
        top = jnp.sum(jnp.where(left, squares, 0.0), axis=1, keepdims=True)
        bottom = jnp.sum(jnp.where(left, 0.0, squares), axis=1, keepdims=True)
        scale = lax.rsqrt(jnp.where(left, top, bottom) / (4 * HEAD_DIM) + 1e-06)
        for j in range(4 * g, 4 * g + 4):
            v = bn[:, 128 * j : 128 * j + 128].astype(F32)
            nn[:, 128 * j : 128 * j + 128] = (v * scale * ft[j, 0:1]).astype(BF16)
    projected = dot(nn[...], wide[...])
    am[0:HALF] = (src_ref[0:HALF].astype(F32) + projected[:, 0:128]).astype(BF16)
    am[HALF:T] = (src_ref[HALF:T].astype(F32) + projected[:, 128:256]).astype(BF16)

    dims = (((1,), (1,)), ((), ()))
    squares = am[...].astype(F32) * am[...].astype(F32)
    high = squares.astype(BF16)
    rest = (squares - high.astype(F32)).astype(BF16)
    ones = jnp.ones((8, 128), BF16)
    sums = lax.dot_general(ones, high, dims, preferred_element_type=F32) + lax.dot_general(
        ones, rest, dims, preferred_element_type=F32
    )
    line = jnp.concatenate([sums, jnp.zeros((8, 3 * 128 - T), F32)], axis=1)
    level = lax.broadcasted_iota(jnp.int32, (8, 128), 0)
    own = jnp.where(
        level == 0,
        line[:, 0:128],
        jnp.where(level == 1, line[:, 128:256], jnp.where(level == 2, line[:, 256:384], 0.0)),
    )
    sq[tp] = own
    so[...] = own

    def sums_to(k, source):
        return pltpu.make_async_remote_copy(
            src_ref=so,
            dst_ref=sq.at[source],
            send_sem=one.at[6],
            recv_sem=one.at[7],
            device_id=(sp, (tp + k) % TP),
            device_id_type=MESH,
        )

    def send_sums(k, carry):
        sums_to((k + 7) % (TP - 1) + 1, tp).start()
        return carry

    lax.fori_loop(0, TP - 1, send_sums, 0)
    ring.drain()

    all_tiles(sq, 6).wait_recv()
    total = sq[0]
    for j in range(1, TP):
        total = total + sq[j]
    line = jnp.concatenate([total[0:1], total[1:2], total[2:3]], axis=1)
    parts = stacked(three(line)).astype(BF16)
    same = one_hot((T, 384), lambda row, col: row == col)
    upright = lax.dot_general(same, parts, dims, preferred_element_type=F32)
    scale = lax.rsqrt((upright[:, 0:1] + upright[:, 1:2] + upright[:, 2:3]) / D + 1e-06)
    own = (am[...].astype(F32) * scale * after_ref[...]).astype(BF16)
    ff[:, mine] = own
    dd[...] = dot(pp[...], own).astype(BF16)

    def rows_of(i):
        return pl.ds(pl.multiple_of(i * SLOTS, SLOTS), SLOTS)

    def deliver(k, source):
        target = (sp + k) % SP
        return pltpu.make_async_remote_copy(
            src_ref=dd.at[rows_of(target)],
            dst_ref=xx.at[rows_of(source), mine],
            send_sem=one.at[8],
            recv_sem=dr.at[source // (SP // CHUNKS)],
            device_id=(target, tp),
            device_id_type=MESH,
        )

    def send_rows(k, carry):
        deliver(k, sp).start()
        return carry

    lax.fori_loop(1, SP, send_rows, 0)
    xx[rows_of(sp), mine] = dd[rows_of(sp)]

    spread_out = [Ring(ff, i * HALF, HALF, sems, 1 + i) for i in range(2)]
    for ring in spread_out:
        ring.start()

    size = ROWS // CHUNKS
    per = SP // CHUNKS

    def some_rows(ref, first, blocks, sent, received):
        part = ref.at[pl.ds(first, blocks * SLOTS), pl.ds(0, 128)]
        return pltpu.make_async_remote_copy(
            src_ref=part,
            dst_ref=part,
            send_sem=one.at[sent],
            recv_sem=received,
            device_id=((sp + 1) % SP, tp),
            device_id_type=MESH,
        )

    def wait_rows(q):
        @pl.when(sp // per == q)
        def _():
            some_rows(xx, q * size, per - 1, 8, dr.at[q]).wait_recv()

        @pl.when(sp // per != q)
        def _():
            some_rows(xx, q * size, per, 8, dr.at[q]).wait_recv()

    for step in (1, 2):
        for ring in spread_out:
            ring.step(step)
    gathers = []
    for q in range(CHUNKS):
        wait_rows(q)
        gathers.append(Ring(xx, q * size, size, sems, 4 + q))
        gathers[-1].start()
    for step in (3, 4):
        for ring in spread_out:
            ring.step(step)
    for ring in gathers:
        ring.step(1)
    for ring in spread_out:
        ring.finish()
    loads[4].wait()
    loads[5].wait()
    both = dot(ff[...], wc[...])
    sh[:, mine] = (jax.nn.silu(both[:, 0:128]) * both[:, 128:256]).astype(BF16)
    hidden_out = Ring(sh, 0, T, sems, 3)
    hidden_out.start()
    for step in (2, 3, 4):
        for ring in gathers:
            ring.step(step)
        hidden_out.step(step - 1)

    loads[1].wait()
    loads[2].wait()
    hiddens = []
    for q in range(CHUNKS):
        gathers[q].finish()
        at = pl.ds(q * size, size)
        both = dot(xx[at, :], wx[...])
        hh[at, mine] = (jax.nn.silu(both[:, 0:128]) * both[:, 128:256]).astype(BF16)
        hiddens.append(Ring(hh, q * size, size, sems, 4 + CHUNKS + q))
        hiddens[-1].start()
    hidden_out.step(4)
    for side in range(2):
        for k in range(3):
            halo(side, k).wait_send()
    all_rows(NX - 1).wait_send()
    all_columns().wait_send()
    all_tiles(ft, 4).wait_send()
    all_tiles(sq, 6).wait_send()
    some_rows(dd, 0, SP - 1, 8, one.at[9]).wait_send()
    for ring in spread_out + gathers:
        ring.drain()
    for ring in hiddens:
        ring.step(1)
    hidden_out.finish()
    loads[6].wait()
    shared = dot(sh[...], wcl[...]).astype(BF16).astype(F32)
    out_ref[...] = shared.astype(BF16)
    hidden_out.drain()
    for step in (2, 3, 4):
        for ring in hiddens:
            ring.step(step)

    def give(i, source):
        return pltpu.make_async_remote_copy(
            src_ref=oo.at[rows_of(i)],
            dst_ref=ret.at[rows_of(source)],
            send_sem=one.at[10],
            recv_sem=one.at[11],
            device_id=(i, tp),
            device_id_type=MESH,
        )

    loads[3].wait()
    for q in range(CHUNKS):
        hiddens[q].finish()

        at = pl.ds(q * size, size)
        oo[at, :] = dot(hh[at, :], wl[...]).astype(BF16)

        def send_back(k, carry):
            i = q * per + (sp + k) % per

            @pl.when(i != sp)
            def _():
                give(i, sp).start()

            return carry

        lax.fori_loop(0, per, send_back, 0)
    ret[rows_of(sp), :] = oo[rows_of(sp), :]

    for ring in hiddens:
        ring.drain()

    some_rows(ret, 0, SP - 1, 10, one.at[11]).wait_recv()
    some_rows(oo, 0, SP - 1, 10, one.at[11]).wait_send()
    routed = dot(qhi[...], ret[...]) + dot(qlo[...], ret[...])
    out_ref[...] = (am[...].astype(F32) + out_ref[...].astype(F32) + routed).astype(BF16)


def whole(*operands):
    vmem = pl.BlockSpec(memory_space=pltpu.VMEM)
    hbm = pl.BlockSpec(memory_space=pl.ANY)
    rings = 4 + 2 * CHUNKS
    dma = pltpu.SemaphoreType.DMA

    def space(*shape, kind=BF16):
        return pltpu.VMEM(shape, kind)

    return pl.pallas_call(
        kernel,
        out_shape=jax.ShapeDtypeStruct((T, 128), BF16),
        in_specs=[vmem] * 15 + [hbm] * 9,
        out_specs=vmem,
        scratch_shapes=[
            space(64, 384),
            space(T, 128),
            space(T, 128),
            space(2, 64, 128),
            space(2, 16, 128),
            space(2, 16, 128),
            space(T + 32, 128, kind=F32),
            space(T + 32, 128, kind=F32),
            space(T, T, kind=F32),
            space(8, T, kind=F32),
            space(2, T, 128),
            space(8, 128, kind=F32),
            space(2, BLOCK, 128),
            space(NX, 2, BLOCK, 128),
            space(2, BLOCK, 128),
            space(NZ, BLOCK, 128),
            space(TP, 8, 128, kind=F32),
            space(TP, 8, 128, kind=F32),
            space(8, 128, kind=F32),
            space(1024, 128),
            space(D, 256),
            space(D, 256),
            space(D, 128),
            space(D, 128),
            space(D, 256),
            space(HALF, D),
            space(HALF, D),
            space(T, 128),
            space(T, D),
            space(T, D),
            space(ROWS, D),
            space(ROWS, D),
            space(ROWS, 128),
            space(ROWS, 128),
            space(ROWS, 128),
            space(ROWS, T),
            space(T, ROWS),
            space(T, ROWS),
            dma((9,)), dma((6,)), dma((6,)), dma((12,)), dma((CHUNKS,)), dma((rings, 2)), dma((rings, 8)),
        ],
        compiler_params=pltpu.CompilerParams(collective_id=0, has_side_effects=True),
        name="mixer_experts",
    )(*operands)


def shards(
    layer_source_vector,
    attention_lane_source,
    result_valve_logits,
    memory_write_matrix,
    memory_query_matrix,
    increment_logits,
    increment_offset,
    log_fade_speed,
    extra_log_fade,
    attention_bypass_factor,
    attention_lane_kernel,
    memory_write_kernel,
    memory_query_kernel,
    cluster_rescale_factor,
    blender_result_matrix,
    specialist_rescale_factor,
    chosen_specialists,
    specialist_shares,
    specialist_valve_matrix,
    specialist_raising_matrix,
    specialist_lowering_matrix,
    common_valve_matrix,
    common_raising_matrix,
    common_lowering_matrix,
):
    return whole(
        attention_lane_source.T,
        result_valve_logits.T,
        increment_logits.reshape(2, T),
        increment_offset.T,
        log_fade_speed.T,
        extra_log_fade.reshape(2, 1, T),
        attention_bypass_factor.reshape(1, 1),
        attention_lane_kernel,
        memory_write_kernel,
        memory_query_kernel,
        cluster_rescale_factor.reshape(1, 64),
        specialist_rescale_factor.reshape(1, 128),
        layer_source_vector,
        chosen_specialists.T,
        specialist_shares.T,
        memory_write_matrix,
        memory_query_matrix,
        blender_result_matrix,
        specialist_valve_matrix,
        specialist_raising_matrix,
        specialist_lowering_matrix,
        common_valve_matrix,
        common_raising_matrix,
        common_lowering_matrix,
    )


def solution(mesh):
    return jax.shard_map(
        shards,
        mesh=mesh,
        in_specs=(
            P("sp", "tp"),
            P("sp", "tp"),
            P("sp", "tp"),
            P("sp", None),
            P("sp", None),
            P(None, "sp", "tp"),
            P(None, "tp"),
            P(None, "tp"),
            P(None, "sp", "tp"),
            P("tp"),
            P(None, "tp"),
            P(),
            P(),
            P("tp"),
            P(None, "tp"),
            P("tp"),
            P("sp", None),
            P("sp", None),
            P("sp", None, "tp"),
            P("sp", None, "tp"),
            P("sp", None, "tp"),
            P(None, "tp"),
            P(None, "tp"),
            P(None, "tp"),
        ),
        out_specs=P("sp", "tp"),
        check_vma=False,
    )
```

time: 150 us -> 121 us (0.81)
  local copies, waits for them, and re-layouts: 11.6 us -> 1.53 us
  other arithmetic: 8.79 us -> 0 us
  starting transfers between devices: 5.23 us -> 0 us
  Pallas kernels: 121 us -> 118 us
  between operations: 2.3 us -> 0.66 us
    ppermute x2 -> x0, starting transfers between devices: 5.23 us -> none  [the longest x1 3.93 us: extended(): lax.ppermute(tail, 'sp', [(i, (i + 1) % count) for i in range(ends)])]
    concatenate x9 -> x0, other arithmetic: 4.7 us -> none  [the longest x4 2.9 us: halves(): return jnp.concatenate([rows[:HALF], rows[HALF:]], axis=1)]
    unnamed x24 -> x1, local copies, waits for them, and re-layouts: 5.99 us -> 1.53 us
    slice x12 -> x0, local copies, waits for them, and re-layouts: 2.87 us -> none  [the longest x2 1.25 us: shards(): backward_total = backward_cum[-1] + fades[1, -1]]
    pallas_call x1, Pallas kernels: 121 us -> 118 us  [whole(): pl.pallas_call(kernel, out_shape=jax.ShapeDtypeStruct((T, 128), BF16), in...]
    dynamic_slice x2 -> x0, local copies, waits for them, and re-layouts: 1.65 us -> none  [the longest x1 0.95 us: shards(): lax.dynamic_slice_in_dim(memory_query_matrix, group * STATE, STATE, 1)]
  transfers between devices with their start and end apart: 2 -> 0, of which waited for: 0 -> 0; matrix products, arithmetic and copies ran while one was open for 8% -> 0% of each run, Pallas kernels for 0% -> 0%
where the time goes in v3:
time: 121 us
  Pallas kernels  118 us (98%)
  local copies, waits for them, and re-layouts  1.53 us (1%)
    pallas_call x1, Pallas kernels, whole(): pl.pallas_call(kernel, out_shape=jax.ShapeDtypeStruct((T, 128), BF16), in...  118 us

profile of v3, /device:TPU:1, one launch (start us, length us, event | category | flops | bytes accessed | tf_op | source)
XLA Modules:
  0.0 120.6 jit_solution(14810321241997056631)
XLA Ops:
  0.7 118.4 %mixer_experts.1 = bf16[320,128]{1,0:T(8,128)(2,1)} custom-call(bf16[64,320]{1,0:T(8,128)(2,1)} %bitcast.12, bf16[64,320]{1,0:T(8,128)(2,1)} %bitcast.13, bf16[2,320]{1,0:T(2,128)(2,1)} %bitcast.17, f32[1,2]{1,0:T(1,128)} %bitcast.18, f32[1,2]{1,0:T(1,128)} %bitcast.19, f32[2,1,320]{2,1,0:T(1,128)} %bitcast.14, f32[1,1]{1,0:T(1,128)} %bitcast.11.byp_ref, ...), custom_call_target="tpu_custom_call" | custom-call | tf_op jit(solution)/shard_map/mixer_experts/pallas_call | solution.py:657
  119.1 1.5 %copy.27 = bf16[320,128]{1,0:T(8,128)(2,1)} copy(bf16[320,128]{1,0:T(8,128)(2,1)} %mixer_experts.1) | data formatting | bytes 163840

commit v4 on v3

--- a/solution.py
+++ b/solution.py
@@ -29,20 +29,24 @@
 
 
 class Ring:
-    def __init__(self, buf, first, rows, sems, index, direct=False):
-        self.buf, self.first, self.rows, self.direct = buf, first, rows, direct
+    def __init__(self, buf, first, rows, sems, index, direct=False, pair=False):
+        self.buf, self.first, self.rows, self.direct, self.pair = buf, first, rows, direct, pair
         self.out, self.near = sems[0].at[index, 0], sems[0].at[index, 1]
         self.recv = sems[1].at[index]
         self.sp, tp = lax.axis_index("sp"), lax.axis_index("tp")
         self.y, self.core = tp // 2, tp % 2
 
     def part(self, chip, core, half=None):
-        column = ((chip + 2 * NY) % NY) * 2 + core
+        column, width = ((chip + 2 * NY) % NY) * 2, 128
+        if self.pair:
+            width = 256
+        else:
+            column = column + core
         first, rows = self.first, self.rows
         if half is not None:
             rows = rows // 2
             first = first + half * rows
-        return self.buf.at[pl.ds(first, rows), pl.ds(pl.multiple_of(column * 128, 128), 128)]
+        return self.buf.at[pl.ds(first, rows), pl.ds(pl.multiple_of(column * 128, 128), width)]
 
     def along(self, way, step, chip, far):
         turn = 1 - 2 * way
@@ -85,20 +89,22 @@
         for step in (4, 3, 2, 1) if self.direct else (1,):
             self.hop(0, step).start()
             self.hop(1, step).start()
-        self.relay(0, 0).start()
+        if not self.pair:
+            self.relay(0, 0).start()
 
     def step(self, step):
         for way in (0, 1):
             self.landed(way, step).wait_recv()
             if step < 4 and not self.direct:
                 self.hop(way, step + 1).start()
-            self.relay(way, step).start()
+            if not self.pair:
+                self.relay(way, step).start()
 
     def finish(self):
         self.several(NY).wait_recv()
 
     def drain(self):
-        self.several(2 * NY - 1).wait_send()
+        self.several(2 * NY - (2 if self.pair else 1)).wait_send()
 
 
 def run(rings):
@@ -145,11 +151,12 @@
     bm_hbm, cm_hbm, blender_hbm, valve_hbm, raising_hbm, lowering_hbm, cvalve_hbm, craising_hbm, clowering_hbm,
     out_ref,
     xpad, braw, craw, hx, hb, hc, bext, cext, gap, cv, mixed, fto,
-    st_ref, rx, tb, rz, ft, sq, so, wb, wx, wc, wl, wcl, wide, bn, nn, am, ff, sh, xx, hh, dd, oo, ret, pp, qhi, qlo,
+    st_ref, rx, tb, rz, ft, sq, so, wb, wx, wc, wl, wcl, wide, bn, nn, am, ff, sh, xx, hh, dd, ss, sl, oo, ret, pp, qhi, qlo,
     wsem, hs, hr, one, dr, rsem, rrecv,
 ):
     sp, tp = lax.axis_index("sp"), lax.axis_index("tp")
     z, x = sp // NX, sp % NX
+    y, core, side_of = tp // 2, tp % 2, sp // (SP // 2)
 
     barrier = pltpu.get_barrier_semaphore()
 
@@ -164,12 +171,15 @@
     lax.fori_loop(1, TP, greet_tp, 0)
     lax.fori_loop(1, SP, greet_sp, 0)
 
+    def lanes_of(i):
+        return pl.ds(pl.multiple_of(i * 128, 128), 128)
+
     at_group = pl.ds(pl.multiple_of((tp // 4) * 128, 128), 128)
     loads = [
         pltpu.make_async_copy(blender_hbm, wb, wsem.at[0]),
-        pltpu.make_async_copy(valve_hbm.at[0], wx.at[:, pl.ds(0, 128)], wsem.at[1]),
-        pltpu.make_async_copy(raising_hbm.at[0], wx.at[:, pl.ds(128, 128)], wsem.at[2]),
-        pltpu.make_async_copy(lowering_hbm.at[0], wl, wsem.at[3]),
+        pltpu.make_async_copy(valve_hbm.at[0], wx.at[:, lanes_of(core)], wsem.at[1]),
+        pltpu.make_async_copy(raising_hbm.at[0], wx.at[:, lanes_of(core + 2)], wsem.at[2]),
+        pltpu.make_async_copy(lowering_hbm.at[0], wl.at[:, lanes_of(core)], wsem.at[3]),
         pltpu.make_async_copy(cvalve_hbm, wc.at[:, pl.ds(0, 128)], wsem.at[4]),
         pltpu.make_async_copy(craising_hbm, wc.at[:, pl.ds(128, 128)], wsem.at[5]),
         pltpu.make_async_copy(clowering_hbm, wcl, wsem.at[6]),
@@ -282,6 +292,21 @@
         halo(1, k).start()
     lax.fori_loop(1, TP, send_tile, 0)
 
+    def to_other(part):
+        return pltpu.make_async_remote_copy(
+            src_ref=part,
+            dst_ref=part,
+            send_sem=one.at[12],
+            recv_sem=one.at[13],
+            device_id=(sp, y * 2 + 1 - core),
+            device_id_type=MESH,
+        )
+
+    for k in (1, 2, 3):
+        loads[k].wait()
+    for part in (wx.at[:, lanes_of(core)], wx.at[:, lanes_of(core + 2)], wl.at[:, lanes_of(core)]):
+        to_other(part).start()
+
     taps = across(same[0:64, 0:64], stacked([xk_ref[j : j + 1, :].astype(F32) for j in range(CONV)]).astype(BF16))
     lane = lax.broadcasted_iota(jnp.int32, (64, 128), 1)
     body = xpad[...].astype(F32)
@@ -453,6 +478,46 @@
     am[0:HALF] = (src_ref[0:HALF].astype(F32) + projected[:, 0:128]).astype(BF16)
     am[HALF:T] = (src_ref[HALF:T].astype(F32) + projected[:, 128:256]).astype(BF16)
 
+    own = (am[...].astype(F32) * after_ref[...]).astype(BF16)
+    ff[:, mine] = own
+    dd[...] = dot(pp[...], own).astype(BF16)
+
+    def rows_of(i):
+        return pl.ds(pl.multiple_of(i * SLOTS, SLOTS), SLOTS)
+
+    per = SP // 2 // CHUNKS
+    size = per * SLOTS
+    local = sp % (SP // 2)
+
+    def deliver(k):
+        target = (sp + k) % SP
+        return pltpu.make_async_remote_copy(
+            src_ref=dd.at[rows_of(target)],
+            dst_ref=xx.at[rows_of(local), mine],
+            send_sem=one.at[8],
+            recv_sem=dr.at[local // per],
+            device_id=(target, y * 2 + side_of),
+            device_id_type=MESH,
+        )
+
+    def send_rows(k, carry):
+        deliver(k).start()
+        return carry
+
+    lax.fori_loop(1, SP, send_rows, 0)
+
+    @pl.when(side_of == core)
+    def _():
+        xx[rows_of(local), mine] = dd[rows_of(sp)]
+
+    @pl.when(side_of != core)
+    def _():
+        deliver(0).start()
+
+    spread_out = [Ring(ff, i * HALF, HALF, sems, 1 + i) for i in range(2)]
+    for spreading in spread_out:
+        spreading.start()
+
     dims = (((1,), (1,)), ((), ()))
     squares = am[...].astype(F32) * am[...].astype(F32)
     high = squares.astype(BF16)
@@ -488,6 +553,39 @@
     lax.fori_loop(0, TP - 1, send_sums, 0)
     ring.drain()
 
+    def some_rows(ref, first, blocks, sent, received):
+        part = ref.at[pl.ds(first, blocks * SLOTS), pl.ds(0, 128)]
+        return pltpu.make_async_remote_copy(
+            src_ref=part,
+            dst_ref=part,
+            send_sem=one.at[sent],
+            recv_sem=received,
+            device_id=((sp + 1) % SP, tp),
+            device_id_type=MESH,
+        )
+
+    def either(test, less, more):
+        @pl.when(test)
+        def _():
+            less()
+
+        @pl.when(jnp.logical_not(test))
+        def _():
+            more()
+
+    for step in (1, 2):
+        for ring in spread_out:
+            ring.step(step)
+    gathers = []
+    for q in range(CHUNKS):
+        either(
+            sp // per == core * CHUNKS + q,
+            lambda: some_rows(xx, 0, 2 * per - 1, 8, dr.at[q]).wait_recv(),
+            lambda: some_rows(xx, 0, 2 * per, 8, dr.at[q]).wait_recv(),
+        )
+        gathers.append(Ring(xx, q * size, size, sems, 4 + q, pair=True))
+        gathers[-1].start()
+
     all_tiles(sq, 6).wait_recv()
     total = sq[0]
     for j in range(1, TP):
@@ -495,68 +593,31 @@
     line = jnp.concatenate([total[0:1], total[1:2], total[2:3]], axis=1)
     parts = stacked(three(line)).astype(BF16)
     same = one_hot((T, 384), lambda row, col: row == col)
-    upright = lax.dot_general(same, parts, dims, preferred_element_type=F32)
+    upright = across(same, parts)
     scale = lax.rsqrt((upright[:, 0:1] + upright[:, 1:2] + upright[:, 2:3]) / D + 1e-06)
-    own = (am[...].astype(F32) * scale * after_ref[...]).astype(BF16)
-    ff[:, mine] = own
-    dd[...] = dot(pp[...], own).astype(BF16)
-
-    def rows_of(i):
-        return pl.ds(pl.multiple_of(i * SLOTS, SLOTS), SLOTS)
-
-    def deliver(k, source):
+    lane = lax.broadcasted_iota(jnp.int32, (T, 128), 1)
+    parts = jnp.zeros((T, 128), F32)
+    for k, part in enumerate(three(scale)):
+        parts = jnp.where(lane == k, part, parts)
+    ss[...] = dot(pp[...], parts.astype(BF16)).astype(BF16)
+
+    def send_scale(k, carry):
         target = (sp + k) % SP
-        return pltpu.make_async_remote_copy(
-            src_ref=dd.at[rows_of(target)],
-            dst_ref=xx.at[rows_of(source), mine],
-            send_sem=one.at[8],
-            recv_sem=dr.at[source // (SP // CHUNKS)],
+        pltpu.make_async_remote_copy(
+            src_ref=ss.at[rows_of(target)],
+            dst_ref=sl.at[rows_of(local)],
+            send_sem=one.at[14],
+            recv_sem=one.at[15],
             device_id=(target, tp),
             device_id_type=MESH,
-        )
-
-    def send_rows(k, carry):
-        deliver(k, sp).start()
+        ).start()
         return carry
 
-    lax.fori_loop(1, SP, send_rows, 0)
-    xx[rows_of(sp), mine] = dd[rows_of(sp)]
-
-    spread_out = [Ring(ff, i * HALF, HALF, sems, 1 + i) for i in range(2)]
-    for ring in spread_out:
-        ring.start()
-
-    size = ROWS // CHUNKS
-    per = SP // CHUNKS
-
-    def some_rows(ref, first, blocks, sent, received):
-        part = ref.at[pl.ds(first, blocks * SLOTS), pl.ds(0, 128)]
-        return pltpu.make_async_remote_copy(
-            src_ref=part,
-            dst_ref=part,
-            send_sem=one.at[sent],
-            recv_sem=received,
-            device_id=((sp + 1) % SP, tp),
-            device_id_type=MESH,
-        )
-
-    def wait_rows(q):
-        @pl.when(sp // per == q)
-        def _():
-            some_rows(xx, q * size, per - 1, 8, dr.at[q]).wait_recv()
-
-        @pl.when(sp // per != q)
-        def _():
-            some_rows(xx, q * size, per, 8, dr.at[q]).wait_recv()
-
-    for step in (1, 2):
-        for ring in spread_out:
-            ring.step(step)
-    gathers = []
-    for q in range(CHUNKS):
-        wait_rows(q)
-        gathers.append(Ring(xx, q * size, size, sems, 4 + q))
-        gathers[-1].start()
+    @pl.when(side_of == core)
+    def _():
+        lax.fori_loop(1, SP, send_scale, 0)
+        sl[rows_of(local), :] = ss[rows_of(sp), :]
+
     for step in (3, 4):
         for ring in spread_out:
             ring.step(step)
@@ -566,7 +627,7 @@
         ring.finish()
     loads[4].wait()
     loads[5].wait()
-    both = dot(ff[...], wc[...])
+    both = dot(ff[...], wc[...]) * scale
     sh[:, mine] = (jax.nn.silu(both[:, 0:128]) * both[:, 128:256]).astype(BF16)
     hidden_out = Ring(sh, 0, T, sems, 3)
     hidden_out.start()
@@ -575,15 +636,23 @@
             ring.step(step)
         hidden_out.step(step - 1)
 
-    loads[1].wait()
-    loads[2].wait()
+    weights = wx.at[:, pl.ds(0, 384)]
+    to_other(weights).wait_recv()
+    either(
+        side_of == core,
+        lambda: some_rows(sl, 0, SP // 2 - 1, 14, one.at[15]).wait_recv(),
+        lambda: some_rows(sl, 0, SP // 2, 14, one.at[15]).wait_recv(),
+    )
+    chip = pl.ds(pl.multiple_of(y * 256, 256), 256)
     hiddens = []
     for q in range(CHUNKS):
-        gathers[q].finish()
         at = pl.ds(q * size, size)
+        level = sl[at, :].astype(F32)
+        level = level[:, 0:1] + level[:, 1:2] + level[:, 2:3]
         both = dot(xx[at, :], wx[...])
-        hh[at, mine] = (jax.nn.silu(both[:, 0:128]) * both[:, 128:256]).astype(BF16)
-        hiddens.append(Ring(hh, q * size, size, sems, 4 + CHUNKS + q))
+        both = both * level
+        hh[at, chip] = (jax.nn.silu(both[:, 0:256]) * both[:, 256:512]).astype(BF16)
+        hiddens.append(Ring(hh, q * size, size, sems, 4 + CHUNKS + q, pair=True))
         hiddens[-1].start()
     hidden_out.step(4)
     for side in range(2):
@@ -593,7 +662,17 @@
     all_columns().wait_send()
     all_tiles(ft, 4).wait_send()
     all_tiles(sq, 6).wait_send()
-    some_rows(dd, 0, SP - 1, 8, one.at[9]).wait_send()
+    either(
+        side_of == core,
+        lambda: some_rows(dd, 0, SP - 1, 8, one.at[9]).wait_send(),
+        lambda: some_rows(dd, 0, SP, 8, one.at[9]).wait_send(),
+    )
+
+    @pl.when(side_of == core)
+    def _():
+        some_rows(dd, 0, SP - 1, 14, one.at[9]).wait_send()
+
+    to_other(weights).wait_send()
     for ring in spread_out + gathers:
         ring.drain()
     for ring in hiddens:
@@ -607,40 +686,49 @@
         for ring in hiddens:
             ring.step(step)
 
-    def give(i, source):
-        return pltpu.make_async_remote_copy(
-            src_ref=oo.at[rows_of(i)],
-            dst_ref=ret.at[rows_of(source)],
+    def give(i, to_core):
+        return pltpu.make_async_remote_copy(
+            src_ref=oo.at[rows_of(i), lanes_of(to_core)],
+            dst_ref=ret.at[rows_of(sp)],
             send_sem=one.at[10],
             recv_sem=one.at[11],
-            device_id=(i, tp),
-            device_id_type=MESH,
-        )
-
-    loads[3].wait()
+            device_id=(core * (SP // 2) + i, y * 2 + to_core),
+            device_id_type=MESH,
+        )
+
     for q in range(CHUNKS):
-        hiddens[q].finish()
-
         at = pl.ds(q * size, size)
         oo[at, :] = dot(hh[at, :], wl[...]).astype(BF16)
 
         def send_back(k, carry):
             i = q * per + (sp + k) % per
-
-            @pl.when(i != sp)
+            here = core * (SP // 2) + i == sp
+
+            @pl.when(jnp.logical_not(here))
             def _():
-                give(i, sp).start()
-
+                give(i, core).start()
+
+            give(i, 1 - core).start()
             return carry
 
         lax.fori_loop(0, per, send_back, 0)
-    ret[rows_of(sp), :] = oo[rows_of(sp), :]
+
+    @pl.when(side_of == core)
+    def _():
+        ret[rows_of(sp), :] = oo[rows_of(local), lanes_of(core)]
 
     for ring in hiddens:
         ring.drain()
-
-    some_rows(ret, 0, SP - 1, 10, one.at[11]).wait_recv()
-    some_rows(oo, 0, SP - 1, 10, one.at[11]).wait_send()
+    either(
+        side_of == core,
+        lambda: some_rows(ret, 0, SP - 1, 10, one.at[11]).wait_recv(),
+        lambda: some_rows(ret, 0, SP, 10, one.at[11]).wait_recv(),
+    )
+    either(
+        side_of == core,
+        lambda: some_rows(ret, 0, SP - 1, 10, one.at[11]).wait_send(),
+        lambda: some_rows(ret, 0, SP, 10, one.at[11]).wait_send(),
+    )
     routed = dot(qhi[...], ret[...]) + dot(qlo[...], ret[...])
     out_ref[...] = (am[...].astype(F32) + out_ref[...].astype(F32) + routed).astype(BF16)
 
@@ -680,9 +768,9 @@
             space(TP, 8, 128, kind=F32),
             space(8, 128, kind=F32),
             space(1024, 128),
+            space(D, 512),
             space(D, 256),
             space(D, 256),
-            space(D, 128),
             space(D, 128),
             space(D, 256),
             space(HALF, D),
@@ -690,15 +778,17 @@
             space(T, 128),
             space(T, D),
             space(T, D),
-            space(ROWS, D),
-            space(ROWS, D),
+            space(ROWS // 2, D),
+            space(ROWS // 2, D),
             space(ROWS, 128),
             space(ROWS, 128),
+            space(ROWS // 2, 128),
+            space(ROWS // 2, 256),
             space(ROWS, 128),
             space(ROWS, T),
             space(T, ROWS),
             space(T, ROWS),
-            dma((9,)), dma((6,)), dma((6,)), dma((12,)), dma((CHUNKS,)), dma((rings, 2)), dma((rings, 8)),
+            dma((9,)), dma((6,)), dma((6,)), dma((16,)), dma((CHUNKS,)), dma((rings, 2)), dma((rings, 8)),
         ],
         compiler_params=pltpu.CompilerParams(collective_id=0, has_side_effects=True),
         name="mixer_experts",

time: 121 us -> 118 us (0.975)
  Pallas kernels: 118 us -> 115 us
    pallas_call x1, Pallas kernels: 118 us -> 115 us  [whole(): pl.pallas_call(kernel, out_shape=jax.ShapeDtypeStruct((T, 128), BF16), in...]
where the time goes in v4:
time: 118 us
  Pallas kernels  115 us (97%)
  local copies, waits for them, and re-layouts  1.53 us (1%)
    pallas_call x1, Pallas kernels, whole(): pl.pallas_call(kernel, out_shape=jax.ShapeDtypeStruct((T, 128), BF16), in...  115 us

profile of v4, /device:TPU:1, one launch (start us, length us, event | category | flops | bytes accessed | tf_op | source)
XLA Modules:
  0.0 117.6 jit_solution(5445669527809570545)
XLA Ops:
  0.7 115.4 %mixer_experts.1 = bf16[320,128]{1,0:T(8,128)(2,1)} custom-call(bf16[64,320]{1,0:T(8,128)(2,1)} %bitcast.12, bf16[64,320]{1,0:T(8,128)(2,1)} %bitcast.13, bf16[2,320]{1,0:T(2,128)(2,1)} %bitcast.17, f32[1,2]{1,0:T(1,128)} %bitcast.18, f32[1,2]{1,0:T(1,128)} %bitcast.19, f32[2,1,320]{2,1,0:T(1,128)} %bitcast.14, f32[1,1]{1,0:T(1,128)} %bitcast.11.byp_ref, ...), custom_call_target="tpu_custom_call" | custom-call | tf_op jit(solution)/shard_map/mixer_experts/pallas_call | solution.py:745
  116.1 1.5 %copy.27 = bf16[320,128]{1,0:T(8,128)(2,1)} copy(bf16[320,128]{1,0:T(8,128)(2,1)} %mixer_experts.1) | data formatting | bytes 163840

commit v5 on v4

--- a/solution.py
+++ b/solution.py
@@ -18,6 +18,8 @@
 HALF = T // 2
 SLOTS = 32
 ROWS = SP * SLOTS
+CAP = 30
+SPLITS = 4
 BLOCK = 80
 CHUNKS = 2
 MESH = pl.DeviceIdType.MESH
@@ -44,8 +46,8 @@
             column = column + core
         first, rows = self.first, self.rows
         if half is not None:
-            rows = rows // 2
-            first = first + half * rows
+            cut = (rows // 2 + 15) // 16 * 16
+            first, rows = (first, cut) if half == 0 else (first + cut, rows - cut)
         return self.buf.at[pl.ds(first, rows), pl.ds(pl.multiple_of(column * 128, 128), width)]
 
     def along(self, way, step, chip, far):
@@ -151,12 +153,12 @@
     bm_hbm, cm_hbm, blender_hbm, valve_hbm, raising_hbm, lowering_hbm, cvalve_hbm, craising_hbm, clowering_hbm,
     out_ref,
     xpad, braw, craw, hx, hb, hc, bext, cext, gap, cv, mixed, fto,
-    st_ref, rx, tb, rz, ft, sq, so, wb, wx, wc, wl, wcl, wide, bn, nn, am, ff, sh, xx, hh, dd, ss, sl, oo, ret, pp, qhi, qlo,
+    st_ref, rx, tb, rz, ft, sq, so, wb, wx, wc, wl, wcl, wide, bn, nn, am, ff, sh, xl, xx, hh, tot, low, dd, ss, sl, oo, ret, pp, qhi, qlo,
     wsem, hs, hr, one, dr, rsem, rrecv,
 ):
     sp, tp = lax.axis_index("sp"), lax.axis_index("tp")
     z, x = sp // NX, sp % NX
-    y, core, side_of = tp // 2, tp % 2, sp // (SP // 2)
+    y, core, side_of = tp // 2, tp % 2, z % 2
 
     barrier = pltpu.get_barrier_semaphore()
 
@@ -445,7 +447,7 @@
     ).astype(BF16)
 
     sems = (rsem, rrecv)
-    ring = Ring(bn, 0, HALF, sems, 0, direct=True)
+    ring = Ring(bn, 0, HALF, sems, 5 + SPLITS, direct=True)
     ring.start()
 
     def all_tiles(ref, at):
@@ -486,35 +488,38 @@
         return pl.ds(pl.multiple_of(i * SLOTS, SLOTS), SLOTS)
 
     per = SP // 2 // CHUNKS
-    size = per * SLOTS
-    local = sp % (SP // 2)
+    local = (x % 2) * 8 + (x // 2) * 4 + z // 2
 
     def deliver(k):
         target = (sp + k) % SP
         return pltpu.make_async_remote_copy(
             src_ref=dd.at[rows_of(target)],
-            dst_ref=xx.at[rows_of(local), mine],
+            dst_ref=xl.at[rows_of(local), lanes_of(core)],
             send_sem=one.at[8],
             recv_sem=dr.at[local // per],
             device_id=(target, y * 2 + side_of),
             device_id_type=MESH,
         )
 
-    def send_rows(k, carry):
-        deliver(k).start()
+    def outward(m):
+        return SP // 2 + (m // 2 + m % 2) * (1 - 2 * (m % 2))
+
+    def send_rows(m, carry):
+        deliver(outward(m)).start()
         return carry
 
-    lax.fori_loop(1, SP, send_rows, 0)
+    lax.fori_loop(0, SP - 1, send_rows, 0)
 
     @pl.when(side_of == core)
     def _():
-        xx[rows_of(local), mine] = dd[rows_of(sp)]
+        xl[rows_of(local), lanes_of(core)] = dd[rows_of(sp)]
 
     @pl.when(side_of != core)
     def _():
         deliver(0).start()
 
-    spread_out = [Ring(ff, i * HALF, HALF, sems, 1 + i) for i in range(2)]
+    cells = T // SPLITS
+    spread_out = [Ring(ff, i * cells, cells, sems, 4 + i) for i in range(SPLITS)]
     for spreading in spread_out:
         spreading.start()
 
@@ -576,16 +581,6 @@
     for step in (1, 2):
         for ring in spread_out:
             ring.step(step)
-    gathers = []
-    for q in range(CHUNKS):
-        either(
-            sp // per == core * CHUNKS + q,
-            lambda: some_rows(xx, 0, 2 * per - 1, 8, dr.at[q]).wait_recv(),
-            lambda: some_rows(xx, 0, 2 * per, 8, dr.at[q]).wait_recv(),
-        )
-        gathers.append(Ring(xx, q * size, size, sems, 4 + q, pair=True))
-        gathers[-1].start()
-
     all_tiles(sq, 6).wait_recv()
     total = sq[0]
     for j in range(1, TP):
@@ -601,8 +596,8 @@
         parts = jnp.where(lane == k, part, parts)
     ss[...] = dot(pp[...], parts.astype(BF16)).astype(BF16)
 
-    def send_scale(k, carry):
-        target = (sp + k) % SP
+    def send_scale(m, carry):
+        target = (sp + outward(m)) % SP
         pltpu.make_async_remote_copy(
             src_ref=ss.at[rows_of(target)],
             dst_ref=sl.at[rows_of(local)],
@@ -615,26 +610,48 @@
 
     @pl.when(side_of == core)
     def _():
-        lax.fori_loop(1, SP, send_scale, 0)
+        lax.fori_loop(0, SP - 1, send_scale, 0)
         sl[rows_of(local), :] = ss[rows_of(sp), :]
 
-    for step in (3, 4):
-        for ring in spread_out:
-            ring.step(step)
-    for ring in gathers:
-        ring.step(1)
+    for ring in spread_out:
+        ring.step(3)
+    chip = pl.ds(pl.multiple_of(y * 256, 256), 256)
+    packed_rows = per * CAP
+    dense = one_hot((packed_rows, per * SLOTS), lambda row, col: row // CAP * SLOTS + row % CAP == col)
+    gathers = []
+    for q in range(CHUNKS):
+        either(
+            jnp.logical_and(side_of == core, x % 2 == q),
+            lambda: some_rows(xl, 0, 2 * per - 1, 8, dr.at[q]).wait_recv(),
+            lambda: some_rows(xl, 0, 2 * per, 8, dr.at[q]).wait_recv(),
+        )
+        at = pl.ds(q * packed_rows, packed_rows)
+        xx[at, chip] = dot(dense, xl[pl.ds(q * per * SLOTS, per * SLOTS), :]).astype(BF16)
+        gathers.append(Ring(xx, q * packed_rows, packed_rows, sems, q, pair=True))
+        gathers[-1].start()
+    for ring in spread_out:
+        ring.step(4)
     for ring in spread_out:
         ring.finish()
     loads[4].wait()
     loads[5].wait()
     both = dot(ff[...], wc[...]) * scale
     sh[:, mine] = (jax.nn.silu(both[:, 0:128]) * both[:, 128:256]).astype(BF16)
-    hidden_out = Ring(sh, 0, T, sems, 3)
+    hidden_out = Ring(sh, 0, T, sems, 4 + SPLITS)
     hidden_out.start()
-    for step in (2, 3, 4):
+    for step in (1, 2, 3):
         for ring in gathers:
             ring.step(step)
-        hidden_out.step(step - 1)
+        if step > 1:
+            hidden_out.step(step - 1)
+
+    def chips(first, count, total, buf, at, weight):
+        def add(k, carry):
+            part = pl.ds(pl.multiple_of((y + k) % NY * 256, 256), 256)
+            total[at, :] += dot(buf[at, part], weight[part, :])
+            return carry
+
+        lax.fori_loop(first, first + count, add, 0)
 
     weights = wx.at[:, pl.ds(0, 384)]
     to_other(weights).wait_recv()
@@ -643,16 +660,22 @@
         lambda: some_rows(sl, 0, SP // 2 - 1, 14, one.at[15]).wait_recv(),
         lambda: some_rows(sl, 0, SP // 2, 14, one.at[15]).wait_recv(),
     )
-    chip = pl.ds(pl.multiple_of(y * 256, 256), 256)
+    tot[...] = jnp.zeros(tot.shape, F32)
+    levels = []
+    for q in range(CHUNKS):
+        at = pl.ds(q * packed_rows, packed_rows)
+        chips(NY - 3, NY - 1, tot, xx, at, wx)
+        level = dot(dense, sl[pl.ds(q * per * SLOTS, per * SLOTS), :])
+        levels.append(level[:, 0:1] + level[:, 1:2] + level[:, 2:3])
+    hidden_out.step(3)
     hiddens = []
     for q in range(CHUNKS):
-        at = pl.ds(q * size, size)
-        level = sl[at, :].astype(F32)
-        level = level[:, 0:1] + level[:, 1:2] + level[:, 2:3]
-        both = dot(xx[at, :], wx[...])
-        both = both * level
+        gathers[q].step(4)
+        at = pl.ds(q * packed_rows, packed_rows)
+        chips(NY // 2, 1, tot, xx, at, wx)
+        both = tot[at, :] * levels[q]
         hh[at, chip] = (jax.nn.silu(both[:, 0:256]) * both[:, 256:512]).astype(BF16)
-        hiddens.append(Ring(hh, q * size, size, sems, 4 + CHUNKS + q, pair=True))
+        hiddens.append(Ring(hh, q * packed_rows, packed_rows, sems, 2 + q, pair=True))
         hiddens[-1].start()
     hidden_out.step(4)
     for side in range(2):
@@ -682,9 +705,13 @@
     shared = dot(sh[...], wcl[...]).astype(BF16).astype(F32)
     out_ref[...] = shared.astype(BF16)
     hidden_out.drain()
-    for step in (2, 3, 4):
+    for step in (2, 3):
         for ring in hiddens:
             ring.step(step)
+    low[...] = jnp.zeros(low.shape, F32)
+    for q in range(CHUNKS):
+        chips(NY - 3, NY - 1, low, hh, pl.ds(q * packed_rows, packed_rows), wl)
+    loose = one_hot((per * SLOTS, packed_rows), lambda row, col: col // CAP * SLOTS + col % CAP == row)
 
     def give(i, to_core):
         return pltpu.make_async_remote_copy(
@@ -692,17 +719,20 @@
             dst_ref=ret.at[rows_of(sp)],
             send_sem=one.at[10],
             recv_sem=one.at[11],
-            device_id=(core * (SP // 2) + i, y * 2 + to_core),
+            device_id=(((i % 4) * 2 + core) * NX + i // 4 % 2 * 2 + i // 8, y * 2 + to_core),
             device_id_type=MESH,
         )
 
     for q in range(CHUNKS):
-        at = pl.ds(q * size, size)
-        oo[at, :] = dot(hh[at, :], wl[...]).astype(BF16)
+        hiddens[q].step(4)
+        at = pl.ds(q * packed_rows, packed_rows)
+        chips(NY // 2, 1, low, hh, at, wl)
+        oo[pl.ds(q * per * SLOTS, per * SLOTS), :] = dot(loose, low[at, :].astype(BF16)).astype(BF16)
 
         def send_back(k, carry):
-            i = q * per + (sp + k) % per
-            here = core * (SP // 2) + i == sp
+            turn = k // 2
+            i = q * per + k % 2 * 4 + (z // 2 + 6 + (turn // 2 + turn % 2) * (1 - 2 * (turn % 2))) % 4
+            here = jnp.logical_and(side_of == core, i == local)
 
             @pl.when(jnp.logical_not(here))
             def _():
@@ -736,7 +766,7 @@
 def whole(*operands):
     vmem = pl.BlockSpec(memory_space=pltpu.VMEM)
     hbm = pl.BlockSpec(memory_space=pl.ANY)
-    rings = 4 + 2 * CHUNKS
+    rings = 6 + SPLITS
     dma = pltpu.SemaphoreType.DMA
 
     def space(*shape, kind=BF16):
@@ -778,8 +808,11 @@
             space(T, 128),
             space(T, D),
             space(T, D),
-            space(ROWS // 2, D),
-            space(ROWS // 2, D),
+            space(ROWS // 2, 256),
+            space(SP // 2 * CAP, D),
+            space(SP // 2 * CAP, D),
+            space(SP // 2 * CAP, 512, kind=F32),
+            space(SP // 2 * CAP, 256, kind=F32),
             space(ROWS, 128),
             space(ROWS, 128),
             space(ROWS // 2, 128),

time: 118 us -> 113 us (0.958)
  Pallas kernels: 115 us -> 111 us
    pallas_call x1, Pallas kernels: 115 us -> 111 us  [whole(): pl.pallas_call(kernel, out_shape=jax.ShapeDtypeStruct((T, 128), BF16), in...]
where the time goes in v5:
time: 113 us
  Pallas kernels  111 us (98%)
  local copies, waits for them, and re-layouts  1.53 us (1%)
    pallas_call x1, Pallas kernels, whole(): pl.pallas_call(kernel, out_shape=jax.ShapeDtypeStruct((T, 128), BF16), in...  111 us

profile of v5, /device:TPU:1, one launch (start us, length us, event | category | flops | bytes accessed | tf_op | source)
XLA Modules:
  0.0 113.2 jit_solution(16925678903686554376)
XLA Ops:
  0.7 111.0 %mixer_experts.1 = bf16[320,128]{1,0:T(8,128)(2,1)} custom-call(bf16[64,320]{1,0:T(8,128)(2,1)} %bitcast.12, bf16[64,320]{1,0:T(8,128)(2,1)} %bitcast.13, bf16[2,320]{1,0:T(2,128)(2,1)} %bitcast.17, f32[1,2]{1,0:T(1,128)} %bitcast.18, f32[1,2]{1,0:T(1,128)} %bitcast.19, f32[2,1,320]{2,1,0:T(1,128)} %bitcast.14, f32[1,1]{1,0:T(1,128)} %bitcast.11.byp_ref, ...), custom_call_target="tpu_custom_call" | custom-call | tf_op jit(solution)/shard_map/mixer_experts/pallas_call | solution.py:775
  111.7 1.5 %copy.27 = bf16[320,128]{1,0:T(8,128)(2,1)} copy(bf16[320,128]{1,0:T(8,128)(2,1)} %mixer_experts.1) | data formatting | bytes 163840

commit v6 on v5

--- a/solution.py
+++ b/solution.py
@@ -31,8 +31,9 @@
 
 
 class Ring:
-    def __init__(self, buf, first, rows, sems, index, direct=False, pair=False):
-        self.buf, self.first, self.rows, self.direct, self.pair = buf, first, rows, direct, pair
+    def __init__(self, buf, first, rows, sems, index, direct=False, pair=False, last=4):
+        self.buf, self.first, self.rows = buf, first, rows
+        self.direct, self.pair, self.last = direct, pair, last
         self.out, self.near = sems[0].at[index, 0], sems[0].at[index, 1]
         self.recv = sems[1].at[index]
         self.sp, tp = lax.axis_index("sp"), lax.axis_index("tp")
@@ -97,7 +98,7 @@
     def step(self, step):
         for way in (0, 1):
             self.landed(way, step).wait_recv()
-            if step < 4 and not self.direct:
+            if step < self.last and not self.direct:
                 self.hop(way, step + 1).start()
             if not self.pair:
                 self.relay(way, step).start()
@@ -106,7 +107,7 @@
         self.several(NY).wait_recv()
 
     def drain(self):
-        self.several(2 * NY - (2 if self.pair else 1)).wait_send()
+        self.several(2 * NY - (1 if not self.pair else 2 if self.last == 4 else 4)).wait_send()
 
 
 def run(rings):
@@ -153,7 +154,7 @@
     bm_hbm, cm_hbm, blender_hbm, valve_hbm, raising_hbm, lowering_hbm, cvalve_hbm, craising_hbm, clowering_hbm,
     out_ref,
     xpad, braw, craw, hx, hb, hc, bext, cext, gap, cv, mixed, fto,
-    st_ref, rx, tb, rz, ft, sq, so, wb, wx, wc, wl, wcl, wide, bn, nn, am, ff, sh, xl, xx, hh, tot, low, dd, ss, sl, oo, ret, pp, qhi, qlo,
+    st_ref, rx, tb, rz, ft, sq, so, wb, wx, wc, wl, wcl, wide, bn, nn, am, ff, sh, xl, x2, xx, hh, tot, low, dd, d2, ss, sl, oo, ret, pp, qhi, qlo,
     wsem, hs, hr, one, dr, rsem, rrecv,
 ):
     sp, tp = lax.axis_index("sp"), lax.axis_index("tp")
@@ -447,7 +448,7 @@
     ).astype(BF16)
 
     sems = (rsem, rrecv)
-    ring = Ring(bn, 0, HALF, sems, 5 + SPLITS, direct=True)
+    ring = Ring(bn, 0, HALF, sems, 6 + SPLITS, direct=True)
     ring.start()
 
     def all_tiles(ref, at):
@@ -490,13 +491,13 @@
     per = SP // 2 // CHUNKS
     local = (x % 2) * 8 + (x // 2) * 4 + z // 2
 
-    def deliver(k):
+    def deliver(k, far=0):
         target = (sp + k) % SP
         return pltpu.make_async_remote_copy(
-            src_ref=dd.at[rows_of(target)],
-            dst_ref=xl.at[rows_of(local), lanes_of(core)],
-            send_sem=one.at[8],
-            recv_sem=dr.at[local // per],
+            src_ref=(d2 if far else dd).at[rows_of(target)],
+            dst_ref=(x2 if far else xl).at[rows_of(local), lanes_of(core)],
+            send_sem=one.at[9 if far else 8],
+            recv_sem=dr.at[local // per + CHUNKS * far],
             device_id=(target, y * 2 + side_of),
             device_id_type=MESH,
         )
@@ -581,6 +582,20 @@
     for step in (1, 2):
         for ring in spread_out:
             ring.step(step)
+    chip = pl.ds(pl.multiple_of(y * 256, 256), 256)
+    packed_rows = per * CAP
+    dense = one_hot((packed_rows, per * SLOTS), lambda row, col: row // CAP * SLOTS + row % CAP == col)
+    gathers = []
+    for q in range(CHUNKS):
+        either(
+            jnp.logical_and(side_of == core, x % 2 == q),
+            lambda: some_rows(xl, 0, 2 * per - 1, 8, dr.at[q]).wait_recv(),
+            lambda: some_rows(xl, 0, 2 * per, 8, dr.at[q]).wait_recv(),
+        )
+        at = pl.ds(q * packed_rows, packed_rows)
+        xx[at, chip] = dot(dense, xl[pl.ds(q * per * SLOTS, per * SLOTS), :]).astype(BF16)
+        gathers.append(Ring(xx, q * packed_rows, packed_rows, sems, q, pair=True, last=3))
+        gathers[-1].start()
     all_tiles(sq, 6).wait_recv()
     total = sq[0]
     for j in range(1, TP):
@@ -615,35 +630,39 @@
 
     for ring in spread_out:
         ring.step(3)
-    chip = pl.ds(pl.multiple_of(y * 256, 256), 256)
-    packed_rows = per * CAP
-    dense = one_hot((packed_rows, per * SLOTS), lambda row, col: row // CAP * SLOTS + row % CAP == col)
-    gathers = []
-    for q in range(CHUNKS):
-        either(
-            jnp.logical_and(side_of == core, x % 2 == q),
-            lambda: some_rows(xl, 0, 2 * per - 1, 8, dr.at[q]).wait_recv(),
-            lambda: some_rows(xl, 0, 2 * per, 8, dr.at[q]).wait_recv(),
-        )
-        at = pl.ds(q * packed_rows, packed_rows)
-        xx[at, chip] = dot(dense, xl[pl.ds(q * per * SLOTS, per * SLOTS), :]).astype(BF16)
-        gathers.append(Ring(xx, q * packed_rows, packed_rows, sems, q, pair=True))
-        gathers[-1].start()
+    for ring in gathers:
+        ring.step(1)
     for ring in spread_out:
         ring.step(4)
+
+    opposite = (y + NY // 2) % NY
+    d2[...] = dot(pp[...], ff[:, lanes_of(opposite * 2 + core)]).astype(BF16)
+
+    def send_more(m, carry):
+        deliver(outward(m), 1).start()
+        return carry
+
+    lax.fori_loop(0, SP - 1, send_more, 0)
+
+    @pl.when(side_of == core)
+    def _():
+        x2[rows_of(local), lanes_of(core)] = d2[rows_of(sp)]
+
+    @pl.when(side_of != core)
+    def _():
+        deliver(0, 1).start()
+
     for ring in spread_out:
         ring.finish()
     loads[4].wait()
     loads[5].wait()
     both = dot(ff[...], wc[...]) * scale
     sh[:, mine] = (jax.nn.silu(both[:, 0:128]) * both[:, 128:256]).astype(BF16)
-    hidden_out = Ring(sh, 0, T, sems, 4 + SPLITS)
-    hidden_out.start()
-    for step in (1, 2, 3):
-        for ring in gathers:
-            ring.step(step)
-        if step > 1:
-            hidden_out.step(step - 1)
+    shared_out = [Ring(sh, i * HALF, HALF, sems, 4 + SPLITS + i) for i in range(2)]
+    for ring in shared_out:
+        ring.start()
+    for ring in gathers:
+        ring.step(2)
 
     def chips(first, count, total, buf, at, weight):
         def add(k, carry):
@@ -664,20 +683,30 @@
     levels = []
     for q in range(CHUNKS):
         at = pl.ds(q * packed_rows, packed_rows)
-        chips(NY - 3, NY - 1, tot, xx, at, wx)
+        chips(NY - 2, NY - 3, tot, xx, at, wx)
+        either(
+            jnp.logical_and(side_of == core, x % 2 == q),
+            lambda: some_rows(x2, 0, 2 * per - 1, 9, dr.at[CHUNKS + q]).wait_recv(),
+            lambda: some_rows(x2, 0, 2 * per, 9, dr.at[CHUNKS + q]).wait_recv(),
+        )
+        turned = pl.ds(pl.multiple_of(opposite * 256, 256), 256)
+        xx[at, turned] = dot(dense, x2[pl.ds(q * per * SLOTS, per * SLOTS), :]).astype(BF16)
+        chips(NY // 2, 1, tot, xx, at, wx)
         level = dot(dense, sl[pl.ds(q * per * SLOTS, per * SLOTS), :])
         levels.append(level[:, 0:1] + level[:, 1:2] + level[:, 2:3])
-    hidden_out.step(3)
     hiddens = []
     for q in range(CHUNKS):
-        gathers[q].step(4)
+        gathers[q].step(3)
+        if q == CHUNKS - 1:
+            for ring in shared_out:
+                ring.step(1)
         at = pl.ds(q * packed_rows, packed_rows)
-        chips(NY // 2, 1, tot, xx, at, wx)
+        chips(3, 1, tot, xx, at, wx)
+        chips(NY - 3, 1, tot, xx, at, wx)
         both = tot[at, :] * levels[q]
         hh[at, chip] = (jax.nn.silu(both[:, 0:256]) * both[:, 256:512]).astype(BF16)
         hiddens.append(Ring(hh, q * packed_rows, packed_rows, sems, 2 + q, pair=True))
         hiddens[-1].start()
-    hidden_out.step(4)
     for side in range(2):
         for k in range(3):
             halo(side, k).wait_send()
@@ -685,32 +714,33 @@
     all_columns().wait_send()
     all_tiles(ft, 4).wait_send()
     all_tiles(sq, 6).wait_send()
-    either(
-        side_of == core,
-        lambda: some_rows(dd, 0, SP - 1, 8, one.at[9]).wait_send(),
-        lambda: some_rows(dd, 0, SP, 8, one.at[9]).wait_send(),
-    )
+    for sent in (8, 9):
+        either(
+            side_of == core,
+            lambda: some_rows(dd, 0, SP - 1, sent, one.at[16]).wait_send(),
+            lambda: some_rows(dd, 0, SP, sent, one.at[16]).wait_send(),
+        )
 
     @pl.when(side_of == core)
     def _():
-        some_rows(dd, 0, SP - 1, 14, one.at[9]).wait_send()
+        some_rows(dd, 0, SP - 1, 14, one.at[16]).wait_send()
 
     to_other(weights).wait_send()
     for ring in spread_out + gathers:
         ring.drain()
-    for ring in hiddens:
-        ring.step(1)
-    hidden_out.finish()
-    loads[6].wait()
-    shared = dot(sh[...], wcl[...]).astype(BF16).astype(F32)
-    out_ref[...] = shared.astype(BF16)
-    hidden_out.drain()
-    for step in (2, 3):
+    low[...] = jnp.zeros(low.shape, F32)
+    for step in (1, 2, 3):
         for ring in hiddens:
             ring.step(step)
-    low[...] = jnp.zeros(low.shape, F32)
-    for q in range(CHUNKS):
-        chips(NY - 3, NY - 1, low, hh, pl.ds(q * packed_rows, packed_rows), wl)
+        if step == 3:
+            for ring in shared_out:
+                ring.step(2)
+        for q in range(CHUNKS):
+            at = pl.ds(q * packed_rows, packed_rows)
+            if step == 1:
+                chips(NY, 1, low, hh, at, wl)
+            chips(step, 1, low, hh, at, wl)
+            chips(NY - step, 1, low, hh, at, wl)
     loose = one_hot((per * SLOTS, packed_rows), lambda row, col: col // CAP * SLOTS + col % CAP == row)
 
     def give(i, to_core):
@@ -747,7 +777,15 @@
     def _():
         ret[rows_of(sp), :] = oo[rows_of(local), lanes_of(core)]
 
-    for ring in hiddens:
+    for step in (3, 4):
+        for ring in shared_out:
+            ring.step(step)
+    for ring in shared_out:
+        ring.finish()
+    loads[6].wait()
+    shared = dot(sh[...], wcl[...]).astype(BF16).astype(F32)
+    out_ref[...] = shared.astype(BF16)
+    for ring in hiddens + shared_out:
         ring.drain()
     either(
         side_of == core,
@@ -766,7 +804,7 @@
 def whole(*operands):
     vmem = pl.BlockSpec(memory_space=pltpu.VMEM)
     hbm = pl.BlockSpec(memory_space=pl.ANY)
-    rings = 6 + SPLITS
+    rings = 7 + SPLITS
     dma = pltpu.SemaphoreType.DMA
 
     def space(*shape, kind=BF16):
@@ -809,10 +847,12 @@
             space(T, D),
             space(T, D),
             space(ROWS // 2, 256),
+            space(ROWS // 2, 256),
             space(SP // 2 * CAP, D),
             space(SP // 2 * CAP, D),
             space(SP // 2 * CAP, 512, kind=F32),
             space(SP // 2 * CAP, 256, kind=F32),
+            space(ROWS, 128),
             space(ROWS, 128),
             space(ROWS, 128),
             space(ROWS // 2, 128),
@@ -821,7 +861,7 @@
             space(ROWS, T),
             space(T, ROWS),
             space(T, ROWS),
-            dma((9,)), dma((6,)), dma((6,)), dma((16,)), dma((CHUNKS,)), dma((rings, 2)), dma((rings, 8)),
+            dma((9,)), dma((6,)), dma((6,)), dma((17,)), dma((2 * CHUNKS,)), dma((rings, 2)), dma((rings, 8)),
         ],
         compiler_params=pltpu.CompilerParams(collective_id=0, has_side_effects=True),
         name="mixer_experts",

time: 113 us -> 106 us (0.938)
  Pallas kernels: 111 us -> 103 us
    pallas_call x1, Pallas kernels: 111 us -> 103 us  [whole(): pl.pallas_call(kernel, out_shape=jax.ShapeDtypeStruct((T, 128), BF16), in...]
where the time goes in v6:
time: 106 us
  Pallas kernels  103 us (97%)
  local copies, waits for them, and re-layouts  1.53 us (1%)
    pallas_call x1, Pallas kernels, whole(): pl.pallas_call(kernel, out_shape=jax.ShapeDtypeStruct((T, 128), BF16), in...  103 us

profile of v6, /device:TPU:1, one launch (start us, length us, event | category | flops | bytes accessed | tf_op | source)
XLA Modules:
  0.0 105.6 jit_solution(9517111921978878577)
XLA Ops:
  0.7 103.4 %mixer_experts.1 = bf16[320,128]{1,0:T(8,128)(2,1)} custom-call(bf16[64,320]{1,0:T(8,128)(2,1)} %bitcast.12, bf16[64,320]{1,0:T(8,128)(2,1)} %bitcast.13, bf16[2,320]{1,0:T(2,128)(2,1)} %bitcast.17, f32[1,2]{1,0:T(1,128)} %bitcast.18, f32[1,2]{1,0:T(1,128)} %bitcast.19, f32[2,1,320]{2,1,0:T(1,128)} %bitcast.14, f32[1,1]{1,0:T(1,128)} %bitcast.11.byp_ref, ...), custom_call_target="tpu_custom_call" | custom-call | tf_op jit(solution)/shard_map/mixer_experts/pallas_call | solution.py:813
  104.0 1.5 %copy.27 = bf16[320,128]{1,0:T(8,128)(2,1)} copy(bf16[320,128]{1,0:T(8,128)(2,1)} %mixer_experts.1) | data formatting | bytes 163840

commit v7 on v6

--- a/solution.py
+++ b/solution.py
@@ -110,12 +110,6 @@
         self.several(2 * NY - (1 if not self.pair else 2 if self.last == 4 else 4)).wait_send()
 
 
-def run(rings):
-    for step in range(1, 5):
-        for ring in rings:
-            ring.step(step)
-
-
 def stacked(rows):
     level = lax.broadcasted_iota(jnp.int32, (8, rows[0].shape[1]), 0)
     total = jnp.zeros(level.shape, F32)
@@ -154,7 +148,7 @@
     bm_hbm, cm_hbm, blender_hbm, valve_hbm, raising_hbm, lowering_hbm, cvalve_hbm, craising_hbm, clowering_hbm,
     out_ref,
     xpad, braw, craw, hx, hb, hc, bext, cext, gap, cv, mixed, fto,
-    st_ref, rx, tb, rz, ft, sq, so, wb, wx, wc, wl, wcl, wide, bn, nn, am, ff, sh, xl, x2, xx, hh, tot, low, dd, d2, ss, sl, oo, ret, pp, qhi, qlo,
+    st_ref, rx, tb, rz, ft, sq, so, wb, wx, wc, wl, wcl, wide, bn, nn, am, ff, sh, xl, x2, xx, hh, tot, low, dd, d2, ss, sl, outs, theirs, oo, ret, pp, qhi, qlo,
     wsem, hs, hr, one, dr, rsem, rrecv,
 ):
     sp, tp = lax.axis_index("sp"), lax.axis_index("tp")
@@ -183,9 +177,9 @@
         pltpu.make_async_copy(valve_hbm.at[0], wx.at[:, lanes_of(core)], wsem.at[1]),
         pltpu.make_async_copy(raising_hbm.at[0], wx.at[:, lanes_of(core + 2)], wsem.at[2]),
         pltpu.make_async_copy(lowering_hbm.at[0], wl.at[:, lanes_of(core)], wsem.at[3]),
-        pltpu.make_async_copy(cvalve_hbm, wc.at[:, pl.ds(0, 128)], wsem.at[4]),
-        pltpu.make_async_copy(craising_hbm, wc.at[:, pl.ds(128, 128)], wsem.at[5]),
-        pltpu.make_async_copy(clowering_hbm, wcl, wsem.at[6]),
+        pltpu.make_async_copy(cvalve_hbm, wc.at[:, lanes_of(core)], wsem.at[4]),
+        pltpu.make_async_copy(craising_hbm, wc.at[:, lanes_of(core + 2)], wsem.at[5]),
+        pltpu.make_async_copy(clowering_hbm, wcl.at[:, lanes_of(core)], wsem.at[6]),
     ]
     grouped = [
         pltpu.make_async_copy(bm_hbm.at[:, at_group], braw, wsem.at[7]),
@@ -223,6 +217,29 @@
     def send_tile(k, carry):
         tile(k, tp).start()
         return carry
+
+    for load in grouped:
+        load.wait()
+    pl.semaphore_wait(barrier, TP + SP - 2)
+
+    def halo(side, k):
+        there = (sp + 1) % SP if side == 0 else (sp + SP - 1) % SP
+        rows = pl.ds(T - 16, 16) if side == 0 else pl.ds(0, 16)
+        lanes = pl.ds(256, 128) if side == 0 else pl.ds(0, 128)
+        source = (xpad.at[:, lanes], braw.at[rows], craw.at[rows])[k]
+        return pltpu.make_async_remote_copy(
+            src_ref=source,
+            dst_ref=(hx, hb, hc)[k].at[side],
+            send_sem=hs.at[3 * side + k],
+            recv_sem=hr.at[3 * side + k],
+            device_id=(there, tp),
+            device_id_type=MESH,
+        )
+
+    for k in range(3):
+        halo(0, k).start()
+        halo(1, k).start()
+    lax.fori_loop(1, TP, send_tile, 0)
 
     lower = one_hot((T, T), lambda row, col: col < row)
     upper = one_hot((T, T), lambda row, col: row < col)
@@ -272,35 +289,12 @@
     cv[...] = stacked(weigh + seen)
     ends = [jnp.broadcast_to(forward_end, (1, 128)), jnp.broadcast_to(backward_end, (1, 128))]
 
-    for load in grouped:
-        load.wait()
-    pl.semaphore_wait(barrier, TP + SP - 2)
-
-    def halo(side, k):
-        there = (sp + 1) % SP if side == 0 else (sp + SP - 1) % SP
-        rows = pl.ds(T - 16, 16) if side == 0 else pl.ds(0, 16)
-        lanes = pl.ds(256, 128) if side == 0 else pl.ds(0, 128)
-        source = (xpad.at[:, lanes], braw.at[rows], craw.at[rows])[k]
-        return pltpu.make_async_remote_copy(
-            src_ref=source,
-            dst_ref=(hx, hb, hc)[k].at[side],
-            send_sem=hs.at[3 * side + k],
-            recv_sem=hr.at[3 * side + k],
-            device_id=(there, tp),
-            device_id_type=MESH,
-        )
-
-    for k in range(3):
-        halo(0, k).start()
-        halo(1, k).start()
-    lax.fori_loop(1, TP, send_tile, 0)
-
-    def to_other(part):
+    def to_other(part, at):
         return pltpu.make_async_remote_copy(
             src_ref=part,
             dst_ref=part,
-            send_sem=one.at[12],
-            recv_sem=one.at[13],
+            send_sem=one.at[at],
+            recv_sem=one.at[at + 1],
             device_id=(sp, y * 2 + 1 - core),
             device_id_type=MESH,
         )
@@ -308,7 +302,7 @@
     for k in (1, 2, 3):
         loads[k].wait()
     for part in (wx.at[:, lanes_of(core)], wx.at[:, lanes_of(core + 2)], wl.at[:, lanes_of(core)]):
-        to_other(part).start()
+        to_other(part, 12).start()
 
     taps = across(same[0:64, 0:64], stacked([xk_ref[j : j + 1, :].astype(F32) for j in range(CONV)]).astype(BF16))
     lane = lax.broadcasted_iota(jnp.int32, (64, 128), 1)
@@ -400,6 +394,11 @@
     for k in (4, 3, 5, 2, 6, 1, 7):
         state_column(k, z).start()
 
+    for k in (4, 5, 6):
+        loads[k].wait()
+    for part in (wc.at[:, lanes_of(core)], wc.at[:, lanes_of(core + 2)], wcl.at[:, lanes_of(core)]):
+        to_other(part, 18).start()
+
     loads[0].wait()
     wide[...] = jnp.zeros(wide.shape, BF16)
 
@@ -462,7 +461,8 @@
         )
 
     all_tiles(ft, 4).wait_recv()
-    run([ring])
+    for step in (4, 3, 2, 1):
+        ring.step(step)
     ring.finish()
 
     left = lax.broadcasted_iota(jnp.int32, (HALF, 128), 1) < 64
@@ -579,7 +579,7 @@
         def _():
             more()
 
-    for step in (1, 2):
+    for step in (1, 2, 3):
         for ring in spread_out:
             ring.step(step)
     chip = pl.ds(pl.multiple_of(y * 256, 256), 256)
@@ -629,36 +629,37 @@
         sl[rows_of(local), :] = ss[rows_of(sp), :]
 
     for ring in spread_out:
-        ring.step(3)
+        ring.step(4)
+
+    opposite = (y + NY // 2) % NY
+    d2[...] = dot(pp[...], ff[:, lanes_of(opposite * 2 + core)]).astype(BF16)
+
+    def send_more(m, carry):
+        deliver(outward(m), 1).start()
+        return carry
+
+    lax.fori_loop(0, SP - 1, send_more, 0)
+
+    @pl.when(side_of == core)
+    def _():
+        x2[rows_of(local), lanes_of(core)] = d2[rows_of(sp)]
+
+    @pl.when(side_of != core)
+    def _():
+        deliver(0, 1).start()
+
     for ring in gathers:
         ring.step(1)
     for ring in spread_out:
-        ring.step(4)
-
-    opposite = (y + NY // 2) % NY
-    d2[...] = dot(pp[...], ff[:, lanes_of(opposite * 2 + core)]).astype(BF16)
-
-    def send_more(m, carry):
-        deliver(outward(m), 1).start()
-        return carry
-
-    lax.fori_loop(0, SP - 1, send_more, 0)
-
-    @pl.when(side_of == core)
-    def _():
-        x2[rows_of(local), lanes_of(core)] = d2[rows_of(sp)]
-
-    @pl.when(side_of != core)
-    def _():
-        deliver(0, 1).start()
-
-    for ring in spread_out:
         ring.finish()
-    loads[4].wait()
-    loads[5].wait()
-    both = dot(ff[...], wc[...]) * scale
-    sh[:, mine] = (jax.nn.silu(both[:, 0:128]) * both[:, 128:256]).astype(BF16)
-    shared_out = [Ring(sh, i * HALF, HALF, sems, 4 + SPLITS + i) for i in range(2)]
+    to_other(wc.at[:, pl.ds(0, 384)], 18).wait_recv()
+    rows = pl.ds(pl.multiple_of(core * HALF, 16), HALF)
+    both = dot(ff[rows, :], wc[...]) * jnp.where(core == 0, scale[0:HALF], scale[HALF:T])
+    sh[rows, chip] = (jax.nn.silu(both[:, 0:256]) * both[:, 256:512]).astype(BF16)
+    shared_out = [
+        Ring(sh, pl.multiple_of(core * HALF + first, 16), count, sems, 4 + SPLITS + i, pair=True)
+        for i, (first, count) in enumerate(((0, 96), (96, 64)))
+    ]
     for ring in shared_out:
         ring.start()
     for ring in gathers:
@@ -672,13 +673,12 @@
 
         lax.fori_loop(first, first + count, add, 0)
 
-    weights = wx.at[:, pl.ds(0, 384)]
-    to_other(weights).wait_recv()
     either(
         side_of == core,
         lambda: some_rows(sl, 0, SP // 2 - 1, 14, one.at[15]).wait_recv(),
         lambda: some_rows(sl, 0, SP // 2, 14, one.at[15]).wait_recv(),
     )
+    to_other(wx.at[:, pl.ds(0, 384)], 12).wait_recv()
     tot[...] = jnp.zeros(tot.shape, F32)
     levels = []
     for q in range(CHUNKS):
@@ -717,15 +717,16 @@
     for sent in (8, 9):
         either(
             side_of == core,
-            lambda: some_rows(dd, 0, SP - 1, sent, one.at[16]).wait_send(),
-            lambda: some_rows(dd, 0, SP, sent, one.at[16]).wait_send(),
+            lambda: some_rows(dd, 0, SP - 1, sent, one.at[20]).wait_send(),
+            lambda: some_rows(dd, 0, SP, sent, one.at[20]).wait_send(),
         )
 
     @pl.when(side_of == core)
     def _():
-        some_rows(dd, 0, SP - 1, 14, one.at[16]).wait_send()
-
-    to_other(weights).wait_send()
+        some_rows(dd, 0, SP - 1, 14, one.at[20]).wait_send()
+
+    to_other(wx.at[:, pl.ds(0, 384)], 12).wait_send()
+    to_other(wc.at[:, pl.ds(0, 384)], 18).wait_send()
     for ring in spread_out + gathers:
         ring.drain()
     low[...] = jnp.zeros(low.shape, F32)
@@ -780,11 +781,21 @@
     for step in (3, 4):
         for ring in shared_out:
             ring.step(step)
-    for ring in shared_out:
-        ring.finish()
-    loads[6].wait()
-    shared = dot(sh[...], wcl[...]).astype(BF16).astype(F32)
-    out_ref[...] = shared.astype(BF16)
+    lowered = dot(sh[rows, :], wcl[...]).astype(BF16)
+    outs[0] = lowered[:, 0:128]
+    outs[1] = lowered[:, 128:256]
+
+    def output(source):
+        return pltpu.make_async_remote_copy(
+            src_ref=outs.at[source],
+            dst_ref=theirs,
+            send_sem=one.at[16],
+            recv_sem=one.at[17],
+            device_id=(sp, y * 2 + 1 - core),
+            device_id_type=MESH,
+        )
+
+    output(1 - core).start()
     for ring in hiddens + shared_out:
         ring.drain()
     either(
@@ -798,7 +809,12 @@
         lambda: some_rows(ret, 0, SP, 10, one.at[11]).wait_send(),
     )
     routed = dot(qhi[...], ret[...]) + dot(qlo[...], ret[...])
-    out_ref[...] = (am[...].astype(F32) + out_ref[...].astype(F32) + routed).astype(BF16)
+    output(1 - core).wait()
+    ours, others = outs[core].astype(F32), theirs[...].astype(F32)
+    shared = jnp.concatenate(
+        [jnp.where(core == 0, ours, others), jnp.where(core == 0, others, ours)], axis=0
+    )
+    out_ref[...] = (am[...].astype(F32) + shared + routed).astype(BF16)
 
 
 def whole(*operands):
@@ -837,9 +853,9 @@
             space(8, 128, kind=F32),
             space(1024, 128),
             space(D, 512),
+            space(D, 512),
             space(D, 256),
             space(D, 256),
-            space(D, 128),
             space(D, 256),
             space(HALF, D),
             space(HALF, D),
@@ -856,12 +872,14 @@
             space(ROWS, 128),
             space(ROWS, 128),
             space(ROWS // 2, 128),
+            space(2, HALF, 128),
+            space(HALF, 128),
             space(ROWS // 2, 256),
             space(ROWS, 128),
             space(ROWS, T),
             space(T, ROWS),
             space(T, ROWS),
-            dma((9,)), dma((6,)), dma((6,)), dma((17,)), dma((2 * CHUNKS,)), dma((rings, 2)), dma((rings, 8)),
+            dma((9,)), dma((6,)), dma((6,)), dma((21,)), dma((2 * CHUNKS,)), dma((rings, 2)), dma((rings, 8)),
         ],
         compiler_params=pltpu.CompilerParams(collective_id=0, has_side_effects=True),
         name="mixer_experts",

time: 106 us -> 105 us (level)
  no operation moved by 1% of the time
where the time goes in v7:
time: 105 us
  Pallas kernels  103 us (98%)
  local copies, waits for them, and re-layouts  1.53 us (1%)
    pallas_call x1, Pallas kernels, whole(): pl.pallas_call(kernel, out_shape=jax.ShapeDtypeStruct((T, 128), BF16), in...  103 us

profile of v7, /device:TPU:1, one launch (start us, length us, event | category | flops | bytes accessed | tf_op | source)
XLA Modules:
  0.0 104.9 jit_solution(2571678727305981594)
XLA Ops:
  0.7 102.7 %mixer_experts.1 = bf16[320,128]{1,0:T(8,128)(2,1)} custom-call(bf16[64,320]{1,0:T(8,128)(2,1)} %bitcast.12, bf16[64,320]{1,0:T(8,128)(2,1)} %bitcast.13, bf16[2,320]{1,0:T(2,128)(2,1)} %bitcast.17, f32[1,2]{1,0:T(1,128)} %bitcast.18, f32[1,2]{1,0:T(1,128)} %bitcast.19, f32[2,1,320]{2,1,0:T(1,128)} %bitcast.14, f32[1,1]{1,0:T(1,128)} %bitcast.11.byp_ref, ...), custom_call_target="tpu_custom_call" | custom-call | tf_op jit(solution)/shard_map/mixer_experts/pallas_call | solution.py:829
  103.3 1.5 %copy.27 = bf16[320,128]{1,0:T(8,128)(2,1)} copy(bf16[320,128]{1,0:T(8,128)(2,1)} %mixer_experts.1) | data formatting | bytes 163840

commit v8 on v7

--- a/solution.py
+++ b/solution.py
@@ -22,6 +22,7 @@
 SPLITS = 4
 BLOCK = 80
 CHUNKS = 2
+PIECE = SLOTS // CHUNKS
 MESH = pl.DeviceIdType.MESH
 F32, BF16 = jnp.float32, jnp.bfloat16
 
@@ -488,16 +489,30 @@
     def rows_of(i):
         return pl.ds(pl.multiple_of(i * SLOTS, SLOTS), SLOTS)
 
-    per = SP // 2 // CHUNKS
     local = (x % 2) * 8 + (x // 2) * 4 + z // 2
-
-    def deliver(k, far=0):
+    landing = pl.ds(pl.multiple_of(local * PIECE, PIECE), PIECE)
+
+    def piece_of(i, q):
+        return pl.ds(pl.multiple_of(i * SLOTS + q * PIECE, PIECE), PIECE)
+
+    def deliver(k, q):
         target = (sp + k) % SP
         return pltpu.make_async_remote_copy(
-            src_ref=(d2 if far else dd).at[rows_of(target)],
-            dst_ref=(x2 if far else xl).at[rows_of(local), lanes_of(core)],
-            send_sem=one.at[9 if far else 8],
-            recv_sem=dr.at[local // per + CHUNKS * far],
+            src_ref=dd.at[piece_of(target, q)],
+            dst_ref=xl.at[q, landing, lanes_of(core)],
+            send_sem=one.at[8],
+            recv_sem=dr.at[q],
+            device_id=(target, y * 2 + side_of),
+            device_id_type=MESH,
+        )
+
+    def deliver_more(k):
+        target = (sp + k) % SP
+        return pltpu.make_async_remote_copy(
+            src_ref=d2.at[rows_of(target)],
+            dst_ref=x2.at[rows_of(local), lanes_of(core)],
+            send_sem=one.at[9],
+            recv_sem=dr.at[CHUNKS],
             device_id=(target, y * 2 + side_of),
             device_id_type=MESH,
         )
@@ -505,19 +520,22 @@
     def outward(m):
         return SP // 2 + (m // 2 + m % 2) * (1 - 2 * (m % 2))
 
-    def send_rows(m, carry):
-        deliver(outward(m)).start()
-        return carry
-
-    lax.fori_loop(0, SP - 1, send_rows, 0)
+    for q in range(CHUNKS):
+
+        def send_rows(m, carry):
+            deliver(outward(m), q).start()
+            return carry
+
+        lax.fori_loop(0, SP - 1, send_rows, 0)
+
+        @pl.when(side_of != core)
+        def _():
+            deliver(0, q).start()
 
     @pl.when(side_of == core)
     def _():
-        xl[rows_of(local), lanes_of(core)] = dd[rows_of(sp)]
-
-    @pl.when(side_of != core)
-    def _():
-        deliver(0).start()
+        for q in range(CHUNKS):
+            xl[q, landing, lanes_of(core)] = dd[piece_of(sp, q)]
 
     cells = T // SPLITS
     spread_out = [Ring(ff, i * cells, cells, sems, 4 + i) for i in range(SPLITS)]
@@ -559,8 +577,8 @@
     lax.fori_loop(0, TP - 1, send_sums, 0)
     ring.drain()
 
-    def some_rows(ref, first, blocks, sent, received):
-        part = ref.at[pl.ds(first, blocks * SLOTS), pl.ds(0, 128)]
+    def some_rows(ref, first, blocks, sent, received, rows=SLOTS):
+        part = ref.at[pl.ds(first, blocks * rows), pl.ds(0, 128)]
         return pltpu.make_async_remote_copy(
             src_ref=part,
             dst_ref=part,
@@ -579,23 +597,41 @@
         def _():
             more()
 
-    for step in (1, 2, 3):
+    for step in (1, 2):
         for ring in spread_out:
             ring.step(step)
     chip = pl.ds(pl.multiple_of(y * 256, 256), 256)
-    packed_rows = per * CAP
-    dense = one_hot((packed_rows, per * SLOTS), lambda row, col: row // CAP * SLOTS + row % CAP == col)
+    used = [PIECE, CAP - PIECE]
+    sources = SP // 2
+    spans = [pl.ds(0, sources * used[0]), pl.ds(sources * used[0], sources * used[1])]
+    dense = [
+        one_hot(
+            (sources * used[q], sources * SLOTS),
+            lambda row, col: row // used[q] * SLOTS + row % used[q] + q * PIECE == col,
+        )
+        for q in range(CHUNKS)
+    ]
+    squeeze = one_hot(
+        (sources * used[1], sources * PIECE),
+        lambda row, col: row // used[1] * PIECE + row % used[1] == col,
+    )
     gathers = []
-    for q in range(CHUNKS):
+
+    def gather(q):
         either(
-            jnp.logical_and(side_of == core, x % 2 == q),
-            lambda: some_rows(xl, 0, 2 * per - 1, 8, dr.at[q]).wait_recv(),
-            lambda: some_rows(xl, 0, 2 * per, 8, dr.at[q]).wait_recv(),
-        )
-        at = pl.ds(q * packed_rows, packed_rows)
-        xx[at, chip] = dot(dense, xl[pl.ds(q * per * SLOTS, per * SLOTS), :]).astype(BF16)
-        gathers.append(Ring(xx, q * packed_rows, packed_rows, sems, q, pair=True, last=3))
-        gathers[-1].start()
+            side_of == core,
+            lambda: some_rows(dd, 0, SP - 1, 8, dr.at[q], PIECE).wait_recv(),
+            lambda: some_rows(dd, 0, SP, 8, dr.at[q], PIECE).wait_recv(),
+        )
+        if used[q] == PIECE:
+            xx[spans[q], chip] = xl[q]
+        else:
+            xx[spans[q], chip] = dot(squeeze, xl[q]).astype(BF16)
+        ring = Ring(xx, sources * used[0] * q, sources * used[q], sems, q, pair=True, last=3)
+        ring.start()
+        gathers.append(ring)
+
+    gather(0)
     all_tiles(sq, 6).wait_recv()
     total = sq[0]
     for j in range(1, TP):
@@ -628,6 +664,11 @@
         lax.fori_loop(0, SP - 1, send_scale, 0)
         sl[rows_of(local), :] = ss[rows_of(sp), :]
 
+    gather(1)
+    for ring in spread_out:
+        ring.step(3)
+    for ring in gathers:
+        ring.step(1)
     for ring in spread_out:
         ring.step(4)
 
@@ -635,7 +676,7 @@
     d2[...] = dot(pp[...], ff[:, lanes_of(opposite * 2 + core)]).astype(BF16)
 
     def send_more(m, carry):
-        deliver(outward(m), 1).start()
+        deliver_more(outward(m)).start()
         return carry
 
     lax.fori_loop(0, SP - 1, send_more, 0)
@@ -646,10 +687,8 @@
 
     @pl.when(side_of != core)
     def _():
-        deliver(0, 1).start()
-
-    for ring in gathers:
-        ring.step(1)
+        deliver_more(0).start()
+
     for ring in spread_out:
         ring.finish()
     to_other(wc.at[:, pl.ds(0, 384)], 18).wait_recv()
@@ -682,17 +721,18 @@
     tot[...] = jnp.zeros(tot.shape, F32)
     levels = []
     for q in range(CHUNKS):
-        at = pl.ds(q * packed_rows, packed_rows)
-        chips(NY - 2, NY - 3, tot, xx, at, wx)
-        either(
-            jnp.logical_and(side_of == core, x % 2 == q),
-            lambda: some_rows(x2, 0, 2 * per - 1, 9, dr.at[CHUNKS + q]).wait_recv(),
-            lambda: some_rows(x2, 0, 2 * per, 9, dr.at[CHUNKS + q]).wait_recv(),
-        )
-        turned = pl.ds(pl.multiple_of(opposite * 256, 256), 256)
-        xx[at, turned] = dot(dense, x2[pl.ds(q * per * SLOTS, per * SLOTS), :]).astype(BF16)
+        chips(NY - 2, NY - 3, tot, xx, spans[q], wx)
+    either(
+        side_of == core,
+        lambda: some_rows(d2, 0, SP - 1, 9, dr.at[CHUNKS]).wait_recv(),
+        lambda: some_rows(d2, 0, SP, 9, dr.at[CHUNKS]).wait_recv(),
+    )
+    turned = pl.ds(pl.multiple_of(opposite * 256, 256), 256)
+    for q in range(CHUNKS):
+        at = spans[q]
+        xx[at, turned] = dot(dense[q], x2[...]).astype(BF16)
         chips(NY // 2, 1, tot, xx, at, wx)
-        level = dot(dense, sl[pl.ds(q * per * SLOTS, per * SLOTS), :])
+        level = dot(dense[q], sl[...])
         levels.append(level[:, 0:1] + level[:, 1:2] + level[:, 2:3])
     hiddens = []
     for q in range(CHUNKS):
@@ -700,12 +740,12 @@
         if q == CHUNKS - 1:
             for ring in shared_out:
                 ring.step(1)
-        at = pl.ds(q * packed_rows, packed_rows)
+        at = spans[q]
         chips(3, 1, tot, xx, at, wx)
         chips(NY - 3, 1, tot, xx, at, wx)
         both = tot[at, :] * levels[q]
         hh[at, chip] = (jax.nn.silu(both[:, 0:256]) * both[:, 256:512]).astype(BF16)
-        hiddens.append(Ring(hh, q * packed_rows, packed_rows, sems, 2 + q, pair=True))
+        hiddens.append(Ring(hh, sources * used[0] * q, sources * used[q], sems, 2 + q, pair=True))
         hiddens[-1].start()
     for side in range(2):
         for k in range(3):
@@ -737,17 +777,23 @@
             for ring in shared_out:
                 ring.step(2)
         for q in range(CHUNKS):
-            at = pl.ds(q * packed_rows, packed_rows)
+            at = spans[q]
             if step == 1:
                 chips(NY, 1, low, hh, at, wl)
             chips(step, 1, low, hh, at, wl)
             chips(NY - step, 1, low, hh, at, wl)
-    loose = one_hot((per * SLOTS, packed_rows), lambda row, col: col // CAP * SLOTS + col % CAP == row)
-
-    def give(i, to_core):
-        return pltpu.make_async_remote_copy(
-            src_ref=oo.at[rows_of(i), lanes_of(to_core)],
-            dst_ref=ret.at[rows_of(sp)],
+    loose = [
+        one_hot(
+            (sources * PIECE, sources * used[q]),
+            lambda row, col: col // used[q] * PIECE + col % used[q] == row,
+        )
+        for q in range(CHUNKS)
+    ]
+
+    def give(i, to_core, q):
+        return pltpu.make_async_remote_copy(
+            src_ref=oo.at[q, pl.ds(pl.multiple_of(i * PIECE, PIECE), PIECE), lanes_of(to_core)],
+            dst_ref=ret.at[piece_of(sp, q)],
             send_sem=one.at[10],
             recv_sem=one.at[11],
             device_id=(((i % 4) * 2 + core) * NX + i // 4 % 2 * 2 + i // 8, y * 2 + to_core),
@@ -756,27 +802,28 @@
 
     for q in range(CHUNKS):
         hiddens[q].step(4)
-        at = pl.ds(q * packed_rows, packed_rows)
+        at = spans[q]
         chips(NY // 2, 1, low, hh, at, wl)
-        oo[pl.ds(q * per * SLOTS, per * SLOTS), :] = dot(loose, low[at, :].astype(BF16)).astype(BF16)
+        oo[q] = dot(loose[q], low[at, :].astype(BF16)).astype(BF16)
 
         def send_back(k, carry):
-            turn = k // 2
-            i = q * per + k % 2 * 4 + (z // 2 + 6 + (turn // 2 + turn % 2) * (1 - 2 * (turn % 2))) % 4
+            turn = k // 4
+            i = k % 4 * 4 + (z // 2 + 6 + (turn // 2 + turn % 2) * (1 - 2 * (turn % 2))) % 4
             here = jnp.logical_and(side_of == core, i == local)
 
             @pl.when(jnp.logical_not(here))
             def _():
-                give(i, core).start()
-
-            give(i, 1 - core).start()
+                give(i, core, q).start()
+
+            give(i, 1 - core, q).start()
             return carry
 
-        lax.fori_loop(0, per, send_back, 0)
+        lax.fori_loop(0, sources, send_back, 0)
 
     @pl.when(side_of == core)
     def _():
-        ret[rows_of(sp), :] = oo[rows_of(local), lanes_of(core)]
+        for q in range(CHUNKS):
+            ret[piece_of(sp, q), :] = oo[q, landing, lanes_of(core)]
 
     for step in (3, 4):
         for ring in shared_out:
@@ -862,7 +909,7 @@
             space(T, 128),
             space(T, D),
             space(T, D),
-            space(ROWS // 2, 256),
+            space(2, ROWS // 4, 256),
             space(ROWS // 2, 256),
             space(SP // 2 * CAP, D),
             space(SP // 2 * CAP, D),
@@ -874,12 +921,12 @@
             space(ROWS // 2, 128),
             space(2, HALF, 128),
             space(HALF, 128),
-            space(ROWS // 2, 256),
+            space(2, ROWS // 4, 256),
             space(ROWS, 128),
             space(ROWS, T),
             space(T, ROWS),
             space(T, ROWS),
-            dma((9,)), dma((6,)), dma((6,)), dma((21,)), dma((2 * CHUNKS,)), dma((rings, 2)), dma((rings, 8)),
+            dma((9,)), dma((6,)), dma((6,)), dma((21,)), dma((CHUNKS + 1,)), dma((rings, 2)), dma((rings, 8)),
         ],
         compiler_params=pltpu.CompilerParams(collective_id=0, has_side_effects=True),
         name="mixer_experts",

time: 105 us -> 106 us (level)
  no operation moved by 1% of the time
where the time goes in v8:
time: 106 us; the launch traced here: 105 us
  Pallas kernels  103 us (97%)
  local copies, waits for them, and re-layouts  1.53 us (1%)
    pallas_call x1, Pallas kernels, whole(): pl.pallas_call(kernel, out_shape=jax.ShapeDtypeStruct((T, 128), BF16), in...  103 us

profile of v8, /device:TPU:1, one launch (start us, length us, event | category | flops | bytes accessed | tf_op | source)
XLA Modules:
  0.0 105.5 jit_solution(18360033165380653026)
XLA Ops:
  0.7 103.3 %mixer_experts.1 = bf16[320,128]{1,0:T(8,128)(2,1)} custom-call(bf16[64,320]{1,0:T(8,128)(2,1)} %bitcast.12, bf16[64,320]{1,0:T(8,128)(2,1)} %bitcast.13, bf16[2,320]{1,0:T(2,128)(2,1)} %bitcast.17, f32[1,2]{1,0:T(1,128)} %bitcast.18, f32[1,2]{1,0:T(1,128)} %bitcast.19, f32[2,1,320]{2,1,0:T(1,128)} %bitcast.14, f32[1,1]{1,0:T(1,128)} %bitcast.11.byp_ref, ...), custom_call_target="tpu_custom_call" | custom-call | tf_op jit(solution)/shard_map/mixer_experts/pallas_call | solution.py:876
  103.9 1.5 %copy.27 = bf16[320,128]{1,0:T(8,128)(2,1)} copy(bf16[320,128]{1,0:T(8,128)(2,1)} %mixer_experts.1) | data formatting | bytes 163840

commit v9 on v8

--- a/solution.py
+++ b/solution.py
@@ -144,13 +144,15 @@
 
 
 def kernel(
-    xt_ref, zt_ref, inc_ref, off_ref, spd_ref, fade_ref, byp_ref, xk_ref, bk_ref, ck_ref, gain_ref,
-    after_ref, src_ref, cht_ref, sht_ref,
+    xt_hbm, zt_hbm, inc_hbm, off_hbm, spd_hbm, fade_hbm, byp_hbm, xk_hbm,
+    bk_hbm, ck_hbm, gain_hbm, after_hbm, src_hbm, cht_hbm, sht_hbm,
     bm_hbm, cm_hbm, blender_hbm, valve_hbm, raising_hbm, lowering_hbm, cvalve_hbm, craising_hbm, clowering_hbm,
     out_ref,
+    xt_ref, zt_ref, inc_ref, off_ref, spd_ref, fade_ref, byp_ref, xk_ref,
+    bk_ref, ck_ref, gain_ref, after_ref, src_ref, cht_ref, sht_ref,
     xpad, braw, craw, hx, hb, hc, bext, cext, gap, cv, mixed, fto,
     st_ref, rx, tb, rz, ft, sq, so, wb, wx, wc, wl, wcl, wide, bn, nn, am, ff, sh, xl, x2, xx, hh, tot, low, dd, d2, ss, sl, outs, theirs, oo, ret, pp, qhi, qlo,
-    wsem, hs, hr, one, dr, rsem, rrecv,
+    isem, wsem, hs, hr, one, dr, rsem, rrecv,
 ):
     sp, tp = lax.axis_index("sp"), lax.axis_index("tp")
     z, x = sp // NX, sp % NX
@@ -186,8 +188,32 @@
         pltpu.make_async_copy(bm_hbm.at[:, at_group], braw, wsem.at[7]),
         pltpu.make_async_copy(cm_hbm.at[:, at_group], craw, wsem.at[8]),
     ]
-    for load in grouped + loads:
+    small = [
+        pltpu.make_async_copy(there, here, isem.at[k])
+        for k, (there, here) in enumerate(
+            (
+                (xt_hbm, xt_ref),
+                (zt_hbm, zt_ref),
+                (inc_hbm, inc_ref),
+                (off_hbm, off_ref),
+                (spd_hbm, spd_ref),
+                (fade_hbm, fade_ref),
+                (byp_hbm, byp_ref),
+                (xk_hbm, xk_ref),
+                (bk_hbm, bk_ref),
+                (ck_hbm, ck_ref),
+                (gain_hbm, gain_ref),
+                (after_hbm, after_ref),
+                (src_hbm, src_ref),
+                (cht_hbm, cht_ref),
+                (sht_hbm, sht_ref),
+            )
+        )
+    ]
+    for load in small + grouped + loads:
         load.start()
+    for load in small:
+        load.wait()
 
     xpad[...] = jnp.zeros(xpad.shape, BF16)
     xpad[:, 0:T] = xt_ref[...]
@@ -348,7 +374,7 @@
     for k in (2, 1, 3):
         state_row(k, x).start()
     inner = across(x_conv, (across(c_conv, b_conv) * gap[...]).astype(BF16))
-    inner = inner + byp_ref[...] * x_wide
+    inner = inner + byp_ref[0] * x_wide
     gate = silu(zt_ref[...].astype(F32))
 
     def all_rows(k):
@@ -484,6 +510,10 @@
 
     own = (am[...].astype(F32) * after_ref[...]).astype(BF16)
     ff[:, mine] = own
+    cells = T // SPLITS
+    spread_out = [Ring(ff, i * cells, cells, sems, 4 + i) for i in range(SPLITS)]
+    for spreading in spread_out:
+        spreading.start()
     dd[...] = dot(pp[...], own).astype(BF16)
 
     def rows_of(i):
@@ -536,11 +566,6 @@
     def _():
         for q in range(CHUNKS):
             xl[q, landing, lanes_of(core)] = dd[piece_of(sp, q)]
-
-    cells = T // SPLITS
-    spread_out = [Ring(ff, i * cells, cells, sems, 4 + i) for i in range(SPLITS)]
-    for spreading in spread_out:
-        spreading.start()
 
     dims = (((1,), (1,)), ((), ()))
     squares = am[...].astype(F32) * am[...].astype(F32)
@@ -876,9 +901,12 @@
     return pl.pallas_call(
         kernel,
         out_shape=jax.ShapeDtypeStruct((T, 128), BF16),
-        in_specs=[vmem] * 15 + [hbm] * 9,
+        in_specs=[hbm] * 24,
         out_specs=vmem,
         scratch_shapes=[
+            (pltpu.VMEM if o.ndim > 1 else pltpu.SMEM)(o.shape, o.dtype) for o in operands[:15]
+        ]
+        + [
             space(64, 384),
             space(T, 128),
             space(T, 128),
@@ -926,7 +954,7 @@
             space(ROWS, T),
             space(T, ROWS),
             space(T, ROWS),
-            dma((9,)), dma((6,)), dma((6,)), dma((21,)), dma((CHUNKS + 1,)), dma((rings, 2)), dma((rings, 8)),
+            dma((15,)), dma((9,)), dma((6,)), dma((6,)), dma((21,)), dma((CHUNKS + 1,)), dma((rings, 2)), dma((rings, 8)),
         ],
         compiler_params=pltpu.CompilerParams(collective_id=0, has_side_effects=True),
         name="mixer_experts",
@@ -966,7 +994,7 @@
         increment_offset.T,
         log_fade_speed.T,
         extra_log_fade.reshape(2, 1, T),
-        attention_bypass_factor.reshape(1, 1),
+        attention_bypass_factor,
         attention_lane_kernel,
         memory_write_kernel,
         memory_query_kernel,

time: 106 us -> 104 us (0.981)
  Pallas kernels: 103 us -> 101 us
    pallas_call x1, Pallas kernels: 103 us -> 101 us  [whole(): pl.pallas_call(kernel, out_shape=jax.ShapeDtypeStruct((T, 128), BF16), in...]
where the time goes in v9:
time: 104 us; the launch traced here: 103 us
  Pallas kernels  101 us (97%)
  local copies, waits for them, and re-layouts  1.53 us (1%)
    pallas_call x1, Pallas kernels, whole(): pl.pallas_call(kernel, out_shape=jax.ShapeDtypeStruct((T, 128), BF16), in...  101 us

profile of v9, /device:TPU:1, one launch (start us, length us, event | category | flops | bytes accessed | tf_op | source)
XLA Modules:
  0.0 103.4 jit_solution(4593091195178886827)
XLA Ops:
  0.7 101.2 %mixer_experts.1 = bf16[320,128]{1,0:T(8,128)(2,1)} custom-call(bf16[64,320]{1,0:T(8,128)(2,1)} %bitcast.10, bf16[64,320]{1,0:T(8,128)(2,1)} %bitcast.11, bf16[2,320]{1,0:T(2,128)(2,1)} %bitcast.15, f32[1,2]{1,0:T(1,128)} %bitcast.16, f32[1,2]{1,0:T(1,128)} %bitcast.17, f32[2,1,320]{2,1,0:T(1,128)} %bitcast.12, f32[1]{0:T(128)S(6)} %copy.26.byp_hbm, ...), custom_call_target="tpu_custom_call" | custom-call | tf_op jit(solution)/shard_map/mixer_experts/pallas_call | solution.py:901
  101.9 1.5 %copy.27 = bf16[320,128]{1,0:T(8,128)(2,1)} copy(bf16[320,128]{1,0:T(8,128)(2,1)} %mixer_experts.1) | data formatting | bytes 163840

commit v10 on v9

--- a/solution.py
+++ b/solution.py
@@ -164,12 +164,28 @@
         pl.semaphore_signal(barrier, inc=1, device_id=(sp, (tp + k) % TP), device_id_type=MESH)
         return carry
 
-    def greet_sp(k, carry):
-        pl.semaphore_signal(barrier, inc=1, device_id=((sp + k) % SP, tp), device_id_type=MESH)
+    def greet_z(k, carry):
+        pl.semaphore_signal(
+            barrier, inc=1, device_id=((z + k) % NZ * NX + x, tp), device_id_type=MESH
+        )
         return carry
 
+    def greet_x(k, carry):
+        pl.semaphore_signal(
+            barrier, inc=1, device_id=(z * NX + (x + k) % NX, tp), device_id_type=MESH
+        )
+        return carry
+
+    def greet_next(k, carry):
+        pl.semaphore_signal(
+            barrier, inc=1, device_id=((sp + k * (SP - 2) + 1) % SP, tp), device_id_type=MESH
+        )
+        return carry
+
     lax.fori_loop(1, TP, greet_tp, 0)
-    lax.fori_loop(1, SP, greet_sp, 0)
+    lax.fori_loop(1, NZ, greet_z, 0)
+    lax.fori_loop(1, NX, greet_x, 0)
+    lax.fori_loop(0, 2, greet_next, 0)
 
     def lanes_of(i):
         return pl.ds(pl.multiple_of(i * 128, 128), 128)
@@ -247,7 +263,7 @@
 
     for load in grouped:
         load.wait()
-    pl.semaphore_wait(barrier, TP + SP - 2)
+    pl.semaphore_wait(barrier, TP - 1 + NZ - 1 + NX - 1 + 2)
 
     def halo(side, k):
         there = (sp + 1) % SP if side == 0 else (sp + SP - 1) % SP
@@ -326,10 +342,6 @@
             device_id_type=MESH,
         )
 
-    for k in (1, 2, 3):
-        loads[k].wait()
-    for part in (wx.at[:, lanes_of(core)], wx.at[:, lanes_of(core + 2)], wl.at[:, lanes_of(core)]):
-        to_other(part, 12).start()
 
     taps = across(same[0:64, 0:64], stacked([xk_ref[j : j + 1, :].astype(F32) for j in range(CONV)]).astype(BF16))
     lane = lax.broadcasted_iota(jnp.int32, (64, 128), 1)
@@ -420,11 +432,6 @@
 
     for k in (4, 3, 5, 2, 6, 1, 7):
         state_column(k, z).start()
-
-    for k in (4, 5, 6):
-        loads[k].wait()
-    for part in (wc.at[:, lanes_of(core)], wc.at[:, lanes_of(core + 2)], wcl.at[:, lanes_of(core)]):
-        to_other(part, 18).start()
 
     loads[0].wait()
     wide[...] = jnp.zeros(wide.shape, BF16)
@@ -567,6 +574,11 @@
         for q in range(CHUNKS):
             xl[q, landing, lanes_of(core)] = dd[piece_of(sp, q)]
 
+    for k in (4, 5, 6):
+        loads[k].wait()
+    for part in (wc.at[:, lanes_of(core)], wc.at[:, lanes_of(core + 2)], wcl.at[:, lanes_of(core)]):
+        to_other(part, 18).start()
+
     dims = (((1,), (1,)), ((), ()))
     squares = am[...].astype(F32) * am[...].astype(F32)
     high = squares.astype(BF16)
@@ -690,6 +702,10 @@
         sl[rows_of(local), :] = ss[rows_of(sp), :]
 
     gather(1)
+    for k in (1, 2, 3):
+        loads[k].wait()
+    for part in (wx.at[:, lanes_of(core)], wx.at[:, lanes_of(core + 2)], wl.at[:, lanes_of(core)]):
+        to_other(part, 12).start()
     for ring in spread_out:
         ring.step(3)
     for ring in gathers:

time: 104 us -> 103 us (level)
  no operation moved by 1% of the time
where the time goes in v10:
time: 103 us
  Pallas kernels  100 us (97%)
  local copies, waits for them, and re-layouts  1.53 us (1%)
    pallas_call x1, Pallas kernels, whole(): pl.pallas_call(kernel, out_shape=jax.ShapeDtypeStruct((T, 128), BF16), in...  100 us

profile of v10, /device:TPU:1, one launch (start us, length us, event | category | flops | bytes accessed | tf_op | source)
XLA Modules:
  0.0 102.7 jit_solution(13769365882424022419)
XLA Ops:
  0.7 100.5 %mixer_experts.1 = bf16[320,128]{1,0:T(8,128)(2,1)} custom-call(bf16[64,320]{1,0:T(8,128)(2,1)} %bitcast.10, bf16[64,320]{1,0:T(8,128)(2,1)} %bitcast.11, bf16[2,320]{1,0:T(2,128)(2,1)} %bitcast.15, f32[1,2]{1,0:T(1,128)} %bitcast.16, f32[1,2]{1,0:T(1,128)} %bitcast.17, f32[2,1,320]{2,1,0:T(1,128)} %bitcast.12, f32[1]{0:T(128)S(6)} %copy.26.byp_hbm, ...), custom_call_target="tpu_custom_call" | custom-call | tf_op jit(solution)/shard_map/mixer_experts/pallas_call | solution.py:917
  101.1 1.5 %copy.27 = bf16[320,128]{1,0:T(8,128)(2,1)} copy(bf16[320,128]{1,0:T(8,128)(2,1)} %mixer_experts.1) | data formatting | bytes 163840

commit v11 on v10

--- a/solution.py
+++ b/solution.py
@@ -701,15 +701,14 @@
         lax.fori_loop(0, SP - 1, send_scale, 0)
         sl[rows_of(local), :] = ss[rows_of(sp), :]
 
+    for ring in spread_out:
+        ring.step(3)
     gather(1)
     for k in (1, 2, 3):
         loads[k].wait()
     for part in (wx.at[:, lanes_of(core)], wx.at[:, lanes_of(core + 2)], wl.at[:, lanes_of(core)]):
         to_other(part, 12).start()
-    for ring in spread_out:
-        ring.step(3)
-    for ring in gathers:
-        ring.step(1)
+    gathers[0].step(1)
     for ring in spread_out:
         ring.step(4)
 
@@ -730,6 +729,7 @@
     def _():
         deliver_more(0).start()
 
+    gathers[1].step(1)
     for ring in spread_out:
         ring.finish()
     to_other(wc.at[:, pl.ds(0, 384)], 18).wait_recv()

time: 103 us -> 102 us (level)
  no operation moved by 1% of the time
where the time goes in v11:
time: 102 us
  Pallas kernels  99.8 us (98%)
  local copies, waits for them, and re-layouts  1.53 us (2%)
    pallas_call x1, Pallas kernels, whole(): pl.pallas_call(kernel, out_shape=jax.ShapeDtypeStruct((T, 128), BF16), in...  99.8 us

profile of v11, /device:TPU:1, one launch (start us, length us, event | category | flops | bytes accessed | tf_op | source)
XLA Modules:
  0.0 102.0 jit_solution(3047024029449709132)
XLA Ops:
  0.7 99.8 %mixer_experts.1 = bf16[320,128]{1,0:T(8,128)(2,1)} custom-call(bf16[64,320]{1,0:T(8,128)(2,1)} %bitcast.10, bf16[64,320]{1,0:T(8,128)(2,1)} %bitcast.11, bf16[2,320]{1,0:T(2,128)(2,1)} %bitcast.15, f32[1,2]{1,0:T(1,128)} %bitcast.16, f32[1,2]{1,0:T(1,128)} %bitcast.17, f32[2,1,320]{2,1,0:T(1,128)} %bitcast.12, f32[1]{0:T(128)S(6)} %copy.26.byp_hbm, ...), custom_call_target="tpu_custom_call" | custom-call | tf_op jit(solution)/shard_map/mixer_experts/pallas_call | solution.py:917
  100.5 1.5 %copy.27 = bf16[320,128]{1,0:T(8,128)(2,1)} copy(bf16[320,128]{1,0:T(8,128)(2,1)} %mixer_experts.1) | data formatting | bytes 163840
